TPU v7x, 512 devices: a whole 4x4x16 slice. The times are simulated.
512 devices in a mesh: dp: 4 (over x), kv: 64 (over z, y), tp: 2 (over core).
Axes of the slice: x: 4, y: 4, z: 16, core: 2. Of those that a mesh axis runs over, the one named last changes fastest.
Arguments:
- tokens: bfloat16 [256, 4096], P('dp', 'kv'), may hold values from -24 to 24
- positions: int32 [256], P(('dp', 'kv')), may hold values from 0 to 4095
- state: float32 [256, 16, 128, 128], P(('dp', 'kv'), 'tp'), may hold values from -0.6 to 0.6
- w_query: bfloat16 [4096, 2048], P('kv', 'tp'), may hold values from -0.09375 to 0.09375
- w_key: bfloat16 [4096, 2048], P('kv', 'tp'), may hold values from -0.09375 to 0.09375
- w_value: bfloat16 [4096, 2048], P('kv', 'tp'), may hold values from -0.09375 to 0.09375
- w_gate: bfloat16 [4096, 2048], P('kv', 'tp'), may hold values from -0.09375 to 0.09375
- w_out: bfloat16 [2048, 4096], P(None, ('kv', 'tp')), may hold values from -0.25 to 0.25
- gain_mix: float32 [4096], replicated, may hold values from 0.1 to 1.9
- w_ffn_gate: bfloat16 [4096, 11008], P(None, ('kv', 'tp')), may hold values from -0.09375 to 0.09375
- w_ffn_up: bfloat16 [4096, 11008], P(None, ('kv', 'tp')), may hold values from -0.09375 to 0.09375
- w_ffn_down: bfloat16 [11008, 4096], P(('kv', 'tp')), may hold values from -0.109375 to 0.109375
- gain_out: float32 [4096], replicated, may hold values from 0.1 to 1.9
Outputs:
- layer_out: bfloat16 [256, 4096], P('dp', ('kv', 'tp'))
- new_state: float32 [256, 16, 128, 128], P(('dp', 'kv'), 'tp')
All inputs are finite; a program needn't handle non-finite values.
Results may differ from a plain program's by a relative error of at most 0.018.
Values may be sent and summed in bfloat16 or wider, within the bound.
No kernel may reach another device: no remote copies, remote signals or barrier semaphores. Data moves between devices by JAX's collectives and lax.ppermute only.
A program may use at most 64 MiB of HBM per device.

v0:
```python
import jax
import jax.numpy as jnp
from jax import lax
from jax.sharding import Mesh
from jax.sharding import PartitionSpec as P

KV = ("kv_0", "kv_1")
KV_TP = ("kv_0", "kv_1", "tp")
DP_KV = ("dp", "kv_0", "kv_1")


def in_blocks(x, dim, count):
    dims = x.shape
    tiles = x.reshape(*dims[:dim], count, dims[dim] // count, *dims[dim + 1 :])
    return jnp.moveaxis(tiles, dim, 0)


def summed_on_arrival(x, axis, dim):
    tiles = in_blocks(x, dim, lax.axis_size(axis))
    arrived = lax.all_to_all(tiles, axis, split_axis=0, concat_axis=0, tiled=True)
    return arrived.sum(axis=0)


def sum_in_two_steps(x, axes, dim):
    far, near = axes
    own = summed_on_arrival(in_blocks(x, dim, lax.axis_size(far)), near, dim + 1)
    return jnp.sum(lax.all_to_all(own, far, 0, 0, tiled=True), axis=0)


def copy_for_each(x, axis):
    count = lax.axis_size(axis)
    return lax.all_to_all(jnp.broadcast_to(x[None], (count, *x.shape)), axis, 0, 0, tiled=True)


def joined_along(tiles, dim):
    dims = list(tiles.shape[1:])
    dims[dim] *= tiles.shape[0]
    return jnp.moveaxis(tiles, 0, dim).reshape(dims)


def whole_of(x, axes, dim):
    far, near = axes
    leading = copy_for_each(x, far)
    tiles = jnp.swapaxes(copy_for_each(leading, near), 0, 1)
    return joined_along(tiles.reshape(-1, *x.shape), dim)


def summed_on_arrival_2(x, axis, dim):
    count = lax.axis_size(axis)
    tiles = lax.all_to_all(in_blocks(x, dim, count), axis, 0, 0, tiled=True)
    return jnp.sum(tiles.astype(jnp.float32), axis=0)


def sum_in_two_steps_2(x, axes, dim):
    far, near = axes
    tiles = in_blocks(x, dim, lax.axis_size(far))
    nearer = summed_on_arrival_2(tiles, near, dim + 1)
    arrived = lax.all_to_all(
        nearer.astype(jnp.bfloat16), far, split_axis=0, concat_axis=0, tiled=True
    )
    return arrived.astype(jnp.float32).sum(axis=0)


def rows_for(lines, count):
    spare = -lines.shape[0] % count
    if not spare:
        return lines
    return jnp.concatenate([lines, jnp.zeros((spare, *lines.shape[1:]), lines.dtype)])


def nested_sum(x, axes):
    lines = x.reshape(-1)
    own = sum_in_two_steps_2(
        rows_for(lines, lax.axis_size(axes[0]) * lax.axis_size(axes[1])), axes, 0
    )
    whole = whole_of(own.astype(jnp.bfloat16), axes, 0)
    return whole[: len(lines)].reshape(x.shape).astype(jnp.float32)


def rotate(vectors, positions):
    half = vectors.shape[-1] // 2
    inverse = 10000.0 ** (-jnp.arange(half, dtype=jnp.float32) / half)
    angle = positions.astype(jnp.float32)[:, None, None] * inverse[None, None, :]
    cosine = jnp.cos(angle)
    sine = jnp.sin(angle)
    first = vectors[..., :half]
    second = vectors[..., half:]
    return jnp.concatenate([first * cosine - second * sine, first * sine + second * cosine], -1)


def finish_norm(values, sums, squares, count, gain):
    mean = sums / count
    var = squares / count - mean * mean
    return (values - mean[:, None]) * lax.rsqrt(var + 1e-05)[:, None] * gain[None, :]


def on_device(
    tokens,
    positions,
    state,
    w_query,
    w_key,
    w_value,
    w_gate,
    w_out,
    gain_mix,
    w_ffn_gate,
    w_ffn_up,
    w_ffn_down,
    gain_out,
):
    seqs = state.shape[0]
    heads = state.shape[1]
    width_head = state.shape[2]
    proj_cols = w_query.shape[1]
    width = w_ffn_gate.shape[0]
    cols = w_out.shape[1]
    group_rows = tokens.shape[0]
    kv_count = lax.axis_size(KV)
    tp_count = lax.axis_size("tp")
    tp_index = lax.axis_index("tp")
    col_start = (lax.axis_index(KV) * tp_count + tp_index) * cols
    projected = sum_in_two_steps(
        jnp.concatenate(
            [
                jnp.dot(tokens, w_query, preferred_element_type=jnp.float32),
                jnp.dot(tokens, w_key, preferred_element_type=jnp.float32),
                jnp.dot(tokens, w_value, preferred_element_type=jnp.float32),
                jnp.dot(tokens, w_gate, preferred_element_type=jnp.float32),
            ],
            axis=1,
        ),
        ("kv_0", "kv_1"),
        0,
    )
    query = projected[:, :proj_cols].reshape(seqs, heads, width_head)
    key = projected[:, proj_cols : 2 * proj_cols].reshape(seqs, heads, width_head)
    value = projected[:, 2 * proj_cols : 3 * proj_cols].reshape(seqs, heads, width_head)
    gate_pre = projected[:, 3 * proj_cols :]
    query = rotate(query, positions)
    key = rotate(key, positions) * width_head ** (-0.5)
    total_heads = heads * tp_count
    head_ids = (tp_index * heads + jnp.arange(heads, dtype=jnp.int32)).astype(jnp.float32)
    decay = 1.0 - 2.0 ** (-5.0 - 6.0 * head_ids / (total_heads - 1))
    new_state = decay[None, :, None, None] * state + key[:, :, :, None] * value[:, :, None, :]
    retained = jnp.einsum("bhd,bhdv->bhv", query, new_state, precision=lax.Precision.HIGHEST)
    mean = jnp.mean(retained, -1, keepdims=True)
    var = jnp.mean(jnp.square(retained - mean), -1, keepdims=True)
    normed = (retained - mean) * lax.rsqrt(var + 1e-05)
    attended = (normed.reshape(seqs, proj_cols) * jax.nn.silu(gate_pre)).astype(jnp.bfloat16)
    gathered = whole_of(attended[None], (("kv_0", "kv_1"), "tp"), 0)
    gathered = gathered.reshape(kv_count, tp_count, seqs, proj_cols)
    out_blocks = w_out.reshape(tp_count, proj_cols, cols)
    mixed = jnp.einsum(
        "itsc,tcd->isd", gathered, out_blocks, preferred_element_type=jnp.float32
    ).reshape(group_rows, cols)
    tokens_own = lax.dynamic_slice_in_dim(tokens, tp_index * cols, cols, 1)
    mixed_pre = (tokens_own.astype(jnp.float32) + mixed).astype(jnp.bfloat16)
    gain_out_own = lax.dynamic_slice_in_dim(gain_out, col_start, cols, 0)
    whole_rows = whole_of(mixed_pre, (("kv_0", "kv_1"), "tp"), 1).astype(jnp.float32)
    hidden = finish_norm(
        whole_rows, jnp.sum(whole_rows, 1), jnp.sum(whole_rows * whole_rows, 1), width, gain_mix
    ).astype(jnp.bfloat16)
    gate = jnp.dot(hidden, w_ffn_gate, preferred_element_type=jnp.float32)
    upward = jnp.dot(hidden, w_ffn_up, preferred_element_type=jnp.float32)
    inner = (jax.nn.silu(gate) * upward).astype(jnp.bfloat16)
    ffn = nested_sum(
        jnp.dot(inner, w_ffn_down, preferred_element_type=jnp.float32).astype(jnp.bfloat16),
        (("kv_0", "kv_1"), "tp"),
    )
    summed = hidden.astype(jnp.float32) + ffn
    out_sums = jnp.sum(summed, 1)
    out_squares = jnp.sum(summed * summed, 1)
    summed_own = lax.dynamic_slice_in_dim(summed, col_start, cols, 1)
    layer_out = finish_norm(summed_own, out_sums, out_squares, width, gain_out_own).astype(
        jnp.bfloat16
    )
    return (layer_out, new_state)


def solution(mesh):
    finer = Mesh(
        mesh.devices.reshape(mesh.shape["dp"], 16, 4, mesh.shape["tp"]),
        ("dp", "kv_0", "kv_1", "tp"),
    )
    return jax.shard_map(
        on_device,
        mesh=finer,
        in_specs=(
            P("dp", KV),
            P(DP_KV),
            P(DP_KV, "tp", None, None),
            P(KV, "tp"),
            P(KV, "tp"),
            P(KV, "tp"),
            P(KV, "tp"),
            P(None, KV_TP),
            P(),
            P(None, KV_TP),
            P(None, KV_TP),
            P(KV_TP, None),
            P(),
        ),
        out_specs=(P("dp", KV_TP), P(DP_KV, "tp", None, None)),
        check_vma=False,
    )
```

profile of v0, /device:TPU:1, one launch (start us, length us, event | category | flops | bytes accessed | tf_op | source)
XLA Modules:
  0.0 232.2 jit_solution(13392947138415657811)
XLA Ops:
  0.6 1.2 fusion.31
  1.8 1.1 fusion.30
  6.1 15.7 %all_to_all.55 = f32[4,16,1,4096]{3,1,2,0:T(8,128)S(1)} all-to-all(f32[4,16,1,4096]{3,1,2,0:T(8,128)S(1)} %bitcast.110), channel_id=1, replica_groups=mesh['dp'=4,'kv_0'=16,'kv_1'=4,'tp'=2] {'kv_1'}, dimensions={0} | all-to-all | bytes 2097152 | tf_op jit(solution)/shard_map/all_to_all | solution.py:20
  22.8 18.4 %all-to-all-start.1 = ((f32[16,1,4096]{2,1,0:T(1,128)}), f32[16,1,4096]{2,1,0:T(1,128)S(1)}, u32[]{:S(2)}, u32[]{:S(2)}) async-start(f32[16,1,4096]{2,1,0:T(1,128)} %reduce_sum.101), calls=%async_computation.1 | async-start | bytes 524288 | tf_op jit(solution)/shard_map/all_to_all | solution.py:27
  42.0 12.0 %all-to-all-done.1 = f32[16,1,4096]{2,1,0:T(1,128)S(1)} async-done(((f32[16,1,4096]{2,1,0:T(1,128)}), f32[16,1,4096]{2,1,0:T(1,128)S(1)}, u32[]{:S(2)}, u32[]{:S(2)}) %all-to-all-start.1) | async-done | bytes 262176 | tf_op jit(solution)/shard_map/all_to_all | solution.py:27
  57.1 1.4 reduce.19
  59.2 11.8 %all-to-all-start.2 = ((bf16[64,2,512]{2,1,0:T(2,128)(2,1)}), bf16[64,2,512]{2,1,0:T(2,128)(2,1)S(1)}, u32[]{:S(2)}, u32[]{:S(2)}) async-start(bf16[64,2,512]{2,1,0:T(2,128)(2,1)} %reshape.223), calls=%async_computation.2 | async-start | bytes 262144 | tf_op jit(solution)/shard_map/all_to_all | solution.py:32
  71.1 14.8 %all-to-all-done.2 = bf16[64,2,512]{2,1,0:T(2,128)(2,1)S(1)} async-done(((bf16[64,2,512]{2,1,0:T(2,128)(2,1)}), bf16[64,2,512]{2,1,0:T(2,128)(2,1)S(1)}, u32[]{:S(2)}, u32[]{:S(2)}) %all-to-all-start.2) | async-done | bytes 131104 | tf_op jit(solution)/shard_map/all_to_all | solution.py:32
  86.1 7.1 %all_to_all.56 = bf16[2,64,1,1,1024]{4,1,3,2,0:T(8,128)(2,1)S(1)} all-to-all(bf16[2,64,1,1,1024]{4,1,3,2,0:T(8,128)(2,1)S(1)} %broadcast_in_dim.21), channel_id=1, replica_groups=mesh['dp'=4,'kv_0'=16,'kv_1'=4,'tp'=2] {'tp'}, dimensions={0} | all-to-all | bytes 524288 | tf_op jit(solution)/shard_map/all_to_all | solution.py:32
  93.8 24.1 %all_to_all.57 = bf16[64,2,1024]{2,1,0:T(2,128)(2,1)S(1)} all-to-all(bf16[64,2,1024]{2,1,0:T(2,128)(2,1)S(1)} %reshape.225), channel_id=1, replica_groups=mesh['dp'=4,'kv_0'=16,'kv_1'=4,'tp'=2] {'kv_0','kv_1'}, dimensions={0} | all-to-all | bytes 524288 | tf_op jit(solution)/shard_map/all_to_all | solution.py:32
  119.2 7.1 %all_to_all.58 = bf16[2,2,65536]{2,1,0:T(2,128)(2,1)S(1)} all-to-all(bf16[2,2,65536]{2,1,0:T(2,128)(2,1)S(1)} %reshape.227), channel_id=1, replica_groups=mesh['dp'=4,'kv_0'=16,'kv_1'=4,'tp'=2] {'tp'}, dimensions={0} | all-to-all | bytes 1048576 | tf_op jit(solution)/shard_map/all_to_all | solution.py:32
  128.6 1.6 copy.29
  130.2 1.4 multiply_convert_fusion
  131.6 1.5 fusion.32
  133.1 2.7 %convolution_convert_fusion = bf16[64,4096]{1,0:T(8,128)(2,1)} fusion(bf16[86,4096]{1,0:T(8,128)(2,1)S(1)} %copy-done, bf16[64,4096]{1,0:T(8,128)(2,1)S(1)} %multiply_convert_fusion, bf16[4096,86]{0,1:T(8,128)(2,1)} %param.23, f32[64,86]{1,0:T(8,128)S(1)} %fusion.32), kind=kOutput, calls=%fused_computation | convolution fusion | flops 90472704 | bytes 2479616 | tf_op jit(solution)/shard_map/dot_general | solution.py:168
  136.9 4.9 %all_to_all.59 = bf16[2,64,2048]{2,1,0:T(8,128)(2,1)} all-to-all(bf16[2,64,2048]{2,1,0:T(8,128)(2,1)S(1)} %bitcast.113), channel_id=1, replica_groups=mesh['dp'=4,'kv_0'=16,'kv_1'=4,'tp'=2] {'tp'}, dimensions={0} | all-to-all | bytes 1048576 | tf_op jit(solution)/shard_map/all_to_all | solution.py:50
  141.8 1.9 reduce_sum.108
  143.7 2.4 %reduce.20 = bf16[64,2048]{1,0:T(8,128)(2,1)} reduce(bf16[64,1,2048]{2,0,1:T(8,128)(2,1)} %bitcast.116, bf16[]{:T(256)} %broadcast.235), dimensions={1}, to_apply=%copy.31.reduce_sub_computation | reduce | bytes 524290 | tf_op jit(solution)/shard_map/all_to_all | solution.py:58
  146.1 1.8 reshape.229
  148.0 26.1 %all_to_all.60 = bf16[64,2,1024]{2,1,0:T(2,128)(2,1)} all-to-all(bf16[64,2,1024]{2,1,0:T(2,128)(2,1)} %reshape.229), channel_id=1, replica_groups=mesh['dp'=4,'kv_0'=16,'kv_1'=4,'tp'=2] {'kv_0','kv_1'}, dimensions={0} | all-to-all | bytes 524288 | tf_op jit(solution)/shard_map/all_to_all | solution.py:58
  174.1 2.8 %reshape.230 = bf16[64,1,2048]{2,1,0:T(2,128)(2,1)} reshape(bf16[64,2,1024]{2,1,0:T(2,128)(2,1)} %all_to_all.60) | data formatting | bytes 524288
  176.8 1.5 reduce_sum.109
  179.4 3.8 %reduce.21 = bf16[64,2048]{1,0:T(8,128)(2,1)} reduce(bf16[64,1,2048]{2,1,0:T(2,128)(2,1)} %broadcast_in_dim.24, bf16[]{:T(256)} %broadcast.235), dimensions={1}, to_apply=%broadcast_in_dim.24.reduce_sub_computation | reduce | bytes 524290 | tf_op jit(solution)/shard_map/broadcast_in_dim | solution.py:32
  183.2 1.8 reshape.231
  185.0 6.8 %all-to-all-start.8 = ((bf16[64,2,1024]{2,1,0:T(2,128)(2,1)}), bf16[64,2,1024]{2,1,0:T(2,128)(2,1)}, u32[]{:S(2)}, u32[]{:S(2)}) async-start(bf16[64,2,1024]{2,1,0:T(2,128)(2,1)} %reshape.231), calls=%async_computation.8 | async-start | bytes 524288 | tf_op jit(solution)/shard_map/all_to_all | solution.py:32
  192.7 18.0 %all-to-all-done.8 = bf16[64,2,1024]{2,1,0:T(2,128)(2,1)} async-done(((bf16[64,2,1024]{2,1,0:T(2,128)(2,1)}), bf16[64,2,1024]{2,1,0:T(2,128)(2,1)}, u32[]{:S(2)}, u32[]{:S(2)}) %all-to-all-start.8) | async-done | bytes 262176 | tf_op jit(solution)/shard_map/all_to_all | solution.py:32
  210.7 2.8 %reshape.232 = bf16[64,1,2048]{2,1,0:T(2,128)(2,1)} reshape(bf16[64,2,1024]{2,1,0:T(2,128)(2,1)} %all-to-all-done.8) | data formatting | bytes 524288
  213.5 1.2 copy.53
  214.7 8.4 %all_to_all.61 = bf16[2,64,2048]{2,1,0:T(8,128)(2,1)S(1)} all-to-all(bf16[2,64,2048]{2,1,0:T(8,128)(2,1)S(1)} %broadcast_in_dim.26), channel_id=1, replica_groups=mesh['dp'=4,'kv_0'=16,'kv_1'=4,'tp'=2] {'tp'}, dimensions={0} | all-to-all | bytes 1048576 | tf_op jit(solution)/shard_map/all_to_all | solution.py:32
  223.2 1.2 convert_bitcast_fusion.2
  225.4 3.2 %copy.33 = f32[64,2,2048]{0,2,1:T(8,128)} copy(f32[64,2,2048]{2,0,1:T(8,128)} %get-tuple-element.6) | data formatting | bytes 2097152 | tf_op jit(solution)/shard_map/convert_element_type | solution.py:77
  228.6 2.0 fusion.4
  (63 shorter events, 18.2 us)
Async XLA Ops:
  0.6 132.5 %copy-start = (bf16[86,4096]{1,0:T(8,128)(2,1)S(1)}, bf16[86,4096]{1,0:T(8,128)(2,1)}, u32[]{:S(2)}) copy-start(bf16[86,4096]{1,0:T(8,128)(2,1)} %param.24) | copy-start | bytes 2113540
  6.1 48.3 %copy-start.2 = (f32[1,8,128,128]{3,2,1,0:T(8,128)S(1)}, f32[1,8,128,128]{3,2,1,0:T(8,128)}, u32[]{:S(2)}) copy-start(f32[1,8,128,128]{3,2,1,0:T(8,128)} %param.15) | copy-start | bytes 1572868
  21.9 49.1 %copy-start.3 = (bf16[64,64]{1,0:T(8,128)(2,1)S(1)}, bf16[64,64]{1,0:T(8,128)(2,1)}, u32[]{:S(2)}) copy-start(bf16[64,64]{1,0:T(8,128)(2,1)} %param.13) | copy-start | bytes 24580
  22.8 31.1 %all-to-all-start.1 = ((f32[16,1,4096]{2,1,0:T(1,128)}), f32[16,1,4096]{2,1,0:T(1,128)S(1)}, u32[]{:S(2)}, u32[]{:S(2)}) async-start(f32[16,1,4096]{2,1,0:T(1,128)} %reduce_sum.101), calls=%async_computation.1 | async-start | bytes 524288 | tf_op jit(solution)/shard_map/all_to_all | solution.py:27
  54.4 38.8 %copy-start.4 = (bf16[2048,32]{0,1:T(8,128)(2,1)S(1)}, bf16[2048,32]{0,1:T(8,128)(2,1)}, u32[]{:S(2)}) copy-start(bf16[2048,32]{0,1:T(8,128)(2,1)} %param.20) | copy-start | bytes 393220
  54.6 0.8 copy-start.1
  59.2 26.8 %all-to-all-start.2 = ((bf16[64,2,512]{2,1,0:T(2,128)(2,1)}), bf16[64,2,512]{2,1,0:T(2,128)(2,1)S(1)}, u32[]{:S(2)}, u32[]{:S(2)}) async-start(bf16[64,2,512]{2,1,0:T(2,128)(2,1)} %reshape.223), calls=%async_computation.2 | async-start | bytes 262144 | tf_op jit(solution)/shard_map/all_to_all | solution.py:32
  128.6 1.6 copy-start.5
  185.0 25.7 %all-to-all-start.8 = ((bf16[64,2,1024]{2,1,0:T(2,128)(2,1)}), bf16[64,2,1024]{2,1,0:T(2,128)(2,1)}, u32[]{:S(2)}, u32[]{:S(2)}) async-start(bf16[64,2,1024]{2,1,0:T(2,128)(2,1)} %reshape.231), calls=%async_computation.8 | async-start | bytes 524288 | tf_op jit(solution)/shard_map/all_to_all | solution.py:32
where the time goes:
time: 234 us; the launch traced here: 232 us
  blocking collectives  93.3 us (40%)
  waiting for transfers between devices  44.8 us (19%)
  starting transfers between devices  37 us (16%)
  local copies, waits for them, and re-layouts  26.9 us (11%)
  other arithmetic  19.1 us (8%)
  matrix products  9.34 us (4%)
    all_to_all x4, blocking collectives, copy_for_each(): lax.all_to_all(jnp.broadcast_to(x[None], (count, *x.shape)), axis, 0, 0,...  46.6 us
    all_to_all x2, waiting for transfers between devices, copy_for_each(): lax.all_to_all(jnp.broadcast_to(x[None], (count, *x.shape)), axis, 0, 0,...  32.8 us
    all_to_all x1, blocking collectives, sum_in_two_steps_2(): lax.all_to_all(nearer.astype(jnp.bfloat16), far, split_axis=0, concat_axi...  26.1 us
    all_to_all x2, starting transfers between devices, copy_for_each(): lax.all_to_all(jnp.broadcast_to(x[None], (count, *x.shape)), axis, 0, 0,...  18.6 us
    all_to_all x1, starting transfers between devices, sum_in_two_steps(): return jnp.sum(lax.all_to_all(own, far, 0, 0, tiled=True), axis=0)  18.4 us
    all_to_all x1, blocking collectives, summed_on_arrival(): lax.all_to_all(tiles, axis, split_axis=0, concat_axis=0, tiled=True)  15.7 us
    unnamed x28, local copies, waits for them, and re-layouts  15.2 us
    all_to_all x1, waiting for transfers between devices, sum_in_two_steps(): return jnp.sum(lax.all_to_all(own, far, 0, 0, tiled=True), axis=0)  12 us
  transfers between devices with their start and end apart: 3, of which 3 were waited for; matrix products, arithmetic and copies ran while one was open for 0% of the time, Pallas kernels for 0%

commit v1 on v0

v1 whole, which is shorter than its diff:
```python
import jax
import jax.numpy as jnp
from jax import lax
from jax.experimental import pallas as pl
from jax.experimental.pallas import tpu as pltpu
from jax.sharding import Mesh
from jax.sharding import PartitionSpec as P

KV = ("kv_0", "kv_1")
YZ = ("kv_1", "kv_0")
Y_TP = ("kv_1", "tp")
KV_TP = ("kv_0", "kv_1", "tp")
DP_KV = ("dp", "kv_0", "kv_1")
F32 = jnp.float32
BF16 = jnp.bfloat16
LANES = 128
NZ = 16
NY = 4
SEQS = NZ * NY
INTERPRET = False

VMEM = pl.BlockSpec(memory_space=pltpu.VMEM)
SMEM = pl.BlockSpec(memory_space=pltpu.SMEM)


def kernel_call(body, out_shape, n_in, scalars=0, scratch=(), name=None):
    single = not isinstance(out_shape, (list, tuple))
    return pl.pallas_call(
        body,
        out_shape=out_shape,
        in_specs=[SMEM] * scalars + [VMEM] * (n_in - scalars),
        out_specs=VMEM if single else [VMEM] * len(out_shape),
        scratch_shapes=list(scratch),
        compiler_params=pltpu.CompilerParams(vmem_limit_bytes=40 * 1024 * 1024),
        interpret=INTERPRET,
        name=name,
    )


def sds(shape, dtype):
    return jax.ShapeDtypeStruct(shape, dtype)


def rows_of(s):
    return (s % NY) * NZ + s // NY


def perm_matrix(dtype):
    d = lax.broadcasted_iota(jnp.int32, (SEQS, SEQS), 0)
    s = lax.broadcasted_iota(jnp.int32, (SEQS, SEQS), 1)
    return (d == rows_of(s)).astype(F32).astype(dtype)


def mm(a, b, ca, cb):
    return lax.dot_general(a, b, (((ca,), (cb,)), ((), ())), preferred_element_type=F32)


def project_kernel(tok_hbm, wq, wk, wv, wg, out, tok, weights, sems):
    sources = (wq, wk, wv, wg)
    copies = [pltpu.make_async_copy(tok_hbm, tok, sems.at[4])]
    for i, w in enumerate(sources):
        copies.append(pltpu.make_async_copy(w, weights.at[i], sems.at[i]))
    for copy in copies:
        copy.start()
    copies[0].wait()
    rows = mm(perm_matrix(BF16), tok[...], 1, 0).astype(BF16)
    width = weights.shape[2]
    for i in range(len(sources)):
        copies[1 + i].wait()
        part = mm(rows, weights[i], 1, 0).astype(BF16)
        for y in range(NY):
            out[y, :, i * width : (i + 1) * width] = part[y * NZ : (y + 1) * NZ]


def near_sum_kernel(x, out, wide):
    for c in range(wide.shape[1]):
        cols = slice(c * LANES, (c + 1) * LANES)
        total = x[0, :, cols].astype(F32)
        for y in range(1, NY):
            total += x[y, :, cols].astype(F32)
        wide[:, c, :] = total
    out[...] = wide[...].astype(BF16)


def retention_kernel(x, aux, state, new_state, out):
    heads, dim = state.shape[1], state.shape[2]
    total = x[0].astype(F32)
    for z in range(1, NZ):
        total += x[z].astype(F32)
    cosine = aux[0:1, :]
    sine = aux[1:2, :]
    query = total[0:heads]
    key = total[heads : 2 * heads]
    value = total[2 * heads : 3 * heads]
    gate = total[3 * heads : 4 * heads]
    query = query * cosine + pltpu.roll(query, dim // 2, 1) * sine
    key = (key * cosine + pltpu.roll(key, dim // 2, 1) * sine) * dim ** (-0.5)
    query_t = query.T
    key_t = key.T
    lines = []
    for h in range(heads):
        updated = aux[8 + h : 9 + h, :] * state[0, h] + key_t[:, h : h + 1] * value[h : h + 1, :]
        new_state[0, h] = updated
        lines.append(jnp.sum(query_t[:, h : h + 1] * updated, axis=0, keepdims=True))
    retained = jnp.concatenate(lines, axis=0)
    mean = jnp.mean(retained, -1, keepdims=True)
    var = jnp.mean(jnp.square(retained - mean), -1, keepdims=True)
    normed = (retained - mean) * lax.rsqrt(var + 1e-05)
    silu = gate / (1.0 + jnp.exp(-gate))
    attended = (normed * silu).astype(BF16)
    out[...] = jnp.broadcast_to(attended[None], out.shape)


def mix_kernel(where, x, w_t, tok, out, wide):
    tp = where[0]
    tps, seqs, heads, dim = x.shape
    cols = w_t.shape[0]
    groups = LANES // cols
    wide[...] = x[...].astype(F32)
    own = lax.broadcasted_iota(jnp.int32, (tok.shape[1], LANES), 0)
    lane = lax.broadcasted_iota(jnp.int32, (tok.shape[1], LANES), 1)
    pick = (own == tp * cols + lane % cols).astype(F32).astype(BF16)
    rows = mm(perm_matrix(BF16), tok[...], 1, 0).astype(BF16)
    acc = mm(rows, pick, 1, 0)
    w4 = jnp.concatenate([w_t[...]] * groups, axis=0)
    for t in range(tps):
        for h in range(heads):
            k = (t * heads + h) * dim
            acc += mm(wide[t, :, h, :].astype(BF16), w4[:, k : k + dim], 1, 1)
    block = lax.broadcasted_iota(jnp.int32, (seqs // groups, LANES), 1) // cols
    per = seqs // groups
    packed = acc[0:per]
    for g in range(1, groups):
        packed = jnp.where(block == g, acc[g * per : (g + 1) * per], packed)
    out[...] = jnp.broadcast_to(packed.astype(BF16)[None], out.shape)


def feed_kernel(where, x, gain, wg_t, wu_t, wd, out, row, wide, narrow, sums_out):
    per = x.shape[2]
    tps = x.shape[0] // NY
    groups = SEQS // per
    cols = LANES // groups
    chips = LANES // (tps * cols)
    width = wide.shape[1]
    lane = lax.broadcasted_iota(jnp.int32, (per, LANES), 1) // cols
    sums = [jnp.zeros((per, LANES), F32) for _ in range(groups)]
    squares = [jnp.zeros((per, LANES), F32) for _ in range(groups)]
    for a in range(SEQS // chips):
        tiles = [None] * groups
        for q in range(groups):
            kv = a * chips + q // tps
            source = x[(kv % NY) * tps + q % tps, kv // NY].astype(F32)
            for g in range(groups):
                shift = ((q - g) * cols) % LANES
                moved = source if shift == 0 else pltpu.roll(source, shift, 1)
                tiles[g] = moved if q == 0 else jnp.where(lane == q, moved, tiles[g])
        for g in range(groups):
            wide[g * per : (g + 1) * per, a * LANES : (a + 1) * LANES] = tiles[g]
            sums[g] += tiles[g]
            squares[g] += tiles[g] * tiles[g]
    mean = jnp.sum(jnp.concatenate(sums, 0), -1, keepdims=True) / width
    var = jnp.sum(jnp.concatenate(squares, 0), -1, keepdims=True) / width - mean * mean
    scale = lax.rsqrt(var + 1e-05)
    for a in range(width // LANES):
        c = slice(a * LANES, (a + 1) * LANES)
        hidden = ((wide[:, c] - mean) * scale * gain[:, c]).astype(BF16)
        narrow[:, c] = hidden
        wide[:, c] = hidden.astype(F32)
    row[...] = wide[pl.ds(where[1], 1), :]
    gate = mm(narrow[...], wg_t[...], 1, 1)
    up = mm(narrow[...], wu_t[...], 1, 1)
    inner = (gate / (1.0 + jnp.exp(-gate)) * up).astype(BF16)
    lines = sums_out.shape[1]
    for c in range(lines):
        sums_out[:, c, :] = mm(inner, wd[:, c * LANES : (c + 1) * LANES], 1, 0)
    half = lines // tps
    for y in range(NY):
        for t in range(tps):
            block = sums_out[y * NZ : (y + 1) * NZ, t * half : (t + 1) * half, :]
            out[y * tps + t] = block.astype(BF16)


def plain_sum_kernel(x, out):
    total = x[0].astype(F32)
    for d in range(1, x.shape[0]):
        total += x[d].astype(F32)
    out[...] = total.astype(BF16)


def ffn_sum_kernel(where, x, hidden, out):
    per = x.shape[1]
    total = hidden[pl.ds(pl.multiple_of(where[0] * per, per), per), :]
    for d in range(x.shape[0]):
        total += x[d].astype(F32)
    out[...] = total


def total_of(x):
    return jnp.sum(jnp.sum(x, 0, keepdims=True), 1, keepdims=True)


def final_norm_kernel(x, gain, out):
    p = x[...]
    count = p.shape[0] * p.shape[1]
    mean = total_of(p) / count
    var = total_of(p * p) / count - mean * mean
    normed = ((p - mean) * lax.rsqrt(var + 1e-05) * gain[...]).astype(BF16)
    lines = p.shape[0]
    d = lax.broadcasted_iota(jnp.int32, (SEQS, lines), 0)
    line = lax.broadcasted_iota(jnp.int32, (SEQS, lines), 1)
    kv = (d % NZ) * NY + d // NZ
    spread = (kv * lines // SEQS == line).astype(F32).astype(BF16)
    out[...] = mm(spread, normed, 1, 0)


def place_kernel(where, x, out, wide):
    wide[...] = mm(x[...].astype(BF16), perm_matrix(BF16), 0, 0)
    cols = out.shape[0]
    out[...] = wide[pl.ds(pl.multiple_of(where[2], cols), cols), :].astype(BF16)


def on_device(
    tokens,
    positions,
    state,
    w_query,
    w_key,
    w_value,
    w_gate,
    w_out,
    gain_mix,
    w_ffn_gate,
    w_ffn_up,
    w_ffn_down,
    gain_out,
):
    heads, dim = state.shape[1], state.shape[2]
    width = w_ffn_gate.shape[0]
    cols = w_out.shape[1]
    proj = 4 * heads
    half = width // 2
    tp = lax.axis_index("tp")
    place = lax.axis_index("kv_1") * NZ + lax.axis_index("kv_0")
    offset = (lax.axis_index("kv_1") % 2) * (2 * cols) + tp * cols
    where = jnp.stack([tp, place, offset]).astype(jnp.int32)

    inverse = 10000.0 ** (-jnp.arange(dim // 2, dtype=F32) / (dim // 2))
    angle = positions.astype(F32)[:, None] * inverse[None, :]
    cosine = jnp.cos(angle)
    sine = jnp.sin(angle)
    head_ids = (tp * heads + jnp.arange(heads, dtype=jnp.int32)).astype(F32)
    decay = 1.0 - 2.0 ** (-5.0 - 6.0 * head_ids / (2 * heads - 1))
    aux = jnp.concatenate(
        [
            jnp.concatenate([cosine, cosine], 1),
            jnp.concatenate([-sine, sine], 1),
            jnp.zeros((6, dim), F32),
            jnp.broadcast_to(decay[:, None], (heads, dim)),
        ],
        0,
    )

    tokens_in, aux, where = lax.optimization_barrier((tokens, aux, where))
    parts = pl.pallas_call(
        project_kernel,
        out_shape=sds((NY, NZ, proj * dim), BF16),
        in_specs=[pl.BlockSpec(memory_space=pl.ANY)] * 5,
        out_specs=VMEM,
        scratch_shapes=[
            pltpu.VMEM(tokens.shape, BF16),
            pltpu.VMEM((4, *w_query.shape), BF16),
            pltpu.SemaphoreType.DMA((5,)),
        ],
        interpret=INTERPRET,
        name="project",
    )(tokens_in, w_query, w_key, w_value, w_gate)
    near = lax.all_to_all(parts, "kv_1", 0, 0, tiled=True)
    near = kernel_call(
        near_sum_kernel,
        sds((NZ, proj, dim), BF16),
        1,
        scratch=[pltpu.VMEM((NZ, proj, dim), F32)],
        name="near_sum",
    )(near)
    far = lax.all_to_all(near, "kv_0", 0, 0, tiled=True)
    new_state, attended = kernel_call(
        retention_kernel,
        [sds(state.shape, F32), sds((SEQS, heads, dim), BF16)],
        3,
        name="retention",
    )(far, aux, state)
    gathered = lax.all_to_all(attended, YZ, 0, 0, tiled=True)
    gathered = lax.all_gather(gathered, "tp", axis=0)
    per = SEQS * cols // LANES
    mixed = kernel_call(
        mix_kernel,
        sds((NZ, per, LANES), BF16),
        4,
        scalars=1,
        scratch=[pltpu.VMEM((2, SEQS, heads, dim), F32)],
        name="mix",
    )(where, gathered.reshape(2, SEQS, heads, dim), w_out.T, tokens)
    rows = lax.all_to_all(mixed, "kv_0", 0, 0, tiled=True)
    rows = jnp.broadcast_to(rows[None], (2 * NY, *rows.shape))
    rows = lax.all_to_all(rows, Y_TP, 0, 0, tiled=True)
    lines = half // LANES
    part, hidden_row = kernel_call(
        feed_kernel,
        [sds((2 * NY, NZ, lines, LANES), BF16), sds((1, width), F32)],
        6,
        scalars=1,
        scratch=[
            pltpu.VMEM((SEQS, width), F32),
            pltpu.VMEM((SEQS, width), BF16),
            pltpu.VMEM((SEQS, 2 * lines, LANES), F32),
        ],
        name="feed",
    )(where, rows, gain_mix[None, :], w_ffn_gate.T, w_ffn_up.T, w_ffn_down)
    part = lax.all_to_all(part, Y_TP, 0, 0, tiled=True)
    part = kernel_call(plain_sum_kernel, sds((NZ, lines, LANES), BF16), 1, name="half_sum")(part)
    part = lax.all_to_all(part, "kv_0", 0, 0, tiled=True)
    summed = kernel_call(
        ffn_sum_kernel, sds((lines, LANES), F32), 3, scalars=1, name="ffn_sum"
    )(where, part, hidden_row.reshape(2 * lines, LANES))
    summed = lax.all_gather(summed, "tp", axis=0, tiled=True)
    spread = kernel_call(final_norm_kernel, sds((SEQS, LANES), F32), 2, name="final_norm")(
        summed, gain_out.reshape(2 * lines, LANES)
    )
    spread = lax.all_to_all(spread.reshape(SEQS, 1, LANES), YZ, 0, 0, tiled=True)
    layer_out = kernel_call(
        place_kernel,
        sds((cols, SEQS), BF16),
        2,
        scalars=1,
        scratch=[pltpu.VMEM((LANES, SEQS), F32)],
        name="place",
    )(where, spread.reshape(SEQS, LANES))
    return (layer_out.T, new_state)


def solution(mesh):
    finer = Mesh(
        mesh.devices.reshape(mesh.shape["dp"], NZ, NY, mesh.shape["tp"]),
        ("dp", "kv_0", "kv_1", "tp"),
    )
    return jax.shard_map(
        on_device,
        mesh=finer,
        in_specs=(
            P("dp", KV),
            P(DP_KV),
            P(DP_KV, "tp", None, None),
            P(KV, "tp"),
            P(KV, "tp"),
            P(KV, "tp"),
            P(KV, "tp"),
            P(None, KV_TP),
            P(),
            P(None, KV_TP),
            P(None, KV_TP),
            P(KV_TP, None),
            P(),
        ),
        out_specs=(P("dp", KV_TP), P(DP_KV, "tp", None, None)),
        check_vma=False,
    )
```

time: 234 us -> 156 us (0.67)
  blocking collectives: 93.3 us -> 143 us
  waiting for transfers between devices: 44.8 us -> 0 us
  starting transfers between devices: 37 us -> 0 us
  local copies, waits for them, and re-layouts: 26.9 us -> 0.26 us
  other arithmetic: 19.1 us -> 0.26 us
  Pallas kernels: 0 us -> 10.3 us
  matrix products: 9.34 us -> 0 us
    all_to_all x3 -> x0, waiting for transfers between devices: 44.8 us -> none  [the longest x2 32.8 us: copy_for_each(): lax.all_to_all(jnp.broadcast_to(x[None], (count, *x.shape)), axis, 0, 0,...]
    all_to_all x7 -> x8, blocking collectives: 93.3 us -> 134 us  [the longest x1 28.4 us: on_device(): far = lax.all_to_all(near, 'kv_0', 0, 0, tiled=True)]
    all_to_all x3 -> x0, starting transfers between devices: 37 us -> none  [the longest x2 18.6 us: copy_for_each(): lax.all_to_all(jnp.broadcast_to(x[None], (count, *x.shape)), axis, 0, 0,...]
    unnamed x28 -> x16, local copies, waits for them, and re-layouts: 15.2 us -> 0.03 us
    pallas_call x0 -> x9, Pallas kernels: none -> 10.3 us  [the longest x1 2.78 us: on_device(): kernel_call(feed_kernel, [sds((2 * NY, NZ, lines, LANES), BF16), sds((1,...]
    all_gather x0 -> x2, blocking collectives: none -> 9.4 us  [the longest x1 5.37 us: on_device(): gathered = lax.all_gather(gathered, 'tp', axis=0)]
    dot_general x8 -> x0, matrix products: 9.34 us -> none  [the longest x1 2.74 us: on_device(): jnp.dot(inner, w_ffn_down, preferred_element_type=jnp.float32)]
    reduce_sum x9 -> x0, other arithmetic: 7.03 us -> none  [the longest x1 1.97 us: on_device(): out_sums = jnp.sum(summed, 1)]
  transfers between devices with their start and end apart: 3 -> 0, of which waited for: 3 -> 0; matrix products, arithmetic and copies ran while one was open for 0% -> 0% of each run, Pallas kernels for 0% -> 0%
where the time goes in v1:
time: 156 us; the launch traced here: 155 us
  blocking collectives  143 us (92%)
  Pallas kernels  10.3 us (7%)
    all_to_all x1, blocking collectives, on_device(): far = lax.all_to_all(near, 'kv_0', 0, 0, tiled=True)  28.4 us
    all_to_all x1, blocking collectives, on_device(): gathered = lax.all_to_all(attended, YZ, 0, 0, tiled=True)  20.4 us
    all_to_all x1, blocking collectives, on_device(): lax.all_to_all(spread.reshape(SEQS, 1, LANES), YZ, 0, 0, tiled=True)  17.3 us
    all_to_all x1, blocking collectives, on_device(): rows = lax.all_to_all(mixed, 'kv_0', 0, 0, tiled=True)  14.7 us
    all_to_all x1, blocking collectives, on_device(): part = lax.all_to_all(part, 'kv_0', 0, 0, tiled=True)  14.2 us
    all_to_all x1, blocking collectives, on_device(): rows = lax.all_to_all(rows, Y_TP, 0, 0, tiled=True)  13.9 us
    all_to_all x1, blocking collectives, on_device(): part = lax.all_to_all(part, Y_TP, 0, 0, tiled=True)  12.8 us
    all_to_all x1, blocking collectives, on_device(): near = lax.all_to_all(parts, 'kv_1', 0, 0, tiled=True)  11.9 us

profile of v1, /device:TPU:1, one launch (start us, length us, event | category | flops | bytes accessed | tf_op | source)
XLA Modules:
  0.0 155.3 jit_solution(15247595764204683105)
XLA Ops:
  1.3 0.1 fusion.2
  1.3 0.1 fusion
  1.4 0.1 pad.8.clone
  1.5 0.1 pad.7.clone
  1.6 0.1 pad_add_fusion.where
  1.7 0.1 maximum_maximum_fusion.aux
  1.7 2.4 %project.1 = bf16[4,16,4096]{2,1,0:T(8,128)(2,1)} custom-call(bf16[64,64]{1,0:T(8,128)(2,1)} %tok.1, bf16[64,1024]{1,0:T(8,128)(2,1)} %wq.1, bf16[64,1024]{1,0:T(8,128)(2,1)} %wk.1, bf16[64,1024]{1,0:T(8,128)(2,1)} %wv.1, bf16[64,1024]{1,0:T(8,128)(2,1)} %wg.1), custom_call_target="tpu_custom_call" | custom-call | tf_op jit(solution)/shard_map/project/pallas_call | solution.py:264
  4.2 11.9 %all_to_all.40.x = bf16[4,16,4096]{2,1,0:T(8,128)(2,1)S(1)} all-to-all(bf16[4,16,4096]{2,1,0:T(8,128)(2,1)} %project.1), channel_id=1, replica_groups=mesh['dp'=4,'kv_0'=16,'kv_1'=4,'tp'=2] {'kv_1'}, dimensions={0} | all-to-all | bytes 1048576 | tf_op jit(solution)/shard_map/all_to_all | solution.py:277
  16.1 0.2 near_sum.1
  16.4 28.4 %all_to_all.41.x = bf16[16,32,128]{2,1,0:T(8,128)(2,1)S(1)} all-to-all(bf16[16,32,128]{2,1,0:T(8,128)(2,1)S(1)} %near_sum.1), channel_id=1, replica_groups=mesh['dp'=4,'kv_0'=16,'kv_1'=4,'tp'=2] {'kv_0'}, dimensions={0} | all-to-all | bytes 262144 | tf_op jit(solution)/shard_map/all_to_all | solution.py:285
  44.8 0.0 copy-done.3
  44.8 1.4 retention.1
  46.1 20.4 %all_to_all.42 = bf16[64,8,128]{2,1,0:T(8,128)(2,1)S(1)} all-to-all(bf16[64,8,128]{2,1,0:T(8,128)(2,1)S(1)} %get-tuple-element.12), channel_id=1, replica_groups=mesh['dp'=4,'kv_0'=16,'kv_1'=4,'tp'=2] {'kv_1','kv_0'}, dimensions={0} | all-to-all | bytes 262144 | tf_op jit(solution)/shard_map/all_to_all | solution.py:292
  66.6 5.4 %all-gather = bf16[128,8,128]{2,1,0:T(8,128)(2,1)S(1)} all-gather(bf16[64,8,128]{2,1,0:T(8,128)(2,1)S(1)} %all_to_all.42), channel_id=2, replica_groups=mesh['dp'=4,'kv_0'=16,'kv_1'=4,'tp'=2] {'tp'}, dimensions={0}, use_global_device_ids=true | all-gather | bytes 393216 | tf_op jit(solution)/shard_map/all_gather | solution.py:293
  72.0 0.0 copy-done.4
  72.0 0.0 copy-done.5
  72.0 1.2 mix.1
  73.2 14.7 %all_to_all.43 = bf16[16,16,128]{2,1,0:T(8,128)(2,1)S(1)} all-to-all(bf16[16,16,128]{2,1,0:T(8,128)(2,1)S(1)} %mix.1), channel_id=1, replica_groups=mesh['dp'=4,'kv_0'=16,'kv_1'=4,'tp'=2] {'kv_0'}, dimensions={0} | all-to-all | bytes 131072 | tf_op jit(solution)/shard_map/all_to_all | solution.py:303
  87.9 0.1 broadcast_in_dim.10
  88.0 0.0 copy-start.6
  88.0 13.9 %all_to_all.44.x = bf16[8,16,16,128]{3,2,1,0:T(8,128)(2,1)S(1)} all-to-all(bf16[8,16,16,128]{3,2,1,0:T(8,128)(2,1)S(1)} %broadcast_in_dim.10), channel_id=1, replica_groups=mesh['dp'=4,'kv_0'=16,'kv_1'=4,'tp'=2] {'kv_1','tp'}, dimensions={0} | all-to-all | bytes 1048576 | tf_op jit(solution)/shard_map/all_to_all | solution.py:305
  102.0 0.0 copy-done.6
  102.0 2.8 %feed.1 = (bf16[8,16,16,128]{3,2,1,0:T(8,128)(2,1)S(1)}, f32[1,4096]{1,0:T(1,128)S(1)}) custom-call(s32[3]{0:T(128)S(1)} %pad_add_fusion.where, bf16[8,16,16,128]{3,2,1,0:T(8,128)(2,1)S(1)} %all_to_all.44.x, f32[1,4096]{1,0:T(1,128)S(1)} %bitcast.22, bf16[86,4096]{1,0:T(8,128)(2,1)S(1)} %bitcast.17, bf16[86,4096]{1,0:T(8,128)(2,1)S(1)} %bitcast.18, ...), custom_call_target="tpu_custom_call" | custom-call | tf_op jit(solution)/shard_map/feed/pallas_call | solution.py:307
  104.8 12.8 %all_to_all.45.x = bf16[8,16,16,128]{3,2,1,0:T(8,128)(2,1)S(1)} all-to-all(bf16[8,16,16,128]{3,2,1,0:T(8,128)(2,1)S(1)} %get-tuple-element.13), channel_id=1, replica_groups=mesh['dp'=4,'kv_0'=16,'kv_1'=4,'tp'=2] {'kv_1','tp'}, dimensions={0} | all-to-all | bytes 1048576 | tf_op jit(solution)/shard_map/all_to_all | solution.py:319
  117.6 0.1 half_sum.1
  117.6 14.2 %all_to_all.46.x = bf16[16,16,128]{2,1,0:T(8,128)(2,1)S(1)} all-to-all(bf16[16,16,128]{2,1,0:T(8,128)(2,1)S(1)} %half_sum.1), channel_id=1, replica_groups=mesh['dp'=4,'kv_0'=16,'kv_1'=4,'tp'=2] {'kv_0'}, dimensions={0} | all-to-all | bytes 131072 | tf_op jit(solution)/shard_map/all_to_all | solution.py:321
  131.8 0.6 ffn_sum.1
  132.4 0.0 copy-start.7
  132.4 4.0 %all_gather.11.x = f32[32,128]{1,0:T(8,128)S(1)} all-gather(f32[16,128]{1,0:T(8,128)S(1)} %ffn_sum.1), channel_id=1, replica_groups=mesh['dp'=4,'kv_0'=16,'kv_1'=4,'tp'=2] {'tp'}, dimensions={0}, use_global_device_ids=true | all-gather | bytes 24576 | tf_op jit(solution)/shard_map/all_gather | solution.py:325
  136.4 0.2 final_norm.1
  136.6 17.3 %all_to_all.47 = f32[64,1,128]{2,1,0:T(1,128)S(1)} all-to-all(f32[64,1,128]{2,1,0:T(1,128)S(1)} %bitcast.21), channel_id=1, replica_groups=mesh['dp'=4,'kv_0'=16,'kv_1'=4,'tp'=2] {'kv_1','kv_0'}, dimensions={0} | all-to-all | bytes 65536 | tf_op jit(solution)/shard_map/all_to_all | solution.py:329
  153.9 1.3 place.1
  (12 shorter events, 0.0 us)
Async XLA Ops:
  16.1 28.6 %copy-start.3 = (f32[1,8,128,128]{3,2,1,0:T(8,128)S(1)}, f32[1,8,128,128]{3,2,1,0:T(8,128)}, u32[]{:S(2)}) copy-start(f32[1,8,128,128]{3,2,1,0:T(8,128)} %state.1) | copy-start | bytes 1572868
  66.6 5.4 %copy-start.4 = (bf16[2048,32]{0,1:T(8,128)(2,1)S(1)}, bf16[2048,32]{0,1:T(8,128)(2,1)}, u32[]{:S(2)}) copy-start(bf16[2048,32]{0,1:T(8,128)(2,1)} %param.20) | copy-start | bytes 393220
  66.6 5.4 %copy-start.5 = (bf16[64,64]{1,0:T(8,128)(2,1)S(1)}, bf16[64,64]{1,0:T(8,128)(2,1)}, u32[]{:S(2)}) copy-start(bf16[64,64]{1,0:T(8,128)(2,1)} %tok.1) | copy-start | bytes 24580
  72.0 30.0 %copy-start.2 = (bf16[86,4096]{1,0:T(8,128)(2,1)S(1)}, bf16[86,4096]{1,0:T(8,128)(2,1)}, u32[]{:S(2)}) copy-start(bf16[86,4096]{1,0:T(8,128)(2,1)} %wd.1) | copy-start | bytes 2113540
  87.9 14.0 %copy-start = (bf16[4096,86]{0,1:T(8,128)(2,1)S(1)}, bf16[4096,86]{0,1:T(8,128)(2,1)}, u32[]{:S(2)}) copy-start(bf16[4096,86]{0,1:T(8,128)(2,1)} %param.22) | copy-start | bytes 2113540
  87.9 14.0 %copy-start.1 = (bf16[4096,86]{0,1:T(8,128)(2,1)S(1)}, bf16[4096,86]{0,1:T(8,128)(2,1)}, u32[]{:S(2)}) copy-start(bf16[4096,86]{0,1:T(8,128)(2,1)} %param.23) | copy-start | bytes 2113540
  88.0 14.0 %copy-start.6 = (f32[4096]{0:T(1024)S(1)}, f32[4096]{0:T(1024)}, u32[]{:S(2)}) copy-start(f32[4096]{0:T(1024)} %param.21) | copy-start | bytes 49156
  132.4 4.0 %copy-start.7 = (f32[4096]{0:T(1024)S(1)}, f32[4096]{0:T(1024)}, u32[]{:S(2)}) copy-start(f32[4096]{0:T(1024)} %param.25) | copy-start | bytes 49156

commit v2 on v1

--- a/solution.py
+++ b/solution.py
@@ -8,7 +8,6 @@
 
 KV = ("kv_0", "kv_1")
 YZ = ("kv_1", "kv_0")
-Y_TP = ("kv_1", "tp")
 KV_TP = ("kv_0", "kv_1", "tp")
 DP_KV = ("dp", "kv_0", "kv_1")
 F32 = jnp.float32
@@ -20,18 +19,18 @@
 INTERPRET = False
 
 VMEM = pl.BlockSpec(memory_space=pltpu.VMEM)
-SMEM = pl.BlockSpec(memory_space=pltpu.SMEM)
-
-
-def kernel_call(body, out_shape, n_in, scalars=0, scratch=(), name=None):
+PARAMS = pltpu.CompilerParams(vmem_limit_bytes=32 * 1024 * 1024)
+
+
+def kernel_call(body, out_shape, n_in, scratch=(), name=None):
     single = not isinstance(out_shape, (list, tuple))
     return pl.pallas_call(
         body,
         out_shape=out_shape,
-        in_specs=[SMEM] * scalars + [VMEM] * (n_in - scalars),
+        in_specs=[VMEM] * n_in,
         out_specs=VMEM if single else [VMEM] * len(out_shape),
         scratch_shapes=list(scratch),
-        compiler_params=pltpu.CompilerParams(vmem_limit_bytes=40 * 1024 * 1024),
+        compiler_params=PARAMS,
         interpret=INTERPRET,
         name=name,
     )
@@ -111,8 +110,8 @@
     out[...] = jnp.broadcast_to(attended[None], out.shape)
 
 
-def mix_kernel(where, x, w_t, tok, out, wide):
-    tp = where[0]
+def mix_kernel(x, w_t, tok, out, wide):
+    tp = lax.axis_index("tp")
     tps, seqs, heads, dim = x.shape
     cols = w_t.shape[0]
     groups = LANES // cols
@@ -135,9 +134,11 @@
     out[...] = jnp.broadcast_to(packed.astype(BF16)[None], out.shape)
 
 
-def feed_kernel(where, x, gain, wg_t, wu_t, wd, out, row, wide, narrow, sums_out):
-    per = x.shape[2]
-    tps = x.shape[0] // NY
+def feed_kernel(x, gain, wg_t, wu_t, wd, own, other, row, wide, narrow, sums_out):
+    tps = x.shape[0]
+    per = x.shape[3]
+    tp = lax.axis_index("tp")
+    place = lax.axis_index("kv_1") * NZ + lax.axis_index("kv_0")
     groups = SEQS // per
     cols = LANES // groups
     chips = LANES // (tps * cols)
@@ -149,7 +150,7 @@
         tiles = [None] * groups
         for q in range(groups):
             kv = a * chips + q // tps
-            source = x[(kv % NY) * tps + q % tps, kv // NY].astype(F32)
+            source = x[q % tps, kv % NY, kv // NY].astype(F32)
             for g in range(groups):
                 shift = ((q - g) * cols) % LANES
                 moved = source if shift == 0 else pltpu.roll(source, shift, 1)
@@ -166,18 +167,25 @@
         hidden = ((wide[:, c] - mean) * scale * gain[:, c]).astype(BF16)
         narrow[:, c] = hidden
         wide[:, c] = hidden.astype(F32)
-    row[...] = wide[pl.ds(where[1], 1), :]
+    row[...] = wide[pl.ds(place, 1), :]
     gate = mm(narrow[...], wg_t[...], 1, 1)
     up = mm(narrow[...], wu_t[...], 1, 1)
     inner = (gate / (1.0 + jnp.exp(-gate)) * up).astype(BF16)
-    lines = sums_out.shape[1]
-    for c in range(lines):
-        sums_out[:, c, :] = mm(inner, wd[:, c * LANES : (c + 1) * LANES], 1, 0)
-    half = lines // tps
-    for y in range(NY):
-        for t in range(tps):
-            block = sums_out[y * NZ : (y + 1) * NZ, t * half : (t + 1) * half, :]
-            out[y * tps + t] = block.astype(BF16)
+    half = own.shape[1]
+    step = 4
+    for t in range(tps):
+        for c in range(0, half, step):
+            k = (t * half + c) * LANES
+            part = mm(inner, wd[:, k : k + step * LANES], 1, 0)
+            for i in range(step):
+                sums_out[t, :, c + i, :] = part[:, i * LANES : (i + 1) * LANES]
+    own[...] = sums_out[tp].astype(BF16)
+    other[...] = sums_out[1 - tp].astype(BF16)
+
+
+def pair_sum_kernel(own, both, out):
+    tp = lax.axis_index("tp")
+    out[...] = (own[...].astype(F32) + both[1 - tp].astype(F32)).astype(BF16)
 
 
 def plain_sum_kernel(x, out):
@@ -187,9 +195,10 @@
     out[...] = total.astype(BF16)
 
 
-def ffn_sum_kernel(where, x, hidden, out):
+def ffn_sum_kernel(x, hidden, out):
     per = x.shape[1]
-    total = hidden[pl.ds(pl.multiple_of(where[0] * per, per), per), :]
+    tp = lax.axis_index("tp")
+    total = hidden[pl.ds(pl.multiple_of(tp * per, per), per), :]
     for d in range(x.shape[0]):
         total += x[d].astype(F32)
     out[...] = total
@@ -208,15 +217,17 @@
     lines = p.shape[0]
     d = lax.broadcasted_iota(jnp.int32, (SEQS, lines), 0)
     line = lax.broadcasted_iota(jnp.int32, (SEQS, lines), 1)
-    kv = (d % NZ) * NY + d // NZ
-    spread = (kv * lines // SEQS == line).astype(F32).astype(BF16)
+    spread = (d * lines // SEQS == line).astype(F32).astype(BF16)
     out[...] = mm(spread, normed, 1, 0)
 
 
-def place_kernel(where, x, out, wide):
-    wide[...] = mm(x[...].astype(BF16), perm_matrix(BF16), 0, 0)
+def place_kernel(x, out):
     cols = out.shape[0]
-    out[...] = wide[pl.ds(pl.multiple_of(where[2], cols), cols), :].astype(BF16)
+    offset = (lax.axis_index("kv_1") % 2) * (2 * cols) + lax.axis_index("tp") * cols
+    col = lax.broadcasted_iota(jnp.int32, (cols, LANES), 0)
+    lane = lax.broadcasted_iota(jnp.int32, (cols, LANES), 1)
+    pick = (lane == col + offset).astype(F32).astype(BF16)
+    out[...] = mm(pick, x[...].astype(BF16), 1, 1).astype(BF16)
 
 
 def on_device(
@@ -240,9 +251,6 @@
     proj = 4 * heads
     half = width // 2
     tp = lax.axis_index("tp")
-    place = lax.axis_index("kv_1") * NZ + lax.axis_index("kv_0")
-    offset = (lax.axis_index("kv_1") % 2) * (2 * cols) + tp * cols
-    where = jnp.stack([tp, place, offset]).astype(jnp.int32)
 
     inverse = 10000.0 ** (-jnp.arange(dim // 2, dtype=F32) / (dim // 2))
     angle = positions.astype(F32)[:, None] * inverse[None, :]
@@ -260,17 +268,18 @@
         0,
     )
 
-    tokens_in, aux, where = lax.optimization_barrier((tokens, aux, where))
+    tokens_in, aux = lax.optimization_barrier((tokens, aux))
     parts = pl.pallas_call(
         project_kernel,
         out_shape=sds((NY, NZ, proj * dim), BF16),
-        in_specs=[pl.BlockSpec(memory_space=pl.ANY)] * 5,
+        in_specs=[pl.BlockSpec(memory_space=pltpu.HBM)] * 5,
         out_specs=VMEM,
         scratch_shapes=[
             pltpu.VMEM(tokens.shape, BF16),
             pltpu.VMEM((4, *w_query.shape), BF16),
             pltpu.SemaphoreType.DMA((5,)),
         ],
+        compiler_params=PARAMS,
         interpret=INTERPRET,
         name="project",
     )(tokens_in, w_query, w_key, w_value, w_gate)
@@ -295,46 +304,43 @@
     mixed = kernel_call(
         mix_kernel,
         sds((NZ, per, LANES), BF16),
-        4,
-        scalars=1,
+        3,
         scratch=[pltpu.VMEM((2, SEQS, heads, dim), F32)],
         name="mix",
-    )(where, gathered.reshape(2, SEQS, heads, dim), w_out.T, tokens)
+    )(gathered.reshape(2, SEQS, heads, dim), w_out.T, tokens)
     rows = lax.all_to_all(mixed, "kv_0", 0, 0, tiled=True)
-    rows = jnp.broadcast_to(rows[None], (2 * NY, *rows.shape))
-    rows = lax.all_to_all(rows, Y_TP, 0, 0, tiled=True)
+    rows = jnp.broadcast_to(rows[None], (NY, *rows.shape))
+    rows = lax.all_to_all(rows, "kv_1", 0, 0, tiled=True)
+    rows = lax.all_gather(rows, "tp", axis=0)
     lines = half // LANES
-    part, hidden_row = kernel_call(
+    own, other, hidden_row = kernel_call(
         feed_kernel,
-        [sds((2 * NY, NZ, lines, LANES), BF16), sds((1, width), F32)],
-        6,
-        scalars=1,
+        [sds((SEQS, lines, LANES), BF16)] * 2 + [sds((1, width), F32)],
+        5,
         scratch=[
             pltpu.VMEM((SEQS, width), F32),
             pltpu.VMEM((SEQS, width), BF16),
-            pltpu.VMEM((SEQS, 2 * lines, LANES), F32),
+            pltpu.VMEM((2, SEQS, lines, LANES), F32),
         ],
         name="feed",
-    )(where, rows, gain_mix[None, :], w_ffn_gate.T, w_ffn_up.T, w_ffn_down)
-    part = lax.all_to_all(part, Y_TP, 0, 0, tiled=True)
+    )(rows, gain_mix[None, :], w_ffn_gate.T, w_ffn_up.T, w_ffn_down)
+    both = lax.all_gather(other, "tp", axis=0)
+    part = kernel_call(pair_sum_kernel, sds(own.shape, BF16), 2, name="pair_sum")(own, both)
+    part = part.reshape(NY, NZ, lines, LANES)
+    part = lax.all_to_all(part, "kv_1", 0, 0, tiled=True)
     part = kernel_call(plain_sum_kernel, sds((NZ, lines, LANES), BF16), 1, name="half_sum")(part)
     part = lax.all_to_all(part, "kv_0", 0, 0, tiled=True)
-    summed = kernel_call(
-        ffn_sum_kernel, sds((lines, LANES), F32), 3, scalars=1, name="ffn_sum"
-    )(where, part, hidden_row.reshape(2 * lines, LANES))
+    summed = kernel_call(ffn_sum_kernel, sds((lines, LANES), F32), 2, name="ffn_sum")(
+        part, hidden_row.reshape(2 * lines, LANES)
+    )
     summed = lax.all_gather(summed, "tp", axis=0, tiled=True)
     spread = kernel_call(final_norm_kernel, sds((SEQS, LANES), F32), 2, name="final_norm")(
         summed, gain_out.reshape(2 * lines, LANES)
     )
-    spread = lax.all_to_all(spread.reshape(SEQS, 1, LANES), YZ, 0, 0, tiled=True)
-    layer_out = kernel_call(
-        place_kernel,
-        sds((cols, SEQS), BF16),
-        2,
-        scalars=1,
-        scratch=[pltpu.VMEM((LANES, SEQS), F32)],
-        name="place",
-    )(where, spread.reshape(SEQS, LANES))
+    spread = lax.all_to_all(spread.reshape(SEQS, 1, LANES), KV, 0, 0, tiled=True)
+    layer_out = kernel_call(place_kernel, sds((cols, SEQS), BF16), 1, name="place")(
+        spread.reshape(SEQS, LANES)
+    )
     return (layer_out.T, new_state)
 
 

time: 156 us -> 155 us (level)
  local copies, waits for them, and re-layouts: 0.26 us -> 4.18 us
  Pallas kernels: 10.3 us -> 7.16 us
  blocking collectives: 143 us -> 141 us
    all_to_all x3, blocking collectives: 44 us -> 34.2 us  [the longest x1 17.4 us: on_device(): lax.all_to_all(spread.reshape(SEQS, 1, LANES), KV, 0, 0, tiled=True)]
    all_gather x0 -> x2, blocking collectives: none -> 7.36 us  [the longest x1 5.18 us: on_device(): rows = lax.all_gather(rows, 'tp', axis=0)]
    unnamed x16 -> x24, local copies, waits for them, and re-layouts: 0.03 us -> 3.99 us
    pallas_call x4 -> x5, Pallas kernels: 5.91 us -> 3.78 us  [the longest x1 2.26 us: on_device(): kernel_call(feed_kernel, [sds((SEQS, lines, LANES), BF16)] * 2 + [sds((1,...]
where the time goes in v2:
time: 155 us; the launch traced here: 154 us
  blocking collectives  141 us (91%)
  Pallas kernels  7.16 us (5%)
  local copies, waits for them, and re-layouts  4.18 us (3%)
    all_to_all x1, blocking collectives, on_device(): far = lax.all_to_all(near, 'kv_0', 0, 0, tiled=True)  28.4 us
    all_to_all x1, blocking collectives, on_device(): gathered = lax.all_to_all(attended, YZ, 0, 0, tiled=True)  20.4 us
    all_to_all x1, blocking collectives, on_device(): lax.all_to_all(spread.reshape(SEQS, 1, LANES), KV, 0, 0, tiled=True)  17.4 us
    all_to_all x1, blocking collectives, on_device(): rows = lax.all_to_all(mixed, 'kv_0', 0, 0, tiled=True)  14.7 us
    all_to_all x1, blocking collectives, on_device(): part = lax.all_to_all(part, 'kv_0', 0, 0, tiled=True)  14.3 us
    all_to_all x1, blocking collectives, on_device(): near = lax.all_to_all(parts, 'kv_1', 0, 0, tiled=True)  11.7 us
    all_to_all x1, blocking collectives, on_device(): part = lax.all_to_all(part, 'kv_1', 0, 0, tiled=True)  8.78 us
    all_to_all x1, blocking collectives, on_device(): rows = lax.all_to_all(rows, 'kv_1', 0, 0, tiled=True)  8.05 us

profile of v2, /device:TPU:1, one launch (start us, length us, event | category | flops | bytes accessed | tf_op | source)
XLA Modules:
  0.0 153.6 jit_solution(11727905848150173649)
XLA Ops:
  1.3 0.1 fusion.2
  1.3 0.1 fusion
  1.4 0.1 pad.5.clone
  1.5 0.1 pad.4.clone
  1.6 0.1 maximum_maximum_fusion.aux
  1.7 0.3 copy-done.9
  2.0 0.9 copy-done.5
  2.9 0.9 copy-done.6
  3.8 0.9 copy-done.7
  4.7 0.9 copy-done.8
  5.6 1.5 project.1
  7.1 11.7 %all_to_all.40.x = bf16[4,16,4096]{2,1,0:T(8,128)(2,1)S(1)} all-to-all(bf16[4,16,4096]{2,1,0:T(8,128)(2,1)S(1)} %project.1), channel_id=1, replica_groups=mesh['dp'=4,'kv_0'=16,'kv_1'=4,'tp'=2] {'kv_1'}, dimensions={0} | all-to-all | bytes 1048576 | tf_op jit(solution)/shard_map/all_to_all | solution.py:286
  18.9 0.2 near_sum.1
  19.1 28.4 %all_to_all.41.x = bf16[16,32,128]{2,1,0:T(8,128)(2,1)S(1)} all-to-all(bf16[16,32,128]{2,1,0:T(8,128)(2,1)S(1)} %near_sum.1), channel_id=1, replica_groups=mesh['dp'=4,'kv_0'=16,'kv_1'=4,'tp'=2] {'kv_0'}, dimensions={0} | all-to-all | bytes 262144 | tf_op jit(solution)/shard_map/all_to_all | solution.py:294
  47.5 1.4 retention.1
  48.9 20.4 %all_to_all.42 = bf16[64,8,128]{2,1,0:T(8,128)(2,1)S(1)} all-to-all(bf16[64,8,128]{2,1,0:T(8,128)(2,1)S(1)} %get-tuple-element.11), channel_id=1, replica_groups=mesh['dp'=4,'kv_0'=16,'kv_1'=4,'tp'=2] {'kv_1','kv_0'}, dimensions={0} | all-to-all | bytes 262144 | tf_op jit(solution)/shard_map/all_to_all | solution.py:301
  69.3 5.4 %all-gather = bf16[128,8,128]{2,1,0:T(8,128)(2,1)S(1)} all-gather(bf16[64,8,128]{2,1,0:T(8,128)(2,1)S(1)} %all_to_all.42), channel_id=2, replica_groups=mesh['dp'=4,'kv_0'=16,'kv_1'=4,'tp'=2] {'tp'}, dimensions={0}, use_global_device_ids=true | all-gather | bytes 393216 | tf_op jit(solution)/shard_map/all_gather | solution.py:302
  74.7 0.7 mix.1
  75.4 14.7 %all_to_all.43 = bf16[16,16,128]{2,1,0:T(8,128)(2,1)S(1)} all-to-all(bf16[16,16,128]{2,1,0:T(8,128)(2,1)S(1)} %mix.1), channel_id=1, replica_groups=mesh['dp'=4,'kv_0'=16,'kv_1'=4,'tp'=2] {'kv_0'}, dimensions={0} | all-to-all | bytes 131072 | tf_op jit(solution)/shard_map/all_to_all | solution.py:311
  90.2 0.0 copy-start
  90.2 8.0 %all_to_all.44 = bf16[4,16,16,128]{3,2,1,0:T(8,128)(2,1)S(1)} all-to-all(bf16[4,16,16,128]{3,2,1,0:T(8,128)(2,1)S(1)} %broadcast_in_dim.10), channel_id=1, replica_groups=mesh['dp'=4,'kv_0'=16,'kv_1'=4,'tp'=2] {'kv_1'}, dimensions={0} | all-to-all | bytes 524288 | tf_op jit(solution)/shard_map/all_to_all | solution.py:313
  98.3 5.2 %all-gather.1 = bf16[8,16,16,128]{3,2,1,0:T(8,128)(2,1)S(1)} all-gather(bf16[4,16,16,128]{3,2,1,0:T(8,128)(2,1)S(1)} %all_to_all.44), channel_id=3, replica_groups=mesh['dp'=4,'kv_0'=16,'kv_1'=4,'tp'=2] {'tp'}, dimensions={0}, use_global_device_ids=true | all-gather | bytes 786432 | tf_op jit(solution)/shard_map/all_gather | solution.py:314
  103.4 0.0 copy-done.2
  103.4 2.3 %feed.1 = (bf16[64,16,128]{2,1,0:T(8,128)(2,1)S(1)}, bf16[64,16,128]{2,1,0:T(8,128)(2,1)S(1)}, f32[1,4096]{1,0:T(1,128)S(1)}) custom-call(bf16[2,4,16,16,128]{4,3,2,1,0:T(8,128)(2,1)S(1)} %bitcast.17, f32[1,4096]{1,0:T(1,128)S(1)} %bitcast.25, bf16[86,4096]{1,0:T(8,128)(2,1)S(1)} %bitcast.20, bf16[86,4096]{1,0:T(8,128)(2,1)S(1)} %bitcast.21, ...), custom_call_target="tpu_custom_call" | custom-call | tf_op jit(solution)/shard_map/feed/pallas_call | solution.py:316
  105.7 2.2 %all-gather.2 = bf16[128,16,128]{2,1,0:T(8,128)(2,1)S(1)} all-gather(bf16[64,16,128]{2,1,0:T(8,128)(2,1)S(1)} %get-tuple-element.13), channel_id=4, replica_groups=mesh['dp'=4,'kv_0'=16,'kv_1'=4,'tp'=2] {'tp'}, dimensions={0}, use_global_device_ids=true | all-gather | bytes 786432 | tf_op jit(solution)/shard_map/all_gather | solution.py:327
  107.9 0.1 pair_sum.1
  108.0 8.8 %all_to_all.45.x = bf16[4,16,16,128]{3,2,1,0:T(8,128)(2,1)S(1)} all-to-all(bf16[4,16,16,128]{3,2,1,0:T(8,128)(2,1)S(1)} %bitcast.19), channel_id=1, replica_groups=mesh['dp'=4,'kv_0'=16,'kv_1'=4,'tp'=2] {'kv_1'}, dimensions={0} | all-to-all | bytes 524288 | tf_op jit(solution)/shard_map/all_to_all | solution.py:330
  116.8 14.3 %all_to_all.46.x = bf16[16,16,128]{2,1,0:T(8,128)(2,1)S(1)} all-to-all(bf16[16,16,128]{2,1,0:T(8,128)(2,1)S(1)} %half_sum.1), channel_id=1, replica_groups=mesh['dp'=4,'kv_0'=16,'kv_1'=4,'tp'=2] {'kv_0'}, dimensions={0} | all-to-all | bytes 131072 | tf_op jit(solution)/shard_map/all_to_all | solution.py:332
  131.1 4.2 %all_gather.27.x = f32[32,128]{1,0:T(8,128)S(1)} all-gather(f32[16,128]{1,0:T(8,128)S(1)} %ffn_sum.1), channel_id=1, replica_groups=mesh['dp'=4,'kv_0'=16,'kv_1'=4,'tp'=2] {'tp'}, dimensions={0}, use_global_device_ids=true | all-gather | bytes 24576 | tf_op jit(solution)/shard_map/all_gather | solution.py:336
  135.3 0.2 final_norm.1
  135.5 17.4 %all_to_all.47 = f32[64,1,128]{2,1,0:T(1,128)S(1)} all-to-all(f32[64,1,128]{2,1,0:T(1,128)S(1)} %bitcast.23), channel_id=1, replica_groups=mesh['dp'=4,'kv_0'=16,'kv_1'=4,'tp'=2] {'kv_0','kv_1'}, dimensions={0} | all-to-all | bytes 65536 | tf_op jit(solution)/shard_map/all_to_all | solution.py:340
  152.9 0.7 place.1
  (22 shorter events, 0.1 us)
Async XLA Ops:
  1.3 0.7 copy-start.9
  2.0 0.9 copy-start.5
  2.9 0.9 copy-start.6
  3.8 0.9 copy-start.7
  4.7 0.9 copy-start.8
  18.9 28.6 %copy-start.3 = (f32[1,8,128,128]{3,2,1,0:T(8,128)S(1)}, f32[1,8,128,128]{3,2,1,0:T(8,128)}, u32[]{:S(2)}) copy-start(f32[1,8,128,128]{3,2,1,0:T(8,128)} %state.1) | copy-start | bytes 1572868
  69.3 5.4 %copy-start.4 = (bf16[2048,32]{0,1:T(8,128)(2,1)S(1)}, bf16[2048,32]{0,1:T(8,128)(2,1)}, u32[]{:S(2)}) copy-start(bf16[2048,32]{0,1:T(8,128)(2,1)} %param.20) | copy-start | bytes 393220
  74.7 28.7 %copy-start.2 = (bf16[86,4096]{1,0:T(8,128)(2,1)S(1)}, bf16[86,4096]{1,0:T(8,128)(2,1)}, u32[]{:S(2)}) copy-start(bf16[86,4096]{1,0:T(8,128)(2,1)} %wd.1) | copy-start | bytes 2113540
  90.2 13.3 %copy-start.1 = (bf16[4096,86]{0,1:T(8,128)(2,1)S(1)}, bf16[4096,86]{0,1:T(8,128)(2,1)}, u32[]{:S(2)}) copy-start(bf16[4096,86]{0,1:T(8,128)(2,1)} %param.23) | copy-start | bytes 2113540
  90.2 13.2 %copy-start = (bf16[4096,86]{0,1:T(8,128)(2,1)S(1)}, bf16[4096,86]{0,1:T(8,128)(2,1)}, u32[]{:S(2)}) copy-start(bf16[4096,86]{0,1:T(8,128)(2,1)} %param.22) | copy-start | bytes 2113540
  98.3 5.2 %copy-start.10 = (f32[4096]{0:T(1024)S(1)}, f32[4096]{0:T(1024)}, u32[]{:S(2)}) copy-start(f32[4096]{0:T(1024)} %param.21) | copy-start | bytes 49156
  131.1 4.2 %copy-start.11 = (f32[4096]{0:T(1024)S(1)}, f32[4096]{0:T(1024)}, u32[]{:S(2)}) copy-start(f32[4096]{0:T(1024)} %param.25) | copy-start | bytes 49156

commit v3 on v2

--- a/solution.py
+++ b/solution.py
@@ -54,21 +54,26 @@
     return lax.dot_general(a, b, (((ca,), (cb,)), ((), ())), preferred_element_type=F32)
 
 
-def project_kernel(tok_hbm, wq, wk, wv, wg, out, tok, weights, sems):
+def project_kernel(tok_hbm, wq, wk, wv, wg, out_hbm, tok, weights, out, sems, out_sems):
     sources = (wq, wk, wv, wg)
-    copies = [pltpu.make_async_copy(tok_hbm, tok, sems.at[4])]
+    count = len(sources)
+    width = weights.shape[2]
+    copies = [pltpu.make_async_copy(tok_hbm, tok, sems.at[count])]
     for i, w in enumerate(sources):
         copies.append(pltpu.make_async_copy(w, weights.at[i], sems.at[i]))
     for copy in copies:
         copy.start()
     copies[0].wait()
     rows = mm(perm_matrix(BF16), tok[...], 1, 0).astype(BF16)
-    width = weights.shape[2]
-    for i in range(len(sources)):
+    sends = []
+    for i in range(count):
         copies[1 + i].wait()
-        part = mm(rows, weights[i], 1, 0).astype(BF16)
-        for y in range(NY):
-            out[y, :, i * width : (i + 1) * width] = part[y * NZ : (y + 1) * NZ]
+        out[i] = mm(rows, weights[i], 1, 0).astype(BF16).reshape(NY, NZ, width)
+        cols = pl.ds(i * width, width)
+        sends.append(pltpu.make_async_copy(out.at[i], out_hbm.at[:, :, cols], out_sems.at[i]))
+        sends[i].start()
+    for send in sends:
+        send.wait()
 
 
 def near_sum_kernel(x, out, wide):
@@ -81,7 +86,7 @@
     out[...] = wide[...].astype(BF16)
 
 
-def retention_kernel(x, aux, state, new_state, out):
+def retention_kernel(x, aux, state, state_out, out, new_state, sems):
     heads, dim = state.shape[1], state.shape[2]
     total = x[0].astype(F32)
     for z in range(1, NZ):
@@ -97,9 +102,12 @@
     query_t = query.T
     key_t = key.T
     lines = []
+    sends = []
     for h in range(heads):
         updated = aux[8 + h : 9 + h, :] * state[0, h] + key_t[:, h : h + 1] * value[h : h + 1, :]
-        new_state[0, h] = updated
+        new_state[h] = updated
+        sends.append(pltpu.make_async_copy(new_state.at[h], state_out.at[0, h], sems.at[h]))
+        sends[h].start()
         lines.append(jnp.sum(query_t[:, h : h + 1] * updated, axis=0, keepdims=True))
     retained = jnp.concatenate(lines, axis=0)
     mean = jnp.mean(retained, -1, keepdims=True)
@@ -108,6 +116,8 @@
     silu = gate / (1.0 + jnp.exp(-gate))
     attended = (normed * silu).astype(BF16)
     out[...] = jnp.broadcast_to(attended[None], out.shape)
+    for send in sends:
+        send.wait()
 
 
 def mix_kernel(x, w_t, tok, out, wide):
@@ -272,14 +282,15 @@
     parts = pl.pallas_call(
         project_kernel,
         out_shape=sds((NY, NZ, proj * dim), BF16),
-        in_specs=[pl.BlockSpec(memory_space=pltpu.HBM)] * 5,
-        out_specs=VMEM,
+        in_specs=[pl.BlockSpec(memory_space=pl.ANY)] * 5,
+        out_specs=pl.BlockSpec(memory_space=pl.ANY),
         scratch_shapes=[
             pltpu.VMEM(tokens.shape, BF16),
             pltpu.VMEM((4, *w_query.shape), BF16),
+            pltpu.VMEM((4, NY, NZ, w_query.shape[1]), BF16),
             pltpu.SemaphoreType.DMA((5,)),
+            pltpu.SemaphoreType.DMA((4,)),
         ],
-        compiler_params=PARAMS,
         interpret=INTERPRET,
         name="project",
     )(tokens_in, w_query, w_key, w_value, w_gate)
@@ -292,10 +303,14 @@
         name="near_sum",
     )(near)
     far = lax.all_to_all(near, "kv_0", 0, 0, tiled=True)
-    new_state, attended = kernel_call(
+    new_state, attended = pl.pallas_call(
         retention_kernel,
-        [sds(state.shape, F32), sds((SEQS, heads, dim), BF16)],
-        3,
+        out_shape=[sds(state.shape, F32), sds((SEQS, heads, dim), BF16)],
+        in_specs=[VMEM] * 3,
+        out_specs=[pl.BlockSpec(memory_space=pl.ANY), VMEM],
+        scratch_shapes=[pltpu.VMEM(state.shape[1:], F32), pltpu.SemaphoreType.DMA((heads,))],
+        compiler_params=PARAMS,
+        interpret=INTERPRET,
         name="retention",
     )(far, aux, state)
     gathered = lax.all_to_all(attended, YZ, 0, 0, tiled=True)

time: 155 us -> 152 us (0.981)
  local copies, waits for them, and re-layouts: 4.18 us -> 0.22 us
    unnamed x24 -> x16, local copies, waits for them, and re-layouts: 3.99 us -> 0.03 us
where the time goes in v3:
time: 152 us; the launch traced here: 151 us
  blocking collectives  141 us (93%)
  Pallas kernels  7.9 us (5%)
    all_to_all x1, blocking collectives, on_device(): far = lax.all_to_all(near, 'kv_0', 0, 0, tiled=True)  28.4 us
    all_to_all x1, blocking collectives, on_device(): gathered = lax.all_to_all(attended, YZ, 0, 0, tiled=True)  20.5 us
    all_to_all x1, blocking collectives, on_device(): lax.all_to_all(spread.reshape(SEQS, 1, LANES), KV, 0, 0, tiled=True)  17.4 us
    all_to_all x1, blocking collectives, on_device(): rows = lax.all_to_all(mixed, 'kv_0', 0, 0, tiled=True)  14.7 us
    all_to_all x1, blocking collectives, on_device(): part = lax.all_to_all(part, 'kv_0', 0, 0, tiled=True)  14.3 us
    all_to_all x1, blocking collectives, on_device(): near = lax.all_to_all(parts, 'kv_1', 0, 0, tiled=True)  11.9 us
    all_to_all x1, blocking collectives, on_device(): part = lax.all_to_all(part, 'kv_1', 0, 0, tiled=True)  8.78 us
    all_to_all x1, blocking collectives, on_device(): rows = lax.all_to_all(rows, 'kv_1', 0, 0, tiled=True)  8.05 us

profile of v3, /device:TPU:1, one launch (start us, length us, event | category | flops | bytes accessed | tf_op | source)
XLA Modules:
  0.0 150.6 jit_solution(8963398407071648363)
XLA Ops:
  1.3 0.1 fusion.2
  1.3 0.1 fusion
  1.4 0.1 pad.5.clone
  1.5 0.1 pad.4.clone
  1.6 0.1 maximum_maximum_fusion.aux
  1.6 2.3 %project.1 = bf16[4,16,4096]{2,1,0:T(8,128)(2,1)} custom-call(bf16[64,64]{1,0:T(8,128)(2,1)} %tok.1, bf16[64,1024]{1,0:T(8,128)(2,1)} %wq.1, bf16[64,1024]{1,0:T(8,128)(2,1)} %wk.1, bf16[64,1024]{1,0:T(8,128)(2,1)} %wv.1, bf16[64,1024]{1,0:T(8,128)(2,1)} %wg.1), custom_call_target="tpu_custom_call" | custom-call | tf_op jit(solution)/shard_map/project/pallas_call | solution.py:282
  4.0 11.9 %all_to_all.40.x = bf16[4,16,4096]{2,1,0:T(8,128)(2,1)S(1)} all-to-all(bf16[4,16,4096]{2,1,0:T(8,128)(2,1)} %project.1), channel_id=1, replica_groups=mesh['dp'=4,'kv_0'=16,'kv_1'=4,'tp'=2] {'kv_1'}, dimensions={0} | all-to-all | bytes 1048576 | tf_op jit(solution)/shard_map/all_to_all | solution.py:297
  15.9 0.2 near_sum.1
  16.2 28.4 %all_to_all.41.x = bf16[16,32,128]{2,1,0:T(8,128)(2,1)S(1)} all-to-all(bf16[16,32,128]{2,1,0:T(8,128)(2,1)S(1)} %near_sum.1), channel_id=1, replica_groups=mesh['dp'=4,'kv_0'=16,'kv_1'=4,'tp'=2] {'kv_0'}, dimensions={0} | all-to-all | bytes 262144 | tf_op jit(solution)/shard_map/all_to_all | solution.py:305
  44.6 0.0 copy-done.3
  44.6 1.3 retention.1
  45.9 20.5 %all_to_all.42 = bf16[64,8,128]{2,1,0:T(8,128)(2,1)S(1)} all-to-all(bf16[64,8,128]{2,1,0:T(8,128)(2,1)S(1)} %get-tuple-element.11), channel_id=1, replica_groups=mesh['dp'=4,'kv_0'=16,'kv_1'=4,'tp'=2] {'kv_1','kv_0'}, dimensions={0} | all-to-all | bytes 262144 | tf_op jit(solution)/shard_map/all_to_all | solution.py:316
  66.3 5.4 %all-gather = bf16[128,8,128]{2,1,0:T(8,128)(2,1)S(1)} all-gather(bf16[64,8,128]{2,1,0:T(8,128)(2,1)S(1)} %all_to_all.42), channel_id=2, replica_groups=mesh['dp'=4,'kv_0'=16,'kv_1'=4,'tp'=2] {'tp'}, dimensions={0}, use_global_device_ids=true | all-gather | bytes 393216 | tf_op jit(solution)/shard_map/all_gather | solution.py:317
  71.7 0.0 copy-done.4
  71.7 0.0 copy-done.5
  71.7 0.7 mix.1
  72.4 14.7 %all_to_all.43 = bf16[16,16,128]{2,1,0:T(8,128)(2,1)S(1)} all-to-all(bf16[16,16,128]{2,1,0:T(8,128)(2,1)S(1)} %mix.1), channel_id=1, replica_groups=mesh['dp'=4,'kv_0'=16,'kv_1'=4,'tp'=2] {'kv_0'}, dimensions={0} | all-to-all | bytes 131072 | tf_op jit(solution)/shard_map/all_to_all | solution.py:326
  87.2 0.0 copy-start
  87.2 8.0 %all_to_all.44 = bf16[4,16,16,128]{3,2,1,0:T(8,128)(2,1)S(1)} all-to-all(bf16[4,16,16,128]{3,2,1,0:T(8,128)(2,1)S(1)} %broadcast_in_dim.10), channel_id=1, replica_groups=mesh['dp'=4,'kv_0'=16,'kv_1'=4,'tp'=2] {'kv_1'}, dimensions={0} | all-to-all | bytes 524288 | tf_op jit(solution)/shard_map/all_to_all | solution.py:328
  95.3 5.2 %all-gather.1 = bf16[8,16,16,128]{3,2,1,0:T(8,128)(2,1)S(1)} all-gather(bf16[4,16,16,128]{3,2,1,0:T(8,128)(2,1)S(1)} %all_to_all.44), channel_id=3, replica_groups=mesh['dp'=4,'kv_0'=16,'kv_1'=4,'tp'=2] {'tp'}, dimensions={0}, use_global_device_ids=true | all-gather | bytes 786432 | tf_op jit(solution)/shard_map/all_gather | solution.py:329
  100.4 0.0 copy-done.2
  100.4 0.0 copy-done.1
  100.4 0.0 copy-done
  100.4 2.3 %feed.1 = (bf16[64,16,128]{2,1,0:T(8,128)(2,1)S(1)}, bf16[64,16,128]{2,1,0:T(8,128)(2,1)S(1)}, f32[1,4096]{1,0:T(1,128)S(1)}) custom-call(bf16[2,4,16,16,128]{4,3,2,1,0:T(8,128)(2,1)S(1)} %bitcast.17, f32[1,4096]{1,0:T(1,128)S(1)} %bitcast.25, bf16[86,4096]{1,0:T(8,128)(2,1)S(1)} %bitcast.20, bf16[86,4096]{1,0:T(8,128)(2,1)S(1)} %bitcast.21, ...), custom_call_target="tpu_custom_call" | custom-call | tf_op jit(solution)/shard_map/feed/pallas_call | solution.py:331
  102.7 2.2 %all-gather.2 = bf16[128,16,128]{2,1,0:T(8,128)(2,1)S(1)} all-gather(bf16[64,16,128]{2,1,0:T(8,128)(2,1)S(1)} %get-tuple-element.13), channel_id=4, replica_groups=mesh['dp'=4,'kv_0'=16,'kv_1'=4,'tp'=2] {'tp'}, dimensions={0}, use_global_device_ids=true | all-gather | bytes 786432 | tf_op jit(solution)/shard_map/all_gather | solution.py:342
  104.9 0.1 pair_sum.1
  105.0 8.8 %all_to_all.45.x = bf16[4,16,16,128]{3,2,1,0:T(8,128)(2,1)S(1)} all-to-all(bf16[4,16,16,128]{3,2,1,0:T(8,128)(2,1)S(1)} %bitcast.19), channel_id=1, replica_groups=mesh['dp'=4,'kv_0'=16,'kv_1'=4,'tp'=2] {'kv_1'}, dimensions={0} | all-to-all | bytes 524288 | tf_op jit(solution)/shard_map/all_to_all | solution.py:345
  113.8 14.3 %all_to_all.46.x = bf16[16,16,128]{2,1,0:T(8,128)(2,1)S(1)} all-to-all(bf16[16,16,128]{2,1,0:T(8,128)(2,1)S(1)} %half_sum.1), channel_id=1, replica_groups=mesh['dp'=4,'kv_0'=16,'kv_1'=4,'tp'=2] {'kv_0'}, dimensions={0} | all-to-all | bytes 131072 | tf_op jit(solution)/shard_map/all_to_all | solution.py:347
  128.1 4.2 %all_gather.27.x = f32[32,128]{1,0:T(8,128)S(1)} all-gather(f32[16,128]{1,0:T(8,128)S(1)} %ffn_sum.1), channel_id=1, replica_groups=mesh['dp'=4,'kv_0'=16,'kv_1'=4,'tp'=2] {'tp'}, dimensions={0}, use_global_device_ids=true | all-gather | bytes 24576 | tf_op jit(solution)/shard_map/all_gather | solution.py:351
  132.3 0.2 final_norm.1
  132.5 17.4 %all_to_all.47 = f32[64,1,128]{2,1,0:T(1,128)S(1)} all-to-all(f32[64,1,128]{2,1,0:T(1,128)S(1)} %bitcast.23), channel_id=1, replica_groups=mesh['dp'=4,'kv_0'=16,'kv_1'=4,'tp'=2] {'kv_0','kv_1'}, dimensions={0} | all-to-all | bytes 65536 | tf_op jit(solution)/shard_map/all_to_all | solution.py:355
  149.9 0.7 place.1
  (14 shorter events, 0.1 us)
Async XLA Ops:
  15.9 28.6 %copy-start.3 = (f32[1,8,128,128]{3,2,1,0:T(8,128)S(1)}, f32[1,8,128,128]{3,2,1,0:T(8,128)}, u32[]{:S(2)}) copy-start(f32[1,8,128,128]{3,2,1,0:T(8,128)} %state.1) | copy-start | bytes 1572868
  66.3 5.4 %copy-start.4 = (bf16[2048,32]{0,1:T(8,128)(2,1)S(1)}, bf16[2048,32]{0,1:T(8,128)(2,1)}, u32[]{:S(2)}) copy-start(bf16[2048,32]{0,1:T(8,128)(2,1)} %param.20) | copy-start | bytes 393220
  66.3 5.4 %copy-start.5 = (bf16[64,64]{1,0:T(8,128)(2,1)S(1)}, bf16[64,64]{1,0:T(8,128)(2,1)}, u32[]{:S(2)}) copy-start(bf16[64,64]{1,0:T(8,128)(2,1)} %tok.1) | copy-start | bytes 24580
  71.7 28.7 %copy-start.2 = (bf16[86,4096]{1,0:T(8,128)(2,1)S(1)}, bf16[86,4096]{1,0:T(8,128)(2,1)}, u32[]{:S(2)}) copy-start(bf16[86,4096]{1,0:T(8,128)(2,1)} %wd.1) | copy-start | bytes 2113540
  87.2 13.3 %copy-start.1 = (bf16[4096,86]{0,1:T(8,128)(2,1)S(1)}, bf16[4096,86]{0,1:T(8,128)(2,1)}, u32[]{:S(2)}) copy-start(bf16[4096,86]{0,1:T(8,128)(2,1)} %param.23) | copy-start | bytes 2113540
  87.2 13.2 %copy-start = (bf16[4096,86]{0,1:T(8,128)(2,1)S(1)}, bf16[4096,86]{0,1:T(8,128)(2,1)}, u32[]{:S(2)}) copy-start(bf16[4096,86]{0,1:T(8,128)(2,1)} %param.22) | copy-start | bytes 2113540
  95.3 5.2 %copy-start.6 = (f32[4096]{0:T(1024)S(1)}, f32[4096]{0:T(1024)}, u32[]{:S(2)}) copy-start(f32[4096]{0:T(1024)} %param.21) | copy-start | bytes 49156
  128.1 4.2 %copy-start.7 = (f32[4096]{0:T(1024)S(1)}, f32[4096]{0:T(1024)}, u32[]{:S(2)}) copy-start(f32[4096]{0:T(1024)} %param.25) | copy-start | bytes 49156

commit v4 on v3

--- a/solution.py
+++ b/solution.py
@@ -136,73 +136,69 @@
         for h in range(heads):
             k = (t * heads + h) * dim
             acc += mm(wide[t, :, h, :].astype(BF16), w4[:, k : k + dim], 1, 1)
-    block = lax.broadcasted_iota(jnp.int32, (seqs // groups, LANES), 1) // cols
     per = seqs // groups
+    turn = (lax.axis_index("kv_1") % (groups // tps)) * tps + tp
+    block = lax.broadcasted_iota(jnp.int32, (per, LANES), 1) // cols
+    block = (block + groups - turn) % groups
     packed = acc[0:per]
     for g in range(1, groups):
         packed = jnp.where(block == g, acc[g * per : (g + 1) * per], packed)
     out[...] = jnp.broadcast_to(packed.astype(BF16)[None], out.shape)
 
 
-def feed_kernel(x, gain, wg_t, wu_t, wd, own, other, row, wide, narrow, sums_out):
+def feed_kernel(x, gain, wg_t, wu_t, wd, own, other, row, wide, narrow, stats):
     tps = x.shape[0]
     per = x.shape[3]
     tp = lax.axis_index("tp")
     place = lax.axis_index("kv_1") * NZ + lax.axis_index("kv_0")
     groups = SEQS // per
     cols = LANES // groups
-    chips = LANES // (tps * cols)
+    chips = groups // tps
     width = wide.shape[1]
     lane = lax.broadcasted_iota(jnp.int32, (per, LANES), 1) // cols
     sums = [jnp.zeros((per, LANES), F32) for _ in range(groups)]
     squares = [jnp.zeros((per, LANES), F32) for _ in range(groups)]
     for a in range(SEQS // chips):
-        tiles = [None] * groups
+        sources = []
         for q in range(groups):
             kv = a * chips + q // tps
-            source = x[q % tps, kv % NY, kv // NY].astype(F32)
-            for g in range(groups):
-                shift = ((q - g) * cols) % LANES
-                moved = source if shift == 0 else pltpu.roll(source, shift, 1)
-                tiles[g] = moved if q == 0 else jnp.where(lane == q, moved, tiles[g])
+            sources.append(x[q % tps, kv % NY, kv // NY].astype(F32))
         for g in range(groups):
-            wide[g * per : (g + 1) * per, a * LANES : (a + 1) * LANES] = tiles[g]
-            sums[g] += tiles[g]
-            squares[g] += tiles[g] * tiles[g]
+            tile = sources[(groups - g) % groups]
+            for j in range(1, groups):
+                tile = jnp.where(lane == j, sources[(j - g) % groups], tile)
+            if g:
+                tile = pltpu.roll(tile, LANES - g * cols, 1)
+            wide[g * per : (g + 1) * per, a * LANES : (a + 1) * LANES] = tile
+            sums[g] += tile
+            squares[g] += tile * tile
     mean = jnp.sum(jnp.concatenate(sums, 0), -1, keepdims=True) / width
     var = jnp.sum(jnp.concatenate(squares, 0), -1, keepdims=True) / width - mean * mean
     scale = lax.rsqrt(var + 1e-05)
+    stats[0] = jnp.broadcast_to(mean, stats.shape[1:])
+    stats[1] = jnp.broadcast_to(scale, stats.shape[1:])
     for a in range(width // LANES):
         c = slice(a * LANES, (a + 1) * LANES)
-        hidden = ((wide[:, c] - mean) * scale * gain[:, c]).astype(BF16)
-        narrow[:, c] = hidden
-        wide[:, c] = hidden.astype(F32)
-    row[...] = wide[pl.ds(place, 1), :]
+        narrow[:, c] = ((wide[:, c] - mean) * scale * gain[:, c]).astype(BF16)
+    own_mean = stats[0, pl.ds(place, 1), 0:1]
+    own_scale = stats[1, pl.ds(place, 1), 0:1]
+    own_row = (wide[pl.ds(place, 1), :] - own_mean) * own_scale * gain[...]
+    row[...] = own_row.astype(BF16).astype(F32)
     gate = mm(narrow[...], wg_t[...], 1, 1)
     up = mm(narrow[...], wu_t[...], 1, 1)
     inner = (gate / (1.0 + jnp.exp(-gate)) * up).astype(BF16)
     half = own.shape[1]
-    step = 4
-    for t in range(tps):
-        for c in range(0, half, step):
-            k = (t * half + c) * LANES
-            part = mm(inner, wd[:, k : k + step * LANES], 1, 0)
-            for i in range(step):
-                sums_out[t, :, c + i, :] = part[:, i * LANES : (i + 1) * LANES]
-    own[...] = sums_out[tp].astype(BF16)
-    other[...] = sums_out[1 - tp].astype(BF16)
+    step = 4 * LANES
+    for c in range(0, half, step):
+        mine = pl.multiple_of(tp * half + c, step)
+        theirs = pl.multiple_of((1 - tp) * half + c, step)
+        own[:, c : c + step] = mm(inner, wd[:, pl.ds(mine, step)], 1, 0).astype(BF16)
+        other[:, c : c + step] = mm(inner, wd[:, pl.ds(theirs, step)], 1, 0).astype(BF16)
 
 
 def pair_sum_kernel(own, both, out):
     tp = lax.axis_index("tp")
     out[...] = (own[...].astype(F32) + both[1 - tp].astype(F32)).astype(BF16)
-
-
-def plain_sum_kernel(x, out):
-    total = x[0].astype(F32)
-    for d in range(1, x.shape[0]):
-        total += x[d].astype(F32)
-    out[...] = total.astype(BF16)
 
 
 def ffn_sum_kernel(x, hidden, out):
@@ -330,20 +326,25 @@
     lines = half // LANES
     own, other, hidden_row = kernel_call(
         feed_kernel,
-        [sds((SEQS, lines, LANES), BF16)] * 2 + [sds((1, width), F32)],
+        [sds((SEQS, half), BF16)] * 2 + [sds((1, width), F32)],
         5,
         scratch=[
             pltpu.VMEM((SEQS, width), F32),
             pltpu.VMEM((SEQS, width), BF16),
-            pltpu.VMEM((2, SEQS, lines, LANES), F32),
+            pltpu.VMEM((2, SEQS, LANES), F32),
         ],
         name="feed",
     )(rows, gain_mix[None, :], w_ffn_gate.T, w_ffn_up.T, w_ffn_down)
     both = lax.all_gather(other, "tp", axis=0)
     part = kernel_call(pair_sum_kernel, sds(own.shape, BF16), 2, name="pair_sum")(own, both)
-    part = part.reshape(NY, NZ, lines, LANES)
-    part = lax.all_to_all(part, "kv_1", 0, 0, tiled=True)
-    part = kernel_call(plain_sum_kernel, sds((NZ, lines, LANES), BF16), 1, name="half_sum")(part)
+    part = lax.all_to_all(part.reshape(NY, NZ, half), "kv_1", 0, 0, tiled=True)
+    part = kernel_call(
+        near_sum_kernel,
+        sds((NZ, lines, LANES), BF16),
+        1,
+        scratch=[pltpu.VMEM((NZ, lines, LANES), F32)],
+        name="half_sum",
+    )(part)
     part = lax.all_to_all(part, "kv_0", 0, 0, tiled=True)
     summed = kernel_call(ffn_sum_kernel, sds((lines, LANES), F32), 2, name="ffn_sum")(
         part, hidden_row.reshape(2 * lines, LANES)

time: 152 us -> 151 us (level)
  no operation moved by 1% of the time
where the time goes in v4:
time: 151 us; the launch traced here: 150 us
  blocking collectives  141 us (93%)
  Pallas kernels  7.05 us (5%)
    all_to_all x1, blocking collectives, on_device(): far = lax.all_to_all(near, 'kv_0', 0, 0, tiled=True)  28.4 us
    all_to_all x1, blocking collectives, on_device(): gathered = lax.all_to_all(attended, YZ, 0, 0, tiled=True)  20.5 us
    all_to_all x1, blocking collectives, on_device(): lax.all_to_all(spread.reshape(SEQS, 1, LANES), KV, 0, 0, tiled=True)  17.4 us
    all_to_all x1, blocking collectives, on_device(): rows = lax.all_to_all(mixed, 'kv_0', 0, 0, tiled=True)  14.7 us
    all_to_all x1, blocking collectives, on_device(): part = lax.all_to_all(part, 'kv_0', 0, 0, tiled=True)  14.3 us
    all_to_all x1, blocking collectives, on_device(): near = lax.all_to_all(parts, 'kv_1', 0, 0, tiled=True)  11.9 us
    all_to_all x1, blocking collectives, on_device(): part = lax.all_to_all(part.reshape(NY, NZ, half), 'kv_1', 0, 0, tiled=True)  8.78 us
    all_to_all x1, blocking collectives, on_device(): rows = lax.all_to_all(rows, 'kv_1', 0, 0, tiled=True)  8.05 us

profile of v4, /device:TPU:1, one launch (start us, length us, event | category | flops | bytes accessed | tf_op | source)
XLA Modules:
  0.0 149.8 jit_solution(15242650996556858166)
XLA Ops:
  1.3 0.1 fusion.2
  1.3 0.1 fusion
  1.4 0.1 pad.5.clone
  1.5 0.1 pad.4.clone
  1.6 0.1 maximum_maximum_fusion.aux
  1.6 2.3 %project.1 = bf16[4,16,4096]{2,1,0:T(8,128)(2,1)} custom-call(bf16[64,64]{1,0:T(8,128)(2,1)} %tok.1, bf16[64,1024]{1,0:T(8,128)(2,1)} %wq.1, bf16[64,1024]{1,0:T(8,128)(2,1)} %wk.1, bf16[64,1024]{1,0:T(8,128)(2,1)} %wv.1, bf16[64,1024]{1,0:T(8,128)(2,1)} %wg.1), custom_call_target="tpu_custom_call" | custom-call | tf_op jit(solution)/shard_map/project/pallas_call | solution.py:278
  4.0 11.9 %all_to_all.40.x = bf16[4,16,4096]{2,1,0:T(8,128)(2,1)S(1)} all-to-all(bf16[4,16,4096]{2,1,0:T(8,128)(2,1)} %project.1), channel_id=1, replica_groups=mesh['dp'=4,'kv_0'=16,'kv_1'=4,'tp'=2] {'kv_1'}, dimensions={0} | all-to-all | bytes 1048576 | tf_op jit(solution)/shard_map/all_to_all | solution.py:293
  15.9 0.2 near_sum.1
  16.2 28.4 %all_to_all.41.x = bf16[16,32,128]{2,1,0:T(8,128)(2,1)S(1)} all-to-all(bf16[16,32,128]{2,1,0:T(8,128)(2,1)S(1)} %near_sum.1), channel_id=1, replica_groups=mesh['dp'=4,'kv_0'=16,'kv_1'=4,'tp'=2] {'kv_0'}, dimensions={0} | all-to-all | bytes 262144 | tf_op jit(solution)/shard_map/all_to_all | solution.py:301
  44.6 0.0 copy-done.3
  44.6 1.3 retention.1
  45.9 20.5 %all_to_all.42 = bf16[64,8,128]{2,1,0:T(8,128)(2,1)S(1)} all-to-all(bf16[64,8,128]{2,1,0:T(8,128)(2,1)S(1)} %get-tuple-element.11), channel_id=1, replica_groups=mesh['dp'=4,'kv_0'=16,'kv_1'=4,'tp'=2] {'kv_1','kv_0'}, dimensions={0} | all-to-all | bytes 262144 | tf_op jit(solution)/shard_map/all_to_all | solution.py:312
  66.3 5.4 %all-gather = bf16[128,8,128]{2,1,0:T(8,128)(2,1)S(1)} all-gather(bf16[64,8,128]{2,1,0:T(8,128)(2,1)S(1)} %all_to_all.42), channel_id=2, replica_groups=mesh['dp'=4,'kv_0'=16,'kv_1'=4,'tp'=2] {'tp'}, dimensions={0}, use_global_device_ids=true | all-gather | bytes 393216 | tf_op jit(solution)/shard_map/all_gather | solution.py:313
  71.7 0.0 copy-done.4
  71.7 0.0 copy-done.5
  71.7 0.7 mix.1
  72.4 14.7 %all_to_all.43 = bf16[16,16,128]{2,1,0:T(8,128)(2,1)S(1)} all-to-all(bf16[16,16,128]{2,1,0:T(8,128)(2,1)S(1)} %mix.1), channel_id=1, replica_groups=mesh['dp'=4,'kv_0'=16,'kv_1'=4,'tp'=2] {'kv_0'}, dimensions={0} | all-to-all | bytes 131072 | tf_op jit(solution)/shard_map/all_to_all | solution.py:322
  87.2 0.0 copy-start
  87.2 8.0 %all_to_all.44 = bf16[4,16,16,128]{3,2,1,0:T(8,128)(2,1)S(1)} all-to-all(bf16[4,16,16,128]{3,2,1,0:T(8,128)(2,1)S(1)} %broadcast_in_dim.10), channel_id=1, replica_groups=mesh['dp'=4,'kv_0'=16,'kv_1'=4,'tp'=2] {'kv_1'}, dimensions={0} | all-to-all | bytes 524288 | tf_op jit(solution)/shard_map/all_to_all | solution.py:324
  95.3 5.2 %all-gather.1 = bf16[8,16,16,128]{3,2,1,0:T(8,128)(2,1)S(1)} all-gather(bf16[4,16,16,128]{3,2,1,0:T(8,128)(2,1)S(1)} %all_to_all.44), channel_id=3, replica_groups=mesh['dp'=4,'kv_0'=16,'kv_1'=4,'tp'=2] {'tp'}, dimensions={0}, use_global_device_ids=true | all-gather | bytes 786432 | tf_op jit(solution)/shard_map/all_gather | solution.py:325
  100.4 0.0 copy-done.2
  100.4 0.0 copy-done
  100.4 1.4 feed.1
  101.8 2.2 %all-gather.2 = bf16[128,2048]{1,0:T(8,128)(2,1)S(1)} all-gather(bf16[64,2048]{1,0:T(8,128)(2,1)S(1)} %get-tuple-element.13), channel_id=4, replica_groups=mesh['dp'=4,'kv_0'=16,'kv_1'=4,'tp'=2] {'tp'}, dimensions={0}, use_global_device_ids=true | all-gather | bytes 786432 | tf_op jit(solution)/shard_map/all_gather | solution.py:338
  104.0 0.1 pair_sum.1
  104.1 8.8 %all_to_all.45.x = bf16[4,16,2048]{2,1,0:T(8,128)(2,1)S(1)} all-to-all(bf16[4,16,2048]{2,1,0:T(8,128)(2,1)S(1)} %bitcast.19), channel_id=1, replica_groups=mesh['dp'=4,'kv_0'=16,'kv_1'=4,'tp'=2] {'kv_1'}, dimensions={0} | all-to-all | bytes 524288 | tf_op jit(solution)/shard_map/all_to_all | solution.py:340
  112.8 0.1 half_sum.1
  112.9 14.3 %all_to_all.46.x = bf16[16,16,128]{2,1,0:T(8,128)(2,1)S(1)} all-to-all(bf16[16,16,128]{2,1,0:T(8,128)(2,1)S(1)} %half_sum.1), channel_id=1, replica_groups=mesh['dp'=4,'kv_0'=16,'kv_1'=4,'tp'=2] {'kv_0'}, dimensions={0} | all-to-all | bytes 131072 | tf_op jit(solution)/shard_map/all_to_all | solution.py:348
  127.3 4.2 %all_gather.27.x = f32[32,128]{1,0:T(8,128)S(1)} all-gather(f32[16,128]{1,0:T(8,128)S(1)} %ffn_sum.1), channel_id=1, replica_groups=mesh['dp'=4,'kv_0'=16,'kv_1'=4,'tp'=2] {'tp'}, dimensions={0}, use_global_device_ids=true | all-gather | bytes 24576 | tf_op jit(solution)/shard_map/all_gather | solution.py:352
  131.4 0.2 final_norm.1
  131.7 17.4 %all_to_all.47 = f32[64,1,128]{2,1,0:T(1,128)S(1)} all-to-all(f32[64,1,128]{2,1,0:T(1,128)S(1)} %bitcast.23), channel_id=1, replica_groups=mesh['dp'=4,'kv_0'=16,'kv_1'=4,'tp'=2] {'kv_0','kv_1'}, dimensions={0} | all-to-all | bytes 65536 | tf_op jit(solution)/shard_map/all_to_all | solution.py:356
  149.0 0.7 place.1
  (14 shorter events, 0.1 us)
Async XLA Ops:
  15.9 28.6 %copy-start.3 = (f32[1,8,128,128]{3,2,1,0:T(8,128)S(1)}, f32[1,8,128,128]{3,2,1,0:T(8,128)}, u32[]{:S(2)}) copy-start(f32[1,8,128,128]{3,2,1,0:T(8,128)} %state.1) | copy-start | bytes 1572868
  66.3 5.4 %copy-start.4 = (bf16[2048,32]{0,1:T(8,128)(2,1)S(1)}, bf16[2048,32]{0,1:T(8,128)(2,1)}, u32[]{:S(2)}) copy-start(bf16[2048,32]{0,1:T(8,128)(2,1)} %param.20) | copy-start | bytes 393220
  66.3 5.4 %copy-start.5 = (bf16[64,64]{1,0:T(8,128)(2,1)S(1)}, bf16[64,64]{1,0:T(8,128)(2,1)}, u32[]{:S(2)}) copy-start(bf16[64,64]{1,0:T(8,128)(2,1)} %tok.1) | copy-start | bytes 24580
  71.7 28.7 %copy-start.2 = (bf16[86,4096]{1,0:T(8,128)(2,1)S(1)}, bf16[86,4096]{1,0:T(8,128)(2,1)}, u32[]{:S(2)}) copy-start(bf16[86,4096]{1,0:T(8,128)(2,1)} %wd.1) | copy-start | bytes 2113540
  87.2 13.3 %copy-start.1 = (bf16[4096,86]{0,1:T(8,128)(2,1)S(1)}, bf16[4096,86]{0,1:T(8,128)(2,1)}, u32[]{:S(2)}) copy-start(bf16[4096,86]{0,1:T(8,128)(2,1)} %param.23) | copy-start | bytes 2113540
  87.2 13.2 %copy-start = (bf16[4096,86]{0,1:T(8,128)(2,1)S(1)}, bf16[4096,86]{0,1:T(8,128)(2,1)}, u32[]{:S(2)}) copy-start(bf16[4096,86]{0,1:T(8,128)(2,1)} %param.22) | copy-start | bytes 2113540
  95.3 5.2 %copy-start.6 = (f32[4096]{0:T(1024)S(1)}, f32[4096]{0:T(1024)}, u32[]{:S(2)}) copy-start(f32[4096]{0:T(1024)} %param.21) | copy-start | bytes 49156
  127.3 4.2 %copy-start.7 = (f32[4096]{0:T(1024)S(1)}, f32[4096]{0:T(1024)}, u32[]{:S(2)}) copy-start(f32[4096]{0:T(1024)} %param.25) | copy-start | bytes 49156

commit v5 on v4

--- a/solution.py
+++ b/solution.py
@@ -7,7 +7,6 @@
 from jax.sharding import PartitionSpec as P
 
 KV = ("kv_0", "kv_1")
-YZ = ("kv_1", "kv_0")
 KV_TP = ("kv_0", "kv_1", "tp")
 DP_KV = ("dp", "kv_0", "kv_1")
 F32 = jnp.float32
@@ -16,6 +15,8 @@
 NZ = 16
 NY = 4
 SEQS = NZ * NY
+ORDER_0 = (0, 3, 1, 2)
+ORDER_1 = (2, 0, 3, 1)
 INTERPRET = False
 
 VMEM = pl.BlockSpec(memory_space=pltpu.VMEM)
@@ -54,7 +55,9 @@
     return lax.dot_general(a, b, (((ca,), (cb,)), ((), ())), preferred_element_type=F32)
 
 
-def project_kernel(tok_hbm, wq, wk, wv, wg, out_hbm, tok, weights, out, sems, out_sems):
+def project_kernel(
+    tok_hbm, wq, wk, wv, wg, w_out, out_hbm, tok, weights, out, residual, sems, out_sems, share_sems
+):
     sources = (wq, wk, wv, wg)
     count = len(sources)
     width = weights.shape[2]
@@ -63,15 +66,31 @@
         copies.append(pltpu.make_async_copy(w, weights.at[i], sems.at[i]))
     for copy in copies:
         copy.start()
+    sends = []
+    depth = w_out.shape[1]
+    for part in range(w_out.shape[0] // NZ):
+        cols = pl.ds(count * width + part * depth, depth)
+        for y in range(NY):
+            sends.append(
+                pltpu.make_async_copy(
+                    w_out.at[pl.ds(part * NZ, NZ)], out_hbm.at[y, :, cols], share_sems.at[part, y]
+                )
+            )
+            sends[-1].start()
     copies[0].wait()
     rows = mm(perm_matrix(BF16), tok[...], 1, 0).astype(BF16)
-    sends = []
+    residual[...] = jnp.zeros(residual.shape, BF16)
+    for y in range(NY):
+        residual[y, :, 0 : rows.shape[1]] = rows[y * NZ : (y + 1) * NZ]
+    tail = pl.ds(out_hbm.shape[2] - LANES, LANES)
+    sends.append(pltpu.make_async_copy(residual, out_hbm.at[:, :, tail], out_sems.at[count]))
+    sends[-1].start()
     for i in range(count):
         copies[1 + i].wait()
         out[i] = mm(rows, weights[i], 1, 0).astype(BF16).reshape(NY, NZ, width)
         cols = pl.ds(i * width, width)
         sends.append(pltpu.make_async_copy(out.at[i], out_hbm.at[:, :, cols], out_sems.at[i]))
-        sends[i].start()
+        sends[-1].start()
     for send in sends:
         send.wait()
 
@@ -120,58 +139,52 @@
         send.wait()
 
 
-def mix_kernel(x, w_t, tok, out, wide):
+def mix_kernel(x, shared, out, wide):
     tp = lax.axis_index("tp")
-    tps, seqs, heads, dim = x.shape
-    cols = w_t.shape[0]
-    groups = LANES // cols
+    tps, _, heads, dim = x.shape
+    cols = LANES // NY
+    depth = tps * heads * dim
+    first = shared.shape[2] - LANES - 2 * depth
     wide[...] = x[...].astype(F32)
-    own = lax.broadcasted_iota(jnp.int32, (tok.shape[1], LANES), 0)
-    lane = lax.broadcasted_iota(jnp.int32, (tok.shape[1], LANES), 1)
-    pick = (own == tp * cols + lane % cols).astype(F32).astype(BF16)
-    rows = mm(perm_matrix(BF16), tok[...], 1, 0).astype(BF16)
-    acc = mm(rows, pick, 1, 0)
-    w4 = jnp.concatenate([w_t[...]] * groups, axis=0)
+    owners = [jnp.where(tp == 0, even, odd) for even, odd in zip(ORDER_0, ORDER_1)]
+    own = lax.broadcasted_iota(jnp.int32, (LANES, LANES), 0)
+    lane = lax.broadcasted_iota(jnp.int32, (LANES, LANES), 1)
+    acc = jnp.zeros((NZ, LANES), F32)
+    for b, y in enumerate(owners):
+        pick = (own == tp * cols + lane % cols) & (lane // cols == b)
+        pick = pick.astype(F32).astype(BF16)
+        acc += mm(shared[y, :, first + 2 * depth :], pick, 1, 0)
     for t in range(tps):
         for h in range(heads):
-            k = (t * heads + h) * dim
-            acc += mm(wide[t, :, h, :].astype(BF16), w4[:, k : k + dim], 1, 1)
-    per = seqs // groups
-    turn = (lax.axis_index("kv_1") % (groups // tps)) * tps + tp
-    block = lax.broadcasted_iota(jnp.int32, (per, LANES), 1) // cols
-    block = (block + groups - turn) % groups
-    packed = acc[0:per]
-    for g in range(1, groups):
-        packed = jnp.where(block == g, acc[g * per : (g + 1) * per], packed)
-    out[...] = jnp.broadcast_to(packed.astype(BF16)[None], out.shape)
+            k = first + (t * heads + h) * dim
+            pieces = []
+            for y in owners:
+                pieces.append(shared[y, :, k : k + dim])
+                pieces.append(shared[y, :, k + depth : k + depth + dim])
+            weight = jnp.concatenate(pieces, axis=0)
+            acc += mm(wide[t, :, h, :].astype(BF16), weight, 1, 1)
+    out[...] = jnp.broadcast_to(acc.astype(BF16)[None], out.shape)
 
 
 def feed_kernel(x, gain, wg_t, wu_t, wd, own, other, row, wide, narrow, stats):
-    tps = x.shape[0]
     per = x.shape[3]
     tp = lax.axis_index("tp")
     place = lax.axis_index("kv_1") * NZ + lax.axis_index("kv_0")
-    groups = SEQS // per
-    cols = LANES // groups
-    chips = groups // tps
+    cols = LANES // NY
     width = wide.shape[1]
-    lane = lax.broadcasted_iota(jnp.int32, (per, LANES), 1) // cols
-    sums = [jnp.zeros((per, LANES), F32) for _ in range(groups)]
-    squares = [jnp.zeros((per, LANES), F32) for _ in range(groups)]
-    for a in range(SEQS // chips):
-        sources = []
-        for q in range(groups):
-            kv = a * chips + q // tps
-            sources.append(x[q % tps, kv % NY, kv // NY].astype(F32))
-        for g in range(groups):
-            tile = sources[(groups - g) % groups]
-            for j in range(1, groups):
-                tile = jnp.where(lane == j, sources[(j - g) % groups], tile)
-            if g:
-                tile = pltpu.roll(tile, LANES - g * cols, 1)
-            wide[g * per : (g + 1) * per, a * LANES : (a + 1) * LANES] = tile
-            sums[g] += tile
-            squares[g] += tile * tile
+    odd = (lax.broadcasted_iota(jnp.int32, (per, LANES), 1) // cols) % 2 == 1
+    sums = [jnp.zeros((per, LANES), F32) for _ in range(NY)]
+    squares = [jnp.zeros((per, LANES), F32) for _ in range(NY)]
+    for z in range(NZ):
+        for y in range(NY):
+            a = x[0, y, z].astype(F32)
+            b = x[1, y, z].astype(F32)
+            low = jnp.where(odd, b, a)
+            high = pltpu.roll(jnp.where(odd, a, b), cols, 1)
+            wide[y * per : (y + 1) * per, 2 * z * LANES : (2 * z + 1) * LANES] = low
+            wide[y * per : (y + 1) * per, (2 * z + 1) * LANES : (2 * z + 2) * LANES] = high
+            sums[y] += low + high
+            squares[y] += low * low + high * high
     mean = jnp.sum(jnp.concatenate(sums, 0), -1, keepdims=True) / width
     var = jnp.sum(jnp.concatenate(squares, 0), -1, keepdims=True) / width - mean * mean
     scale = lax.rsqrt(var + 1e-05)
@@ -275,33 +288,36 @@
     )
 
     tokens_in, aux = lax.optimization_barrier((tokens, aux))
+    depth = w_out.shape[0]
     parts = pl.pallas_call(
         project_kernel,
-        out_shape=sds((NY, NZ, proj * dim), BF16),
-        in_specs=[pl.BlockSpec(memory_space=pl.ANY)] * 5,
+        out_shape=sds((NY, NZ, proj * dim + depth * cols // NZ + LANES), BF16),
+        in_specs=[pl.BlockSpec(memory_space=pl.ANY)] * 6,
         out_specs=pl.BlockSpec(memory_space=pl.ANY),
         scratch_shapes=[
             pltpu.VMEM(tokens.shape, BF16),
             pltpu.VMEM((4, *w_query.shape), BF16),
             pltpu.VMEM((4, NY, NZ, w_query.shape[1]), BF16),
+            pltpu.VMEM((NY, NZ, LANES), BF16),
             pltpu.SemaphoreType.DMA((5,)),
-            pltpu.SemaphoreType.DMA((4,)),
+            pltpu.SemaphoreType.DMA((5,)),
+            pltpu.SemaphoreType.DMA((cols // NZ, NY)),
         ],
         interpret=INTERPRET,
         name="project",
-    )(tokens_in, w_query, w_key, w_value, w_gate)
-    near = lax.all_to_all(parts, "kv_1", 0, 0, tiled=True)
+    )(tokens_in, w_query, w_key, w_value, w_gate, w_out.T)
+    shared = lax.all_to_all(parts, "kv_1", 0, 0, tiled=True)
     near = kernel_call(
         near_sum_kernel,
         sds((NZ, proj, dim), BF16),
         1,
         scratch=[pltpu.VMEM((NZ, proj, dim), F32)],
         name="near_sum",
-    )(near)
+    )(shared)
     far = lax.all_to_all(near, "kv_0", 0, 0, tiled=True)
     new_state, attended = pl.pallas_call(
         retention_kernel,
-        out_shape=[sds(state.shape, F32), sds((SEQS, heads, dim), BF16)],
+        out_shape=[sds(state.shape, F32), sds((NZ, heads, dim), BF16)],
         in_specs=[VMEM] * 3,
         out_specs=[pl.BlockSpec(memory_space=pl.ANY), VMEM],
         scratch_shapes=[pltpu.VMEM(state.shape[1:], F32), pltpu.SemaphoreType.DMA((heads,))],
@@ -309,16 +325,15 @@
         interpret=INTERPRET,
         name="retention",
     )(far, aux, state)
-    gathered = lax.all_to_all(attended, YZ, 0, 0, tiled=True)
+    gathered = lax.all_to_all(attended, "kv_0", 0, 0, tiled=True)
     gathered = lax.all_gather(gathered, "tp", axis=0)
-    per = SEQS * cols // LANES
     mixed = kernel_call(
         mix_kernel,
-        sds((NZ, per, LANES), BF16),
-        3,
-        scratch=[pltpu.VMEM((2, SEQS, heads, dim), F32)],
+        sds((NZ, NZ, LANES), BF16),
+        2,
+        scratch=[pltpu.VMEM((2, NZ, heads, dim), F32)],
         name="mix",
-    )(gathered.reshape(2, SEQS, heads, dim), w_out.T, tokens)
+    )(gathered, shared)
     rows = lax.all_to_all(mixed, "kv_0", 0, 0, tiled=True)
     rows = jnp.broadcast_to(rows[None], (NY, *rows.shape))
     rows = lax.all_to_all(rows, "kv_1", 0, 0, tiled=True)

time: 151 us -> 166 us (1.099)
  Pallas kernels: 7.05 us -> 21.6 us
    pallas_call x3, Pallas kernels: 4.32 us -> 18.9 us  [the longest x1 17.2 us: on_device(): pl.pallas_call(project_kernel, out_shape=sds((NY, NZ, proj * dim + depth...]
    all_to_all x1, blocking collectives: 28.4 us -> 31.1 us  [on_device(): far = lax.all_to_all(near, 'kv_0', 0, 0, tiled=True)]
where the time goes in v5:
time: 166 us; the launch traced here: 165 us
  blocking collectives  141 us (85%)
  Pallas kernels  21.6 us (13%)
    all_to_all x1, blocking collectives, on_device(): far = lax.all_to_all(near, 'kv_0', 0, 0, tiled=True)  31.1 us
    all_to_all x1, blocking collectives, on_device(): lax.all_to_all(spread.reshape(SEQS, 1, LANES), KV, 0, 0, tiled=True)  17.4 us
    pallas_call x1, Pallas kernels, on_device(): pl.pallas_call(project_kernel, out_shape=sds((NY, NZ, proj * dim + depth...  17.2 us
    all_to_all x1, blocking collectives, on_device(): gathered = lax.all_to_all(attended, 'kv_0', 0, 0, tiled=True)  16.1 us
    all_to_all x1, blocking collectives, on_device(): shared = lax.all_to_all(parts, 'kv_1', 0, 0, tiled=True)  14.8 us
    all_to_all x1, blocking collectives, on_device(): rows = lax.all_to_all(mixed, 'kv_0', 0, 0, tiled=True)  14.5 us
    all_to_all x1, blocking collectives, on_device(): part = lax.all_to_all(part, 'kv_0', 0, 0, tiled=True)  14.3 us
    all_to_all x1, blocking collectives, on_device(): part = lax.all_to_all(part.reshape(NY, NZ, half), 'kv_1', 0, 0, tiled=True)  8.78 us

profile of v5, /device:TPU:1, one launch (start us, length us, event | category | flops | bytes accessed | tf_op | source)
XLA Modules:
  0.0 164.8 jit_solution(18278544237800972969)
XLA Ops:
  1.3 0.1 fusion.2
  1.3 0.1 fusion
  1.4 0.1 pad.5.clone
  1.5 0.1 pad.4.clone
  1.6 0.1 maximum_maximum_fusion.aux
  1.6 17.2 %project.1 = bf16[4,16,8320]{2,1,0:T(8,128)(2,1)} custom-call(bf16[64,64]{1,0:T(8,128)(2,1)} %tok_hbm, bf16[64,1024]{1,0:T(8,128)(2,1)} %wq.1, bf16[64,1024]{1,0:T(8,128)(2,1)} %wk.1, bf16[64,1024]{1,0:T(8,128)(2,1)} %wv.1, bf16[64,1024]{1,0:T(8,128)(2,1)} %wg.1, bf16[32,2048]{1,0:T(8,128)(2,1)} %bitcast.27), custom_call_target="tpu_custom_call" | custom-call | tf_op jit(solution)/shard_map/project/pallas_call | solution.py:292
  18.8 14.8 %all_to_all.40.x.shared = bf16[4,16,8320]{2,1,0:T(8,128)(2,1)S(1)} all-to-all(bf16[4,16,8320]{2,1,0:T(8,128)(2,1)} %project.1), channel_id=1, replica_groups=mesh['dp'=4,'kv_0'=16,'kv_1'=4,'tp'=2] {'kv_1'}, dimensions={0} | all-to-all | bytes 2129920 | tf_op jit(solution)/shard_map/all_to_all | solution.py:309
  33.7 0.2 near_sum.1
  33.9 31.1 %all_to_all.41.x = bf16[16,32,128]{2,1,0:T(8,128)(2,1)S(1)} all-to-all(bf16[16,32,128]{2,1,0:T(8,128)(2,1)S(1)} %near_sum.1), channel_id=1, replica_groups=mesh['dp'=4,'kv_0'=16,'kv_1'=4,'tp'=2] {'kv_0'}, dimensions={0} | all-to-all | bytes 262144 | tf_op jit(solution)/shard_map/all_to_all | solution.py:317
  65.0 0.0 copy-done.3
  65.0 1.3 retention.1
  66.3 16.1 %all_to_all.42 = bf16[16,8,128]{2,1,0:T(8,128)(2,1)S(1)} all-to-all(bf16[16,8,128]{2,1,0:T(8,128)(2,1)S(1)} %get-tuple-element.11), channel_id=1, replica_groups=mesh['dp'=4,'kv_0'=16,'kv_1'=4,'tp'=2] {'kv_0'}, dimensions={0} | all-to-all | bytes 65536 | tf_op jit(solution)/shard_map/all_to_all | solution.py:328
  82.4 5.4 %all-gather = bf16[32,8,128]{2,1,0:T(8,128)(2,1)S(1)} all-gather(bf16[16,8,128]{2,1,0:T(8,128)(2,1)S(1)} %all_to_all.42), channel_id=2, replica_groups=mesh['dp'=4,'kv_0'=16,'kv_1'=4,'tp'=2] {'tp'}, dimensions={0}, use_global_device_ids=true | all-gather | bytes 98304 | tf_op jit(solution)/shard_map/all_gather | solution.py:329
  87.8 0.4 mix.1
  88.2 0.0 copy-start
  88.2 0.0 copy-start.1
  88.2 0.0 copy-start.4
  88.2 14.5 %all_to_all.43 = bf16[16,16,128]{2,1,0:T(8,128)(2,1)S(1)} all-to-all(bf16[16,16,128]{2,1,0:T(8,128)(2,1)S(1)} %mix.1), channel_id=1, replica_groups=mesh['dp'=4,'kv_0'=16,'kv_1'=4,'tp'=2] {'kv_0'}, dimensions={0} | all-to-all | bytes 131072 | tf_op jit(solution)/shard_map/all_to_all | solution.py:337
  102.7 7.9 %all_to_all.44 = bf16[4,16,16,128]{3,2,1,0:T(8,128)(2,1)S(1)} all-to-all(bf16[4,16,16,128]{3,2,1,0:T(8,128)(2,1)S(1)} %broadcast_in_dim.10), channel_id=1, replica_groups=mesh['dp'=4,'kv_0'=16,'kv_1'=4,'tp'=2] {'kv_1'}, dimensions={0} | all-to-all | bytes 524288 | tf_op jit(solution)/shard_map/all_to_all | solution.py:339
  110.7 4.9 %all-gather.1 = bf16[8,16,16,128]{3,2,1,0:T(8,128)(2,1)S(1)} all-gather(bf16[4,16,16,128]{3,2,1,0:T(8,128)(2,1)S(1)} %all_to_all.44), channel_id=3, replica_groups=mesh['dp'=4,'kv_0'=16,'kv_1'=4,'tp'=2] {'tp'}, dimensions={0}, use_global_device_ids=true | all-gather | bytes 786432 | tf_op jit(solution)/shard_map/all_gather | solution.py:340
  115.6 0.0 copy-done.2
  115.6 0.0 copy-done.1
  115.6 1.3 feed.1
  116.9 2.2 %all-gather.2 = bf16[128,2048]{1,0:T(8,128)(2,1)S(1)} all-gather(bf16[64,2048]{1,0:T(8,128)(2,1)S(1)} %get-tuple-element.13), channel_id=4, replica_groups=mesh['dp'=4,'kv_0'=16,'kv_1'=4,'tp'=2] {'tp'}, dimensions={0}, use_global_device_ids=true | all-gather | bytes 786432 | tf_op jit(solution)/shard_map/all_gather | solution.py:353
  119.1 0.1 pair_sum.1
  119.1 8.8 %all_to_all.45.x = bf16[4,16,2048]{2,1,0:T(8,128)(2,1)S(1)} all-to-all(bf16[4,16,2048]{2,1,0:T(8,128)(2,1)S(1)} %bitcast.18), channel_id=1, replica_groups=mesh['dp'=4,'kv_0'=16,'kv_1'=4,'tp'=2] {'kv_1'}, dimensions={0} | all-to-all | bytes 524288 | tf_op jit(solution)/shard_map/all_to_all | solution.py:355
  127.9 0.1 half_sum.1
  128.0 14.3 %all_to_all.46.x = bf16[16,16,128]{2,1,0:T(8,128)(2,1)S(1)} all-to-all(bf16[16,16,128]{2,1,0:T(8,128)(2,1)S(1)} %half_sum.1), channel_id=1, replica_groups=mesh['dp'=4,'kv_0'=16,'kv_1'=4,'tp'=2] {'kv_0'}, dimensions={0} | all-to-all | bytes 131072 | tf_op jit(solution)/shard_map/all_to_all | solution.py:363
  142.3 4.2 %all_gather.27.x = f32[32,128]{1,0:T(8,128)S(1)} all-gather(f32[16,128]{1,0:T(8,128)S(1)} %ffn_sum.1), channel_id=1, replica_groups=mesh['dp'=4,'kv_0'=16,'kv_1'=4,'tp'=2] {'tp'}, dimensions={0}, use_global_device_ids=true | all-gather | bytes 24576 | tf_op jit(solution)/shard_map/all_gather | solution.py:367
  146.5 0.2 final_norm.1
  146.7 17.4 %all_to_all.47 = f32[64,1,128]{2,1,0:T(1,128)S(1)} all-to-all(f32[64,1,128]{2,1,0:T(1,128)S(1)} %bitcast.23), channel_id=1, replica_groups=mesh['dp'=4,'kv_0'=16,'kv_1'=4,'tp'=2] {'kv_0','kv_1'}, dimensions={0} | all-to-all | bytes 65536 | tf_op jit(solution)/shard_map/all_to_all | solution.py:371
  164.1 0.7 place.1
  (10 shorter events, 0.1 us)
Async XLA Ops:
  33.7 31.4 %copy-start.3 = (f32[1,8,128,128]{3,2,1,0:T(8,128)S(1)}, f32[1,8,128,128]{3,2,1,0:T(8,128)}, u32[]{:S(2)}) copy-start(f32[1,8,128,128]{3,2,1,0:T(8,128)} %state.1) | copy-start | bytes 1572868
  87.8 27.8 %copy-start.2 = (bf16[86,4096]{1,0:T(8,128)(2,1)S(1)}, bf16[86,4096]{1,0:T(8,128)(2,1)}, u32[]{:S(2)}) copy-start(bf16[86,4096]{1,0:T(8,128)(2,1)} %wd.1) | copy-start | bytes 2113540
  88.2 27.4 %copy-start = (bf16[4096,86]{0,1:T(8,128)(2,1)S(1)}, bf16[4096,86]{0,1:T(8,128)(2,1)}, u32[]{:S(2)}) copy-start(bf16[4096,86]{0,1:T(8,128)(2,1)} %param.22) | copy-start | bytes 2113540
  88.2 27.4 %copy-start.1 = (bf16[4096,86]{0,1:T(8,128)(2,1)S(1)}, bf16[4096,86]{0,1:T(8,128)(2,1)}, u32[]{:S(2)}) copy-start(bf16[4096,86]{0,1:T(8,128)(2,1)} %param.23) | copy-start | bytes 2113540
  88.2 27.3 %copy-start.4 = (f32[4096]{0:T(1024)S(1)}, f32[4096]{0:T(1024)}, u32[]{:S(2)}) copy-start(f32[4096]{0:T(1024)} %param.21) | copy-start | bytes 49156
  119.1 27.4 %copy-start.5 = (f32[4096]{0:T(1024)S(1)}, f32[4096]{0:T(1024)}, u32[]{:S(2)}) copy-start(f32[4096]{0:T(1024)} %param.25) | copy-start | bytes 49156

commit v6 on v5

--- a/solution.py
+++ b/solution.py
@@ -56,7 +56,8 @@
 
 
 def project_kernel(
-    tok_hbm, wq, wk, wv, wg, w_out, out_hbm, tok, weights, out, residual, sems, out_sems, share_sems
+    tok_hbm, wq, wk, wv, wg, w_out, out_hbm,
+    tok, weights, out, share, residual, sems, out_sems, share_sems,
 ):
     sources = (wq, wk, wv, wg)
     count = len(sources)
@@ -66,17 +67,9 @@
         copies.append(pltpu.make_async_copy(w, weights.at[i], sems.at[i]))
     for copy in copies:
         copy.start()
+    load = pltpu.make_async_copy(w_out, share, sems.at[count + 1])
+    load.start()
     sends = []
-    depth = w_out.shape[1]
-    for part in range(w_out.shape[0] // NZ):
-        cols = pl.ds(count * width + part * depth, depth)
-        for y in range(NY):
-            sends.append(
-                pltpu.make_async_copy(
-                    w_out.at[pl.ds(part * NZ, NZ)], out_hbm.at[y, :, cols], share_sems.at[part, y]
-                )
-            )
-            sends[-1].start()
     copies[0].wait()
     rows = mm(perm_matrix(BF16), tok[...], 1, 0).astype(BF16)
     residual[...] = jnp.zeros(residual.shape, BF16)
@@ -91,6 +84,17 @@
         cols = pl.ds(i * width, width)
         sends.append(pltpu.make_async_copy(out.at[i], out_hbm.at[:, :, cols], out_sems.at[i]))
         sends[-1].start()
+    load.wait()
+    depth = share.shape[1]
+    for part in range(share.shape[0] // NZ):
+        cols = pl.ds(count * width + part * depth, depth)
+        for y in range(NY):
+            sends.append(
+                pltpu.make_async_copy(
+                    share.at[pl.ds(part * NZ, NZ)], out_hbm.at[y, :, cols], share_sems.at[part, y]
+                )
+            )
+            sends[-1].start()
     for send in sends:
         send.wait()
 
@@ -298,8 +302,9 @@
             pltpu.VMEM(tokens.shape, BF16),
             pltpu.VMEM((4, *w_query.shape), BF16),
             pltpu.VMEM((4, NY, NZ, w_query.shape[1]), BF16),
+            pltpu.VMEM((cols, depth), BF16),
             pltpu.VMEM((NY, NZ, LANES), BF16),
-            pltpu.SemaphoreType.DMA((5,)),
+            pltpu.SemaphoreType.DMA((6,)),
             pltpu.SemaphoreType.DMA((5,)),
             pltpu.SemaphoreType.DMA((cols // NZ, NY)),
         ],

time: 166 us -> 151 us (0.910)
  Pallas kernels: 21.6 us -> 7.04 us
    pallas_call x1, Pallas kernels: 17.2 us -> 2.64 us  [on_device(): pl.pallas_call(project_kernel, out_shape=sds((NY, NZ, proj * dim + depth...]
where the time goes in v6:
time: 151 us; the launch traced here: 150 us
  blocking collectives  141 us (93%)
  Pallas kernels  7.04 us (5%)
    all_to_all x1, blocking collectives, on_device(): far = lax.all_to_all(near, 'kv_0', 0, 0, tiled=True)  31.1 us
    all_to_all x1, blocking collectives, on_device(): lax.all_to_all(spread.reshape(SEQS, 1, LANES), KV, 0, 0, tiled=True)  17.4 us
    all_to_all x1, blocking collectives, on_device(): gathered = lax.all_to_all(attended, 'kv_0', 0, 0, tiled=True)  16.1 us
    all_to_all x1, blocking collectives, on_device(): shared = lax.all_to_all(parts, 'kv_1', 0, 0, tiled=True)  14.8 us
    all_to_all x1, blocking collectives, on_device(): rows = lax.all_to_all(mixed, 'kv_0', 0, 0, tiled=True)  14.5 us
    all_to_all x1, blocking collectives, on_device(): part = lax.all_to_all(part, 'kv_0', 0, 0, tiled=True)  14.3 us
    all_to_all x1, blocking collectives, on_device(): part = lax.all_to_all(part.reshape(NY, NZ, half), 'kv_1', 0, 0, tiled=True)  8.78 us
    all_to_all x1, blocking collectives, on_device(): rows = lax.all_to_all(rows, 'kv_1', 0, 0, tiled=True)  7.92 us

profile of v6, /device:TPU:1, one launch (start us, length us, event | category | flops | bytes accessed | tf_op | source)
XLA Modules:
  0.0 150.3 jit_solution(9394245843502296607)
XLA Ops:
  1.3 0.1 fusion.2
  1.3 0.1 fusion
  1.4 0.1 pad.5.clone
  1.5 0.1 pad.4.clone
  1.6 0.1 maximum_maximum_fusion.aux
  1.6 2.6 %project.1 = bf16[4,16,8320]{2,1,0:T(8,128)(2,1)} custom-call(bf16[64,64]{1,0:T(8,128)(2,1)} %tok_hbm, bf16[64,1024]{1,0:T(8,128)(2,1)} %wq.1, bf16[64,1024]{1,0:T(8,128)(2,1)} %wk.1, bf16[64,1024]{1,0:T(8,128)(2,1)} %wv.1, bf16[64,1024]{1,0:T(8,128)(2,1)} %wg.1, bf16[32,2048]{1,0:T(8,128)(2,1)} %bitcast.27), custom_call_target="tpu_custom_call" | custom-call | tf_op jit(solution)/shard_map/project/pallas_call | solution.py:296
  4.3 14.8 %all_to_all.40.x.shared = bf16[4,16,8320]{2,1,0:T(8,128)(2,1)S(1)} all-to-all(bf16[4,16,8320]{2,1,0:T(8,128)(2,1)} %project.1), channel_id=1, replica_groups=mesh['dp'=4,'kv_0'=16,'kv_1'=4,'tp'=2] {'kv_1'}, dimensions={0} | all-to-all | bytes 2129920 | tf_op jit(solution)/shard_map/all_to_all | solution.py:314
  19.1 0.2 near_sum.1
  19.4 31.1 %all_to_all.41.x = bf16[16,32,128]{2,1,0:T(8,128)(2,1)S(1)} all-to-all(bf16[16,32,128]{2,1,0:T(8,128)(2,1)S(1)} %near_sum.1), channel_id=1, replica_groups=mesh['dp'=4,'kv_0'=16,'kv_1'=4,'tp'=2] {'kv_0'}, dimensions={0} | all-to-all | bytes 262144 | tf_op jit(solution)/shard_map/all_to_all | solution.py:322
  50.5 0.0 copy-done.3
  50.5 1.3 retention.1
  51.8 16.1 %all_to_all.42 = bf16[16,8,128]{2,1,0:T(8,128)(2,1)S(1)} all-to-all(bf16[16,8,128]{2,1,0:T(8,128)(2,1)S(1)} %get-tuple-element.11), channel_id=1, replica_groups=mesh['dp'=4,'kv_0'=16,'kv_1'=4,'tp'=2] {'kv_0'}, dimensions={0} | all-to-all | bytes 65536 | tf_op jit(solution)/shard_map/all_to_all | solution.py:333
  67.9 5.4 %all-gather = bf16[32,8,128]{2,1,0:T(8,128)(2,1)S(1)} all-gather(bf16[16,8,128]{2,1,0:T(8,128)(2,1)S(1)} %all_to_all.42), channel_id=2, replica_groups=mesh['dp'=4,'kv_0'=16,'kv_1'=4,'tp'=2] {'tp'}, dimensions={0}, use_global_device_ids=true | all-gather | bytes 98304 | tf_op jit(solution)/shard_map/all_gather | solution.py:334
  73.2 0.4 mix.1
  73.7 0.0 copy-start
  73.7 0.0 copy-start.1
  73.7 0.0 copy-start.4
  73.7 14.5 %all_to_all.43 = bf16[16,16,128]{2,1,0:T(8,128)(2,1)S(1)} all-to-all(bf16[16,16,128]{2,1,0:T(8,128)(2,1)S(1)} %mix.1), channel_id=1, replica_groups=mesh['dp'=4,'kv_0'=16,'kv_1'=4,'tp'=2] {'kv_0'}, dimensions={0} | all-to-all | bytes 131072 | tf_op jit(solution)/shard_map/all_to_all | solution.py:342
  88.2 7.9 %all_to_all.44 = bf16[4,16,16,128]{3,2,1,0:T(8,128)(2,1)S(1)} all-to-all(bf16[4,16,16,128]{3,2,1,0:T(8,128)(2,1)S(1)} %broadcast_in_dim.10), channel_id=1, replica_groups=mesh['dp'=4,'kv_0'=16,'kv_1'=4,'tp'=2] {'kv_1'}, dimensions={0} | all-to-all | bytes 524288 | tf_op jit(solution)/shard_map/all_to_all | solution.py:344
  96.1 4.9 %all-gather.1 = bf16[8,16,16,128]{3,2,1,0:T(8,128)(2,1)S(1)} all-gather(bf16[4,16,16,128]{3,2,1,0:T(8,128)(2,1)S(1)} %all_to_all.44), channel_id=3, replica_groups=mesh['dp'=4,'kv_0'=16,'kv_1'=4,'tp'=2] {'tp'}, dimensions={0}, use_global_device_ids=true | all-gather | bytes 786432 | tf_op jit(solution)/shard_map/all_gather | solution.py:345
  101.0 0.0 copy-done.4
  101.0 1.3 feed.1
  102.3 2.2 %all-gather.2 = bf16[128,2048]{1,0:T(8,128)(2,1)S(1)} all-gather(bf16[64,2048]{1,0:T(8,128)(2,1)S(1)} %get-tuple-element.13), channel_id=4, replica_groups=mesh['dp'=4,'kv_0'=16,'kv_1'=4,'tp'=2] {'tp'}, dimensions={0}, use_global_device_ids=true | all-gather | bytes 786432 | tf_op jit(solution)/shard_map/all_gather | solution.py:358
  104.5 0.1 pair_sum.1
  104.6 8.8 %all_to_all.45.x = bf16[4,16,2048]{2,1,0:T(8,128)(2,1)S(1)} all-to-all(bf16[4,16,2048]{2,1,0:T(8,128)(2,1)S(1)} %bitcast.18), channel_id=1, replica_groups=mesh['dp'=4,'kv_0'=16,'kv_1'=4,'tp'=2] {'kv_1'}, dimensions={0} | all-to-all | bytes 524288 | tf_op jit(solution)/shard_map/all_to_all | solution.py:360
  113.4 0.1 half_sum.1
  113.5 14.3 %all_to_all.46.x = bf16[16,16,128]{2,1,0:T(8,128)(2,1)S(1)} all-to-all(bf16[16,16,128]{2,1,0:T(8,128)(2,1)S(1)} %half_sum.1), channel_id=1, replica_groups=mesh['dp'=4,'kv_0'=16,'kv_1'=4,'tp'=2] {'kv_0'}, dimensions={0} | all-to-all | bytes 131072 | tf_op jit(solution)/shard_map/all_to_all | solution.py:368
  127.8 4.1 %all_gather.27.x = f32[32,128]{1,0:T(8,128)S(1)} all-gather(f32[16,128]{1,0:T(8,128)S(1)} %ffn_sum.1), channel_id=1, replica_groups=mesh['dp'=4,'kv_0'=16,'kv_1'=4,'tp'=2] {'tp'}, dimensions={0}, use_global_device_ids=true | all-gather | bytes 24576 | tf_op jit(solution)/shard_map/all_gather | solution.py:372
  131.9 0.0 copy-done.5
  131.9 0.2 final_norm.1
  132.1 17.4 %all_to_all.47 = f32[64,1,128]{2,1,0:T(1,128)S(1)} all-to-all(f32[64,1,128]{2,1,0:T(1,128)S(1)} %bitcast.23), channel_id=1, replica_groups=mesh['dp'=4,'kv_0'=16,'kv_1'=4,'tp'=2] {'kv_0','kv_1'}, dimensions={0} | all-to-all | bytes 65536 | tf_op jit(solution)/shard_map/all_to_all | solution.py:376
  149.6 0.7 place.1
  (10 shorter events, 0.1 us)
Async XLA Ops:
  19.1 31.4 %copy-start.3 = (f32[1,8,128,128]{3,2,1,0:T(8,128)S(1)}, f32[1,8,128,128]{3,2,1,0:T(8,128)}, u32[]{:S(2)}) copy-start(f32[1,8,128,128]{3,2,1,0:T(8,128)} %state.1) | copy-start | bytes 1572868
  73.2 27.8 %copy-start.2 = (bf16[86,4096]{1,0:T(8,128)(2,1)S(1)}, bf16[86,4096]{1,0:T(8,128)(2,1)}, u32[]{:S(2)}) copy-start(bf16[86,4096]{1,0:T(8,128)(2,1)} %wd.1) | copy-start | bytes 2113540
  73.7 27.4 %copy-start = (bf16[4096,86]{0,1:T(8,128)(2,1)S(1)}, bf16[4096,86]{0,1:T(8,128)(2,1)}, u32[]{:S(2)}) copy-start(bf16[4096,86]{0,1:T(8,128)(2,1)} %param.22) | copy-start | bytes 2113540
  73.7 27.4 %copy-start.1 = (bf16[4096,86]{0,1:T(8,128)(2,1)S(1)}, bf16[4096,86]{0,1:T(8,128)(2,1)}, u32[]{:S(2)}) copy-start(bf16[4096,86]{0,1:T(8,128)(2,1)} %param.23) | copy-start | bytes 2113540
  73.7 27.3 %copy-start.4 = (f32[4096]{0:T(1024)S(1)}, f32[4096]{0:T(1024)}, u32[]{:S(2)}) copy-start(f32[4096]{0:T(1024)} %param.21) | copy-start | bytes 49156
  104.5 27.4 %copy-start.5 = (f32[4096]{0:T(1024)S(1)}, f32[4096]{0:T(1024)}, u32[]{:S(2)}) copy-start(f32[4096]{0:T(1024)} %param.25) | copy-start | bytes 49156

commit v7 on v4

--- a/solution.py
+++ b/solution.py
@@ -8,6 +8,8 @@
 
 KV = ("kv_0", "kv_1")
 YZ = ("kv_1", "kv_0")
+Z_TP = ("kv_0", "tp")
+Y_TP = ("kv_1", "tp")
 KV_TP = ("kv_0", "kv_1", "tp")
 DP_KV = ("dp", "kv_0", "kv_1")
 F32 = jnp.float32
@@ -38,6 +40,33 @@
 
 def sds(shape, dtype):
     return jax.ShapeDtypeStruct(shape, dtype)
+
+
+def far_z(z):
+    return z // (NZ // 2)
+
+
+def far_y(y):
+    return y // (NY // 2)
+
+
+Z_GROUPS = [[z * 2 + (t ^ far_z(z)) for z in range(NZ)] for t in range(2)]
+Y_GROUPS = [[y * 2 + (t ^ far_y(y)) for y in range(NY)] for t in range(2)]
+ALL_GROUPS = [
+    [(z * NY + y) * 2 + (t ^ far_z(z)) for z in range(NZ) for y in range(NY)] for t in range(2)
+]
+
+
+def exchange(x, axes, groups):
+    return lax.all_to_all(x, axes, 0, 0, tiled=True, axis_index_groups=groups)
+
+
+def own_side():
+    return (far_z(lax.axis_index("kv_0")) + far_y(lax.axis_index("kv_1"))) % 2
+
+
+def own_half():
+    return (lax.axis_index("tp") + own_side()) % 2
 
 
 def rows_of(s):
@@ -149,7 +178,9 @@
 def feed_kernel(x, gain, wg_t, wu_t, wd, own, other, row, wide, narrow, stats):
     tps = x.shape[0]
     per = x.shape[3]
-    tp = lax.axis_index("tp")
+    side = own_side()
+    cores = (side, 1 - side)
+    tp = own_half()
     place = lax.axis_index("kv_1") * NZ + lax.axis_index("kv_0")
     groups = SEQS // per
     cols = LANES // groups
@@ -162,7 +193,9 @@
         sources = []
         for q in range(groups):
             kv = a * chips + q // tps
-            sources.append(x[q % tps, kv % NY, kv // NY].astype(F32))
+            y, z = kv % NY, kv // NY
+            core = cores[(q % tps) ^ far_y(y) ^ far_z(z)]
+            sources.append(x[core, y, z].astype(F32))
         for g in range(groups):
             tile = sources[(groups - g) % groups]
             for j in range(1, groups):
@@ -203,8 +236,7 @@
 
 def ffn_sum_kernel(x, hidden, out):
     per = x.shape[1]
-    tp = lax.axis_index("tp")
-    total = hidden[pl.ds(pl.multiple_of(tp * per, per), per), :]
+    total = hidden[pl.ds(pl.multiple_of(own_half() * per, per), per), :]
     for d in range(x.shape[0]):
         total += x[d].astype(F32)
     out[...] = total
@@ -215,7 +247,8 @@
 
 
 def final_norm_kernel(x, gain, out):
-    p = x[...]
+    side = own_side()
+    p = jnp.concatenate([x[side], x[1 - side]], axis=0)
     count = p.shape[0] * p.shape[1]
     mean = total_of(p) / count
     var = total_of(p * p) / count - mean * mean
@@ -319,9 +352,9 @@
         scratch=[pltpu.VMEM((2, SEQS, heads, dim), F32)],
         name="mix",
     )(gathered.reshape(2, SEQS, heads, dim), w_out.T, tokens)
-    rows = lax.all_to_all(mixed, "kv_0", 0, 0, tiled=True)
+    rows = exchange(mixed, Z_TP, Z_GROUPS)
     rows = jnp.broadcast_to(rows[None], (NY, *rows.shape))
-    rows = lax.all_to_all(rows, "kv_1", 0, 0, tiled=True)
+    rows = exchange(rows, Y_TP, Y_GROUPS)
     rows = lax.all_gather(rows, "tp", axis=0)
     lines = half // LANES
     own, other, hidden_row = kernel_call(
@@ -337,7 +370,7 @@
     )(rows, gain_mix[None, :], w_ffn_gate.T, w_ffn_up.T, w_ffn_down)
     both = lax.all_gather(other, "tp", axis=0)
     part = kernel_call(pair_sum_kernel, sds(own.shape, BF16), 2, name="pair_sum")(own, both)
-    part = lax.all_to_all(part.reshape(NY, NZ, half), "kv_1", 0, 0, tiled=True)
+    part = exchange(part.reshape(NY, NZ, half), Y_TP, Y_GROUPS)
     part = kernel_call(
         near_sum_kernel,
         sds((NZ, lines, LANES), BF16),
@@ -345,15 +378,15 @@
         scratch=[pltpu.VMEM((NZ, lines, LANES), F32)],
         name="half_sum",
     )(part)
-    part = lax.all_to_all(part, "kv_0", 0, 0, tiled=True)
+    part = exchange(part, Z_TP, Z_GROUPS)
     summed = kernel_call(ffn_sum_kernel, sds((lines, LANES), F32), 2, name="ffn_sum")(
         part, hidden_row.reshape(2 * lines, LANES)
     )
-    summed = lax.all_gather(summed, "tp", axis=0, tiled=True)
+    summed = lax.all_gather(summed, "tp", axis=0)
     spread = kernel_call(final_norm_kernel, sds((SEQS, LANES), F32), 2, name="final_norm")(
         summed, gain_out.reshape(2 * lines, LANES)
     )
-    spread = lax.all_to_all(spread.reshape(SEQS, 1, LANES), KV, 0, 0, tiled=True)
+    spread = exchange(spread.reshape(SEQS, 1, LANES), KV_TP, ALL_GROUPS)
     layer_out = kernel_call(place_kernel, sds((cols, SEQS), BF16), 1, name="place")(
         spread.reshape(SEQS, LANES)
     )

time: 151 us -> 153 us (1.013)
  blocking collectives: 141 us -> 143 us
    all_to_all x5, blocking collectives: 63.2 us -> 70.7 us  [exchange(): return lax.all_to_all(x, axes, 0, 0, tiled=True, axis_index_groups=groups)]
    all_gather x1, blocking collectives: 5.18 us -> 2.3 us  [on_device(): rows = lax.all_gather(rows, 'tp', axis=0)]
    all_gather x1, blocking collectives: 4.17 us -> 1.82 us  [on_device(): summed = lax.all_gather(summed, 'tp', axis=0)]
where the time goes in v7:
time: 153 us; the launch traced here: 152 us
  blocking collectives  143 us (93%)
  Pallas kernels  7.12 us (5%)
    all_to_all x5, blocking collectives, exchange(): return lax.all_to_all(x, axes, 0, 0, tiled=True, axis_index_groups=groups)  70.7 us
    all_to_all x1, blocking collectives, on_device(): far = lax.all_to_all(near, 'kv_0', 0, 0, tiled=True)  28.4 us
    all_to_all x1, blocking collectives, on_device(): gathered = lax.all_to_all(attended, YZ, 0, 0, tiled=True)  20.5 us
    all_to_all x1, blocking collectives, on_device(): near = lax.all_to_all(parts, 'kv_1', 0, 0, tiled=True)  11.9 us
    all_gather x1, blocking collectives, on_device(): gathered = lax.all_gather(gathered, 'tp', axis=0)  5.37 us

profile of v7, /device:TPU:1, one launch (start us, length us, event | category | flops | bytes accessed | tf_op | source)
XLA Modules:
  0.0 152.0 jit_solution(13460321382567188393)
XLA Ops:
  1.3 0.1 fusion.2
  1.3 0.1 fusion
  1.4 0.1 pad.5.clone
  1.5 0.1 pad.4.clone
  1.6 0.1 maximum_maximum_fusion.aux
  1.6 2.3 %project.1 = bf16[4,16,4096]{2,1,0:T(8,128)(2,1)} custom-call(bf16[64,64]{1,0:T(8,128)(2,1)} %tok.1, bf16[64,1024]{1,0:T(8,128)(2,1)} %wq.1, bf16[64,1024]{1,0:T(8,128)(2,1)} %wk.1, bf16[64,1024]{1,0:T(8,128)(2,1)} %wv.1, bf16[64,1024]{1,0:T(8,128)(2,1)} %wg.1), custom_call_target="tpu_custom_call" | custom-call | tf_op jit(solution)/shard_map/project/pallas_call | solution.py:311
  4.0 11.9 %all_to_all.40.x = bf16[4,16,4096]{2,1,0:T(8,128)(2,1)S(1)} all-to-all(bf16[4,16,4096]{2,1,0:T(8,128)(2,1)} %project.1), channel_id=1, replica_groups=mesh['dp'=4,'kv_0'=16,'kv_1'=4,'tp'=2] {'kv_1'}, dimensions={0} | all-to-all | bytes 1048576 | tf_op jit(solution)/shard_map/all_to_all | solution.py:326
  15.9 0.2 near_sum.1
  16.2 28.4 %all_to_all.41.x = bf16[16,32,128]{2,1,0:T(8,128)(2,1)S(1)} all-to-all(bf16[16,32,128]{2,1,0:T(8,128)(2,1)S(1)} %near_sum.1), channel_id=1, replica_groups=mesh['dp'=4,'kv_0'=16,'kv_1'=4,'tp'=2] {'kv_0'}, dimensions={0} | all-to-all | bytes 262144 | tf_op jit(solution)/shard_map/all_to_all | solution.py:334
  44.6 0.0 copy-done.3
  44.6 1.3 retention.1
  45.9 20.5 %all_to_all.42 = bf16[64,8,128]{2,1,0:T(8,128)(2,1)S(1)} all-to-all(bf16[64,8,128]{2,1,0:T(8,128)(2,1)S(1)} %get-tuple-element.11), channel_id=1, replica_groups=mesh['dp'=4,'kv_0'=16,'kv_1'=4,'tp'=2] {'kv_1','kv_0'}, dimensions={0} | all-to-all | bytes 262144 | tf_op jit(solution)/shard_map/all_to_all | solution.py:345
  66.3 5.4 %all-gather = bf16[128,8,128]{2,1,0:T(8,128)(2,1)S(1)} all-gather(bf16[64,8,128]{2,1,0:T(8,128)(2,1)S(1)} %all_to_all.42), channel_id=2, replica_groups=mesh['dp'=4,'kv_0'=16,'kv_1'=4,'tp'=2] {'tp'}, dimensions={0}, use_global_device_ids=true | all-gather | bytes 393216 | tf_op jit(solution)/shard_map/all_gather | solution.py:346
  71.7 0.0 copy-done.4
  71.7 0.0 copy-done.5
  71.7 0.7 mix.1
  72.4 16.1 %all_to_all.43 = bf16[16,16,128]{2,1,0:T(8,128)(2,1)S(1)} all-to-all(bf16[16,16,128]{2,1,0:T(8,128)(2,1)S(1)} %mix.1), channel_id=1, replica_groups={{0,8,16,24,32,40,48,56,65,73,81,89,97,105,113,121},{1,9,17,25,33,41,49,..., dimensions={0} | all-to-all | bytes 131072 | tf_op jit(solution)/shard_map/all_to_all | solution.py:61
  88.6 0.0 copy-start
  88.6 9.5 %all_to_all.44 = bf16[4,16,16,128]{3,2,1,0:T(8,128)(2,1)S(1)} all-to-all(bf16[4,16,16,128]{3,2,1,0:T(8,128)(2,1)S(1)} %broadcast_in_dim.10), channel_id=1, replica_groups={{0,2,5,7},{1,3,4,6},{8,10,13,15},{9,11,12,14},{16,18,21,23},{17,19,20,2..., dimensions={0} | all-to-all | bytes 524288 | tf_op jit(solution)/shard_map/all_to_all | solution.py:61
  98.1 2.3 %all-gather.1 = bf16[8,16,16,128]{3,2,1,0:T(8,128)(2,1)S(1)} all-gather(bf16[4,16,16,128]{3,2,1,0:T(8,128)(2,1)S(1)} %all_to_all.44), channel_id=3, replica_groups=mesh['dp'=4,'kv_0'=16,'kv_1'=4,'tp'=2] {'tp'}, dimensions={0}, use_global_device_ids=true | all-gather | bytes 786432 | tf_op jit(solution)/shard_map/all_gather | solution.py:358
  100.4 0.0 copy-done.2
  100.4 0.0 copy-done.1
  100.4 1.4 feed.1
  101.8 2.2 %all-gather.2 = bf16[128,2048]{1,0:T(8,128)(2,1)S(1)} all-gather(bf16[64,2048]{1,0:T(8,128)(2,1)S(1)} %get-tuple-element.13), channel_id=4, replica_groups=mesh['dp'=4,'kv_0'=16,'kv_1'=4,'tp'=2] {'tp'}, dimensions={0}, use_global_device_ids=true | all-gather | bytes 786432 | tf_op jit(solution)/shard_map/all_gather | solution.py:371
  104.0 0.1 pair_sum.1
  104.1 9.4 %all_to_all.45.x = bf16[4,16,2048]{2,1,0:T(8,128)(2,1)S(1)} all-to-all(bf16[4,16,2048]{2,1,0:T(8,128)(2,1)S(1)} %bitcast.20), channel_id=1, replica_groups={{0,2,5,7},{1,3,4,6},{8,10,13,15},{9,11,12,14},{16,18,21,23},{17,19,20,2..., dimensions={0} | all-to-all | bytes 524288 | tf_op jit(solution)/shard_map/all_to_all | solution.py:61
  113.5 0.1 half_sum.1
  113.6 16.6 %all_to_all.46.x = bf16[16,16,128]{2,1,0:T(8,128)(2,1)S(1)} all-to-all(bf16[16,16,128]{2,1,0:T(8,128)(2,1)S(1)} %half_sum.1), channel_id=1, replica_groups={{0,8,16,24,32,40,48,56,65,73,81,89,97,105,113,121},{1,9,17,25,33,41,49,..., dimensions={0} | all-to-all | bytes 131072 | tf_op jit(solution)/shard_map/all_to_all | solution.py:61
  130.2 1.8 %all-gather.3 = f32[32,128]{1,0:T(8,128)S(1)} all-gather(f32[16,128]{1,0:T(8,128)S(1)} %ffn_sum.1), channel_id=5, replica_groups=mesh['dp'=4,'kv_0'=16,'kv_1'=4,'tp'=2] {'tp'}, dimensions={0}, use_global_device_ids=true | all-gather | bytes 24576 | tf_op jit(solution)/shard_map/all_gather | solution.py:385
  132.1 0.2 final_norm.1
  132.3 19.0 %all_to_all.47 = f32[64,1,128]{2,1,0:T(1,128)S(1)} all-to-all(f32[64,1,128]{2,1,0:T(1,128)S(1)} %bitcast.24), channel_id=1, replica_groups={{0,2,4,6,8,10,12,14,16,18,20,22,24,26,28,30,32,34,36,38,40,42,44,46,48,..., dimensions={0} | all-to-all | bytes 65536 | tf_op jit(solution)/shard_map/all_to_all | solution.py:61
  151.3 0.7 place.1
  (14 shorter events, 0.1 us)
Async XLA Ops:
  15.9 28.6 %copy-start.3 = (f32[1,8,128,128]{3,2,1,0:T(8,128)S(1)}, f32[1,8,128,128]{3,2,1,0:T(8,128)}, u32[]{:S(2)}) copy-start(f32[1,8,128,128]{3,2,1,0:T(8,128)} %state.1) | copy-start | bytes 1572868
  66.3 5.4 %copy-start.4 = (bf16[2048,32]{0,1:T(8,128)(2,1)S(1)}, bf16[2048,32]{0,1:T(8,128)(2,1)}, u32[]{:S(2)}) copy-start(bf16[2048,32]{0,1:T(8,128)(2,1)} %param.20) | copy-start | bytes 393220
  66.3 5.4 %copy-start.5 = (bf16[64,64]{1,0:T(8,128)(2,1)S(1)}, bf16[64,64]{1,0:T(8,128)(2,1)}, u32[]{:S(2)}) copy-start(bf16[64,64]{1,0:T(8,128)(2,1)} %tok.1) | copy-start | bytes 24580
  71.7 28.7 %copy-start.2 = (bf16[86,4096]{1,0:T(8,128)(2,1)S(1)}, bf16[86,4096]{1,0:T(8,128)(2,1)}, u32[]{:S(2)}) copy-start(bf16[86,4096]{1,0:T(8,128)(2,1)} %wd.1) | copy-start | bytes 2113540
  88.5 11.9 %copy-start.1 = (bf16[4096,86]{0,1:T(8,128)(2,1)S(1)}, bf16[4096,86]{0,1:T(8,128)(2,1)}, u32[]{:S(2)}) copy-start(bf16[4096,86]{0,1:T(8,128)(2,1)} %param.23) | copy-start | bytes 2113540
  88.6 11.9 %copy-start = (bf16[4096,86]{0,1:T(8,128)(2,1)S(1)}, bf16[4096,86]{0,1:T(8,128)(2,1)}, u32[]{:S(2)}) copy-start(bf16[4096,86]{0,1:T(8,128)(2,1)} %param.22) | copy-start | bytes 2113540
  98.1 2.3 %copy-start.6 = (f32[4096]{0:T(1024)S(1)}, f32[4096]{0:T(1024)}, u32[]{:S(2)}) copy-start(f32[4096]{0:T(1024)} %param.21) | copy-start | bytes 49156
  130.2 1.8 %copy-start.7 = (f32[4096]{0:T(1024)S(1)}, f32[4096]{0:T(1024)}, u32[]{:S(2)}) copy-start(f32[4096]{0:T(1024)} %param.25) | copy-start | bytes 49156

commit v8 on v4

--- a/solution.py
+++ b/solution.py
@@ -1,3 +1,5 @@
+import math
+
 import jax
 import jax.numpy as jnp
 from jax import lax
@@ -40,6 +42,15 @@
     return jax.ShapeDtypeStruct(shape, dtype)
 
 
+def far_z(z):
+    return z // (NZ // 2)
+
+
+ALL_GROUPS = [
+    [(z * NY + y) * 2 + (t ^ far_z(z)) for z in range(NZ) for y in range(NY)] for t in range(2)
+]
+
+
 def rows_of(s):
     return (s % NY) * NZ + s // NY
 
@@ -54,7 +65,9 @@
     return lax.dot_general(a, b, (((ca,), (cb,)), ((), ())), preferred_element_type=F32)
 
 
-def project_kernel(tok_hbm, wq, wk, wv, wg, out_hbm, tok, weights, out, sems, out_sems):
+def project_kernel(
+    tok_hbm, position_hbm, wq, wk, wv, wg, out_hbm, turns, tok, position, weights, out, sems, out_sems
+):
     sources = (wq, wk, wv, wg)
     count = len(sources)
     width = weights.shape[2]
@@ -63,6 +76,16 @@
         copies.append(pltpu.make_async_copy(w, weights.at[i], sems.at[i]))
     for copy in copies:
         copy.start()
+    where = pltpu.make_async_copy(position_hbm, position, sems.at[count + 1])
+    where.start()
+    where.wait()
+    dim = turns.shape[1]
+    lane = lax.broadcasted_iota(jnp.int32, (1, dim), 1)
+    power = (lane % (dim // 2)).astype(F32) / (dim // 2)
+    angle = position[0].astype(F32) * jnp.exp(power * -math.log(10000.0))
+    turns[0:1, :] = jnp.cos(angle)
+    sine = jnp.sin(angle)
+    turns[1:2, :] = jnp.where(lane < dim // 2, -sine, sine)
     copies[0].wait()
     rows = mm(perm_matrix(BF16), tok[...], 1, 0).astype(BF16)
     sends = []
@@ -86,13 +109,15 @@
     out[...] = wide[...].astype(BF16)
 
 
-def retention_kernel(x, aux, state, state_out, out, new_state, sems):
+def retention_kernel(x, turns, state, new_state, out):
     heads, dim = state.shape[1], state.shape[2]
+    cosine = turns[0:1, :]
+    sine = turns[1:2, :]
+    line = lax.broadcasted_iota(jnp.int32, (heads, dim), 0) + lax.axis_index("tp") * heads
+    decay = 1.0 - jnp.exp2(-5.0 - 6.0 * line.astype(F32) / (2 * heads - 1))
     total = x[0].astype(F32)
     for z in range(1, NZ):
         total += x[z].astype(F32)
-    cosine = aux[0:1, :]
-    sine = aux[1:2, :]
     query = total[0:heads]
     key = total[heads : 2 * heads]
     value = total[2 * heads : 3 * heads]
@@ -102,12 +127,9 @@
     query_t = query.T
     key_t = key.T
     lines = []
-    sends = []
     for h in range(heads):
-        updated = aux[8 + h : 9 + h, :] * state[0, h] + key_t[:, h : h + 1] * value[h : h + 1, :]
-        new_state[h] = updated
-        sends.append(pltpu.make_async_copy(new_state.at[h], state_out.at[0, h], sems.at[h]))
-        sends[h].start()
+        updated = decay[h : h + 1, :] * state[0, h] + key_t[:, h : h + 1] * value[h : h + 1, :]
+        new_state[0, h] = updated
         lines.append(jnp.sum(query_t[:, h : h + 1] * updated, axis=0, keepdims=True))
     retained = jnp.concatenate(lines, axis=0)
     mean = jnp.mean(retained, -1, keepdims=True)
@@ -116,8 +138,6 @@
     silu = gate / (1.0 + jnp.exp(-gate))
     attended = (normed * silu).astype(BF16)
     out[...] = jnp.broadcast_to(attended[None], out.shape)
-    for send in sends:
-        send.wait()
 
 
 def mix_kernel(x, w_t, tok, out, wide):
@@ -146,7 +166,11 @@
     out[...] = jnp.broadcast_to(packed.astype(BF16)[None], out.shape)
 
 
-def feed_kernel(x, gain, wg_t, wu_t, wd, own, other, row, wide, narrow, stats):
+def feed_kernel(
+    x, gain, wg_t, wu_t, wd, state, own, other, row, state_out, wide, narrow, stats, sem
+):
+    keep = pltpu.make_async_copy(state, state_out, sem)
+    keep.start()
     tps = x.shape[0]
     per = x.shape[3]
     tp = lax.axis_index("tp")
@@ -194,6 +218,7 @@
         theirs = pl.multiple_of((1 - tp) * half + c, step)
         own[:, c : c + step] = mm(inner, wd[:, pl.ds(mine, step)], 1, 0).astype(BF16)
         other[:, c : c + step] = mm(inner, wd[:, pl.ds(theirs, step)], 1, 0).astype(BF16)
+    keep.wait()
 
 
 def pair_sum_kernel(own, both, out):
@@ -258,38 +283,22 @@
     half = width // 2
     tp = lax.axis_index("tp")
 
-    inverse = 10000.0 ** (-jnp.arange(dim // 2, dtype=F32) / (dim // 2))
-    angle = positions.astype(F32)[:, None] * inverse[None, :]
-    cosine = jnp.cos(angle)
-    sine = jnp.sin(angle)
-    head_ids = (tp * heads + jnp.arange(heads, dtype=jnp.int32)).astype(F32)
-    decay = 1.0 - 2.0 ** (-5.0 - 6.0 * head_ids / (2 * heads - 1))
-    aux = jnp.concatenate(
-        [
-            jnp.concatenate([cosine, cosine], 1),
-            jnp.concatenate([-sine, sine], 1),
-            jnp.zeros((6, dim), F32),
-            jnp.broadcast_to(decay[:, None], (heads, dim)),
-        ],
-        0,
-    )
-
-    tokens_in, aux = lax.optimization_barrier((tokens, aux))
-    parts = pl.pallas_call(
+    parts, turns = pl.pallas_call(
         project_kernel,
-        out_shape=sds((NY, NZ, proj * dim), BF16),
-        in_specs=[pl.BlockSpec(memory_space=pl.ANY)] * 5,
-        out_specs=pl.BlockSpec(memory_space=pl.ANY),
+        out_shape=[sds((NY, NZ, proj * dim), BF16), sds((2, dim), F32)],
+        in_specs=[pl.BlockSpec(memory_space=pl.ANY)] * 6,
+        out_specs=[pl.BlockSpec(memory_space=pl.ANY), VMEM],
         scratch_shapes=[
             pltpu.VMEM(tokens.shape, BF16),
+            pltpu.SMEM((1,), jnp.int32),
             pltpu.VMEM((4, *w_query.shape), BF16),
             pltpu.VMEM((4, NY, NZ, w_query.shape[1]), BF16),
-            pltpu.SemaphoreType.DMA((5,)),
+            pltpu.SemaphoreType.DMA((6,)),
             pltpu.SemaphoreType.DMA((4,)),
         ],
         interpret=INTERPRET,
         name="project",
-    )(tokens_in, w_query, w_key, w_value, w_gate)
+    )(tokens, positions, w_query, w_key, w_value, w_gate)
     near = lax.all_to_all(parts, "kv_1", 0, 0, tiled=True)
     near = kernel_call(
         near_sum_kernel,
@@ -299,16 +308,12 @@
         name="near_sum",
     )(near)
     far = lax.all_to_all(near, "kv_0", 0, 0, tiled=True)
-    new_state, attended = pl.pallas_call(
+    updated, attended = kernel_call(
         retention_kernel,
-        out_shape=[sds(state.shape, F32), sds((SEQS, heads, dim), BF16)],
-        in_specs=[VMEM] * 3,
-        out_specs=[pl.BlockSpec(memory_space=pl.ANY), VMEM],
-        scratch_shapes=[pltpu.VMEM(state.shape[1:], F32), pltpu.SemaphoreType.DMA((heads,))],
-        compiler_params=PARAMS,
-        interpret=INTERPRET,
+        [sds(state.shape, F32), sds((SEQS, heads, dim), BF16)],
+        3,
         name="retention",
-    )(far, aux, state)
+    )(far, turns, state)
     gathered = lax.all_to_all(attended, YZ, 0, 0, tiled=True)
     gathered = lax.all_gather(gathered, "tp", axis=0)
     per = SEQS * cols // LANES
@@ -324,17 +329,26 @@
     rows = lax.all_to_all(rows, "kv_1", 0, 0, tiled=True)
     rows = lax.all_gather(rows, "tp", axis=0)
     lines = half // LANES
-    own, other, hidden_row = kernel_call(
+    own, other, hidden_row, new_state = pl.pallas_call(
         feed_kernel,
-        [sds((SEQS, half), BF16)] * 2 + [sds((1, width), F32)],
-        5,
-        scratch=[
+        out_shape=[
+            sds((SEQS, half), BF16),
+            sds((SEQS, half), BF16),
+            sds((1, width), F32),
+            sds(state.shape, F32),
+        ],
+        in_specs=[VMEM] * 6,
+        out_specs=[VMEM] * 3 + [pl.BlockSpec(memory_space=pl.ANY)],
+        scratch_shapes=[
             pltpu.VMEM((SEQS, width), F32),
             pltpu.VMEM((SEQS, width), BF16),
             pltpu.VMEM((2, SEQS, LANES), F32),
+            pltpu.SemaphoreType.DMA,
         ],
+        compiler_params=PARAMS,
+        interpret=INTERPRET,
         name="feed",
-    )(rows, gain_mix[None, :], w_ffn_gate.T, w_ffn_up.T, w_ffn_down)
+    )(rows, gain_mix[None, :], w_ffn_gate.T, w_ffn_up.T, w_ffn_down, updated)
     both = lax.all_gather(other, "tp", axis=0)
     part = kernel_call(pair_sum_kernel, sds(own.shape, BF16), 2, name="pair_sum")(own, both)
     part = lax.all_to_all(part.reshape(NY, NZ, half), "kv_1", 0, 0, tiled=True)
@@ -353,7 +367,9 @@
     spread = kernel_call(final_norm_kernel, sds((SEQS, LANES), F32), 2, name="final_norm")(
         summed, gain_out.reshape(2 * lines, LANES)
     )
-    spread = lax.all_to_all(spread.reshape(SEQS, 1, LANES), KV, 0, 0, tiled=True)
+    spread = lax.all_to_all(
+        spread.reshape(SEQS, 1, LANES), KV_TP, 0, 0, tiled=True, axis_index_groups=ALL_GROUPS
+    )
     layer_out = kernel_call(place_kernel, sds((cols, SEQS), BF16), 1, name="place")(
         spread.reshape(SEQS, LANES)
     )

time: 151 us -> 152 us (level)
  no operation moved by 1% of the time
where the time goes in v8:
time: 152 us; the launch traced here: 151 us
  blocking collectives  142 us (93%)
  Pallas kernels  7.44 us (5%)
    all_to_all x1, blocking collectives, on_device(): far = lax.all_to_all(near, 'kv_0', 0, 0, tiled=True)  28.4 us
    all_to_all x1, blocking collectives, on_device(): gathered = lax.all_to_all(attended, YZ, 0, 0, tiled=True)  20.5 us
    all_to_all x1, blocking collectives, on_device(): lax.all_to_all(spread.reshape(SEQS, 1, LANES), KV_TP, 0, 0, tiled=True, a...  18.2 us
    all_to_all x1, blocking collectives, on_device(): rows = lax.all_to_all(mixed, 'kv_0', 0, 0, tiled=True)  14.7 us
    all_to_all x1, blocking collectives, on_device(): part = lax.all_to_all(part, 'kv_0', 0, 0, tiled=True)  14.3 us
    all_to_all x1, blocking collectives, on_device(): near = lax.all_to_all(parts, 'kv_1', 0, 0, tiled=True)  11.9 us
    all_to_all x1, blocking collectives, on_device(): part = lax.all_to_all(part.reshape(NY, NZ, half), 'kv_1', 0, 0, tiled=True)  8.78 us
    all_to_all x1, blocking collectives, on_device(): rows = lax.all_to_all(rows, 'kv_1', 0, 0, tiled=True)  8.05 us

profile of v8, /device:TPU:1, one launch (start us, length us, event | category | flops | bytes accessed | tf_op | source)
XLA Modules:
  0.0 151.3 jit_solution(934624060994715864)
XLA Ops:
  1.3 2.9 %project.1 = (bf16[4,16,4096]{2,1,0:T(8,128)(2,1)}, f32[2,128]{1,0:T(2,128)}) custom-call(bf16[64,64]{1,0:T(8,128)(2,1)} %tok.1, s32[1]{0:T(128)S(6)} %copy.16.position_hbm, bf16[64,1024]{1,0:T(8,128)(2,1)} %wq.1, bf16[64,1024]{1,0:T(8,128)(2,1)} %wk.1, bf16[64,1024]{1,0:T(8,128)(2,1)} %wv.1, bf16[64,1024]{1,0:T(8,128)(2,1)} %wg.1), custom_call_target="tpu_custom_call" | custom-call | tf_op jit(solution)/shard_map/project/pallas_call | solution.py:286
  4.2 11.9 %all_to_all.40.x = bf16[4,16,4096]{2,1,0:T(8,128)(2,1)S(1)} all-to-all(bf16[4,16,4096]{2,1,0:T(8,128)(2,1)} %get-tuple-element.10), channel_id=1, replica_groups=mesh['dp'=4,'kv_0'=16,'kv_1'=4,'tp'=2] {'kv_1'}, dimensions={0} | all-to-all | bytes 1048576 | tf_op jit(solution)/shard_map/all_to_all | solution.py:302
  16.1 0.0 copy-start.3
  16.1 0.2 near_sum.1
  16.4 28.4 %all_to_all.41.x = bf16[16,32,128]{2,1,0:T(8,128)(2,1)S(1)} all-to-all(bf16[16,32,128]{2,1,0:T(8,128)(2,1)S(1)} %near_sum.1), channel_id=1, replica_groups=mesh['dp'=4,'kv_0'=16,'kv_1'=4,'tp'=2] {'kv_0'}, dimensions={0} | all-to-all | bytes 262144 | tf_op jit(solution)/shard_map/all_to_all | solution.py:310
  44.8 0.0 copy-done.3
  44.8 0.7 copy-done.8
  45.4 0.8 retention.1
  46.2 20.5 %all_to_all.42 = bf16[64,8,128]{2,1,0:T(8,128)(2,1)S(1)} all-to-all(bf16[64,8,128]{2,1,0:T(8,128)(2,1)S(1)} %get-tuple-element.12), channel_id=1, replica_groups=mesh['dp'=4,'kv_0'=16,'kv_1'=4,'tp'=2] {'kv_1','kv_0'}, dimensions={0} | all-to-all | bytes 262144 | tf_op jit(solution)/shard_map/all_to_all | solution.py:317
  66.7 5.4 %all-gather = bf16[128,8,128]{2,1,0:T(8,128)(2,1)S(1)} all-gather(bf16[64,8,128]{2,1,0:T(8,128)(2,1)S(1)} %all_to_all.42), channel_id=2, replica_groups=mesh['dp'=4,'kv_0'=16,'kv_1'=4,'tp'=2] {'tp'}, dimensions={0}, use_global_device_ids=true | all-gather | bytes 393216 | tf_op jit(solution)/shard_map/all_gather | solution.py:318
  72.0 0.0 copy-done.4
  72.1 0.0 copy-done.5
  72.1 0.7 mix.1
  72.7 14.7 %all_to_all.43 = bf16[16,16,128]{2,1,0:T(8,128)(2,1)S(1)} all-to-all(bf16[16,16,128]{2,1,0:T(8,128)(2,1)S(1)} %mix.1), channel_id=1, replica_groups=mesh['dp'=4,'kv_0'=16,'kv_1'=4,'tp'=2] {'kv_0'}, dimensions={0} | all-to-all | bytes 131072 | tf_op jit(solution)/shard_map/all_to_all | solution.py:327
  87.5 0.0 copy-start
  87.5 8.0 %all_to_all.44 = bf16[4,16,16,128]{3,2,1,0:T(8,128)(2,1)S(1)} all-to-all(bf16[4,16,16,128]{3,2,1,0:T(8,128)(2,1)S(1)} %broadcast_in_dim.4), channel_id=1, replica_groups=mesh['dp'=4,'kv_0'=16,'kv_1'=4,'tp'=2] {'kv_1'}, dimensions={0} | all-to-all | bytes 524288 | tf_op jit(solution)/shard_map/all_to_all | solution.py:329
  95.6 5.2 %all-gather.1 = bf16[8,16,16,128]{3,2,1,0:T(8,128)(2,1)S(1)} all-gather(bf16[4,16,16,128]{3,2,1,0:T(8,128)(2,1)S(1)} %all_to_all.44), channel_id=3, replica_groups=mesh['dp'=4,'kv_0'=16,'kv_1'=4,'tp'=2] {'tp'}, dimensions={0}, use_global_device_ids=true | all-gather | bytes 786432 | tf_op jit(solution)/shard_map/all_gather | solution.py:330
  100.8 0.0 copy-done.2
  100.8 0.0 copy-done.1
  100.8 0.0 copy-done
  100.8 0.0 copy-done.6
  100.8 1.7 %feed.1 = (bf16[64,2048]{1,0:T(8,128)(2,1)S(1)}, bf16[64,2048]{1,0:T(8,128)(2,1)S(1)}, f32[1,4096]{1,0:T(1,128)S(1)}, f32[1,8,128,128]{3,2,1,0:T(8,128)}) custom-call(bf16[2,4,16,16,128]{4,3,2,1,0:T(8,128)(2,1)S(1)} %bitcast.15, f32[1,4096]{1,0:T(1,128)S(1)} %bitcast.24, bf16[86,4096]{1,0:T(8,128)(2,1)S(1)} %bitcast.19, bf16[86,4096]{1,0:T(8,128)(2,1)S(1)} %bitcast.20, ...), custom_call_target="tpu_custom_call" | custom-call | tf_op jit(solution)/shard_map/feed/pallas_call | solution.py:332
  102.5 2.2 %all-gather.2 = bf16[128,2048]{1,0:T(8,128)(2,1)S(1)} all-gather(bf16[64,2048]{1,0:T(8,128)(2,1)S(1)} %get-tuple-element.15), channel_id=4, replica_groups=mesh['dp'=4,'kv_0'=16,'kv_1'=4,'tp'=2] {'tp'}, dimensions={0}, use_global_device_ids=true | all-gather | bytes 786432 | tf_op jit(solution)/shard_map/all_gather | solution.py:352
  104.7 0.1 pair_sum.1
  104.8 8.8 %all_to_all.45.x = bf16[4,16,2048]{2,1,0:T(8,128)(2,1)S(1)} all-to-all(bf16[4,16,2048]{2,1,0:T(8,128)(2,1)S(1)} %bitcast.18), channel_id=1, replica_groups=mesh['dp'=4,'kv_0'=16,'kv_1'=4,'tp'=2] {'kv_1'}, dimensions={0} | all-to-all | bytes 524288 | tf_op jit(solution)/shard_map/all_to_all | solution.py:354
  113.5 0.1 half_sum.1
  113.6 14.3 %all_to_all.46.x = bf16[16,16,128]{2,1,0:T(8,128)(2,1)S(1)} all-to-all(bf16[16,16,128]{2,1,0:T(8,128)(2,1)S(1)} %half_sum.1), channel_id=1, replica_groups=mesh['dp'=4,'kv_0'=16,'kv_1'=4,'tp'=2] {'kv_0'}, dimensions={0} | all-to-all | bytes 131072 | tf_op jit(solution)/shard_map/all_to_all | solution.py:362
  128.0 4.2 %all_gather.27.x = f32[32,128]{1,0:T(8,128)S(1)} all-gather(f32[16,128]{1,0:T(8,128)S(1)} %ffn_sum.1), channel_id=1, replica_groups=mesh['dp'=4,'kv_0'=16,'kv_1'=4,'tp'=2] {'tp'}, dimensions={0}, use_global_device_ids=true | all-gather | bytes 24576 | tf_op jit(solution)/shard_map/all_gather | solution.py:366
  132.1 0.0 copy-done.7
  132.1 0.2 final_norm.1
  132.3 18.2 %all_to_all.47 = f32[64,1,128]{2,1,0:T(1,128)S(1)} all-to-all(f32[64,1,128]{2,1,0:T(1,128)S(1)} %bitcast.22), channel_id=1, replica_groups={{0,2,4,6,8,10,12,14,16,18,20,22,24,26,28,30,32,34,36,38,40,42,44,46,48,..., dimensions={0} | all-to-all | bytes 65536 | tf_op jit(solution)/shard_map/all_to_all | solution.py:370
  150.6 0.7 place.1
  (9 shorter events, 0.1 us)
Async XLA Ops:
  16.1 28.6 %copy-start.3 = (f32[1,8,128,128]{3,2,1,0:T(8,128)S(1)}, f32[1,8,128,128]{3,2,1,0:T(8,128)}, u32[]{:S(2)}) copy-start(f32[1,8,128,128]{3,2,1,0:T(8,128)} %state.1) | copy-start | bytes 1572868
  44.8 0.7 copy-start.8
  66.7 5.4 %copy-start.4 = (bf16[2048,32]{0,1:T(8,128)(2,1)S(1)}, bf16[2048,32]{0,1:T(8,128)(2,1)}, u32[]{:S(2)}) copy-start(bf16[2048,32]{0,1:T(8,128)(2,1)} %param.20) | copy-start | bytes 393220
  66.7 5.4 %copy-start.5 = (bf16[64,64]{1,0:T(8,128)(2,1)S(1)}, bf16[64,64]{1,0:T(8,128)(2,1)}, u32[]{:S(2)}) copy-start(bf16[64,64]{1,0:T(8,128)(2,1)} %tok.1) | copy-start | bytes 24580
  72.1 28.7 %copy-start.2 = (bf16[86,4096]{1,0:T(8,128)(2,1)S(1)}, bf16[86,4096]{1,0:T(8,128)(2,1)}, u32[]{:S(2)}) copy-start(bf16[86,4096]{1,0:T(8,128)(2,1)} %wd.1) | copy-start | bytes 2113540
  87.5 13.3 %copy-start.1 = (bf16[4096,86]{0,1:T(8,128)(2,1)S(1)}, bf16[4096,86]{0,1:T(8,128)(2,1)}, u32[]{:S(2)}) copy-start(bf16[4096,86]{0,1:T(8,128)(2,1)} %param.23) | copy-start | bytes 2113540
  87.5 13.2 %copy-start = (bf16[4096,86]{0,1:T(8,128)(2,1)S(1)}, bf16[4096,86]{0,1:T(8,128)(2,1)}, u32[]{:S(2)}) copy-start(bf16[4096,86]{0,1:T(8,128)(2,1)} %param.22) | copy-start | bytes 2113540
  95.6 5.2 %copy-start.6 = (f32[4096]{0:T(1024)S(1)}, f32[4096]{0:T(1024)}, u32[]{:S(2)}) copy-start(f32[4096]{0:T(1024)} %param.21) | copy-start | bytes 49156
  127.9 4.2 %copy-start.7 = (f32[4096]{0:T(1024)S(1)}, f32[4096]{0:T(1024)}, u32[]{:S(2)}) copy-start(f32[4096]{0:T(1024)} %param.25) | copy-start | bytes 49156

commit v9 on v8

--- a/solution.py
+++ b/solution.py
@@ -38,6 +38,10 @@
     )
 
 
+def in_hbm(x):
+    return pltpu.with_memory_space_constraint(x, pltpu.HBM)
+
+
 def sds(shape, dtype):
     return jax.ShapeDtypeStruct(shape, dtype)
 
@@ -65,9 +69,7 @@
     return lax.dot_general(a, b, (((ca,), (cb,)), ((), ())), preferred_element_type=F32)
 
 
-def project_kernel(
-    tok_hbm, position_hbm, wq, wk, wv, wg, out_hbm, turns, tok, position, weights, out, sems, out_sems
-):
+def project_kernel(position, tok_hbm, wq, wk, wv, wg, out, tok, weights, sems):
     sources = (wq, wk, wv, wg)
     count = len(sources)
     width = weights.shape[2]
@@ -76,27 +78,12 @@
         copies.append(pltpu.make_async_copy(w, weights.at[i], sems.at[i]))
     for copy in copies:
         copy.start()
-    where = pltpu.make_async_copy(position_hbm, position, sems.at[count + 1])
-    where.start()
-    where.wait()
-    dim = turns.shape[1]
-    lane = lax.broadcasted_iota(jnp.int32, (1, dim), 1)
-    power = (lane % (dim // 2)).astype(F32) / (dim // 2)
-    angle = position[0].astype(F32) * jnp.exp(power * -math.log(10000.0))
-    turns[0:1, :] = jnp.cos(angle)
-    sine = jnp.sin(angle)
-    turns[1:2, :] = jnp.where(lane < dim // 2, -sine, sine)
     copies[0].wait()
     rows = mm(perm_matrix(BF16), tok[...], 1, 0).astype(BF16)
-    sends = []
     for i in range(count):
         copies[1 + i].wait()
-        out[i] = mm(rows, weights[i], 1, 0).astype(BF16).reshape(NY, NZ, width)
-        cols = pl.ds(i * width, width)
-        sends.append(pltpu.make_async_copy(out.at[i], out_hbm.at[:, :, cols], out_sems.at[i]))
-        sends[i].start()
-    for send in sends:
-        send.wait()
+        part = mm(rows, weights[i], 1, 0).astype(BF16)
+        out[:, :, i * width : (i + 1) * width] = part.reshape(NY, NZ, width)
 
 
 def near_sum_kernel(x, out, wide):
@@ -107,6 +94,17 @@
             total += x[y, :, cols].astype(F32)
         wide[:, c, :] = total
     out[...] = wide[...].astype(BF16)
+
+
+def first_sum_kernel(position, x, out, turns, wide):
+    dim = turns.shape[1]
+    lane = lax.broadcasted_iota(jnp.int32, (1, dim), 1)
+    power = (lane % (dim // 2)).astype(F32) / (dim // 2)
+    angle = position[0].astype(F32) * jnp.exp(power * -math.log(10000.0))
+    turns[0:1, :] = jnp.cos(angle)
+    sine = jnp.sin(angle)
+    turns[1:2, :] = jnp.where(lane < dim // 2, -sine, sine)
+    near_sum_kernel(x, out, wide)
 
 
 def retention_kernel(x, turns, state, new_state, out):
@@ -283,30 +281,32 @@
     half = width // 2
     tp = lax.axis_index("tp")
 
-    parts, turns = pl.pallas_call(
+    smem = pl.BlockSpec(memory_space=pltpu.SMEM)
+    parts = pl.pallas_call(
         project_kernel,
-        out_shape=[sds((NY, NZ, proj * dim), BF16), sds((2, dim), F32)],
-        in_specs=[pl.BlockSpec(memory_space=pl.ANY)] * 6,
-        out_specs=[pl.BlockSpec(memory_space=pl.ANY), VMEM],
+        out_shape=sds((NY, NZ, proj * dim), BF16),
+        in_specs=[smem] + [pl.BlockSpec(memory_space=pl.ANY)] * 5,
+        out_specs=VMEM,
         scratch_shapes=[
             pltpu.VMEM(tokens.shape, BF16),
-            pltpu.SMEM((1,), jnp.int32),
             pltpu.VMEM((4, *w_query.shape), BF16),
-            pltpu.VMEM((4, NY, NZ, w_query.shape[1]), BF16),
-            pltpu.SemaphoreType.DMA((6,)),
-            pltpu.SemaphoreType.DMA((4,)),
+            pltpu.SemaphoreType.DMA((5,)),
         ],
+        compiler_params=PARAMS,
         interpret=INTERPRET,
         name="project",
-    )(tokens, positions, w_query, w_key, w_value, w_gate)
+    )(positions, *map(in_hbm, (tokens, w_query, w_key, w_value, w_gate)))
     near = lax.all_to_all(parts, "kv_1", 0, 0, tiled=True)
-    near = kernel_call(
-        near_sum_kernel,
-        sds((NZ, proj, dim), BF16),
-        1,
-        scratch=[pltpu.VMEM((NZ, proj, dim), F32)],
+    near, turns = pl.pallas_call(
+        first_sum_kernel,
+        out_shape=[sds((NZ, proj, dim), BF16), sds((2, dim), F32)],
+        in_specs=[smem, VMEM],
+        out_specs=[VMEM, VMEM],
+        scratch_shapes=[pltpu.VMEM((NZ, proj, dim), F32)],
+        compiler_params=PARAMS,
+        interpret=INTERPRET,
         name="near_sum",
-    )(near)
+    )(positions, near)
     far = lax.all_to_all(near, "kv_0", 0, 0, tiled=True)
     updated, attended = kernel_call(
         retention_kernel,

time: 152 us -> 150 us (0.987)
  no operation moved by 1% of the time
where the time goes in v9:
time: 150 us; the launch traced here: 149 us
  blocking collectives  142 us (95%)
  Pallas kernels  6.19 us (4%)
    all_to_all x1, blocking collectives, on_device(): far = lax.all_to_all(near, 'kv_0', 0, 0, tiled=True)  28.4 us
    all_to_all x1, blocking collectives, on_device(): gathered = lax.all_to_all(attended, YZ, 0, 0, tiled=True)  20.5 us
    all_to_all x1, blocking collectives, on_device(): lax.all_to_all(spread.reshape(SEQS, 1, LANES), KV_TP, 0, 0, tiled=True, a...  18.2 us
    all_to_all x1, blocking collectives, on_device(): rows = lax.all_to_all(mixed, 'kv_0', 0, 0, tiled=True)  14.7 us
    all_to_all x1, blocking collectives, on_device(): part = lax.all_to_all(part, 'kv_0', 0, 0, tiled=True)  14.3 us
    all_to_all x1, blocking collectives, on_device(): near = lax.all_to_all(parts, 'kv_1', 0, 0, tiled=True)  11.7 us
    all_to_all x1, blocking collectives, on_device(): part = lax.all_to_all(part.reshape(NY, NZ, half), 'kv_1', 0, 0, tiled=True)  8.78 us
    all_to_all x1, blocking collectives, on_device(): rows = lax.all_to_all(rows, 'kv_1', 0, 0, tiled=True)  8.05 us

profile of v9, /device:TPU:1, one launch (start us, length us, event | category | flops | bytes accessed | tf_op | source)
XLA Modules:
  0.0 149.2 jit_solution(1499495323857144294)
XLA Ops:
  1.3 1.6 %project.1 = bf16[4,16,4096]{2,1,0:T(8,128)(2,1)S(1)} custom-call(s32[1]{0:T(128)S(6)} %copy.16.position, bf16[64,64]{1,0:T(8,128)(2,1)} %tok.1, bf16[64,1024]{1,0:T(8,128)(2,1)} %wq.1, bf16[64,1024]{1,0:T(8,128)(2,1)} %wk.1, bf16[64,1024]{1,0:T(8,128)(2,1)} %wv.1, bf16[64,1024]{1,0:T(8,128)(2,1)} %wg.1), custom_call_target="tpu_custom_call" | custom-call | tf_op jit(solution)/shard_map/project/pallas_call | solution.py:285
  2.9 11.7 %all_to_all.40.x = bf16[4,16,4096]{2,1,0:T(8,128)(2,1)S(1)} all-to-all(bf16[4,16,4096]{2,1,0:T(8,128)(2,1)S(1)} %project.1), channel_id=1, replica_groups=mesh['dp'=4,'kv_0'=16,'kv_1'=4,'tp'=2] {'kv_1'}, dimensions={0} | all-to-all | bytes 1048576 | tf_op jit(solution)/shard_map/all_to_all | solution.py:299
  14.7 0.3 near_sum.1
  14.9 28.4 %all_to_all.41.x = bf16[16,32,128]{2,1,0:T(8,128)(2,1)S(1)} all-to-all(bf16[16,32,128]{2,1,0:T(8,128)(2,1)S(1)} %get-tuple-element.10), channel_id=1, replica_groups=mesh['dp'=4,'kv_0'=16,'kv_1'=4,'tp'=2] {'kv_0'}, dimensions={0} | all-to-all | bytes 262144 | tf_op jit(solution)/shard_map/all_to_all | solution.py:310
  43.3 0.0 copy-done.3
  43.3 0.8 retention.1
  44.1 20.5 %all_to_all.42 = bf16[64,8,128]{2,1,0:T(8,128)(2,1)S(1)} all-to-all(bf16[64,8,128]{2,1,0:T(8,128)(2,1)S(1)} %get-tuple-element.12), channel_id=1, replica_groups=mesh['dp'=4,'kv_0'=16,'kv_1'=4,'tp'=2] {'kv_1','kv_0'}, dimensions={0} | all-to-all | bytes 262144 | tf_op jit(solution)/shard_map/all_to_all | solution.py:317
  64.5 0.0 copy-start.4
  64.5 0.0 copy-start.5
  64.5 5.4 %all-gather = bf16[128,8,128]{2,1,0:T(8,128)(2,1)S(1)} all-gather(bf16[64,8,128]{2,1,0:T(8,128)(2,1)S(1)} %all_to_all.42), channel_id=2, replica_groups=mesh['dp'=4,'kv_0'=16,'kv_1'=4,'tp'=2] {'tp'}, dimensions={0}, use_global_device_ids=true | all-gather | bytes 393216 | tf_op jit(solution)/shard_map/all_gather | solution.py:318
  69.9 0.0 copy-done.4
  69.9 0.0 copy-done.5
  69.9 0.7 mix.1
  70.6 14.7 %all_to_all.43 = bf16[16,16,128]{2,1,0:T(8,128)(2,1)S(1)} all-to-all(bf16[16,16,128]{2,1,0:T(8,128)(2,1)S(1)} %mix.1), channel_id=1, replica_groups=mesh['dp'=4,'kv_0'=16,'kv_1'=4,'tp'=2] {'kv_0'}, dimensions={0} | all-to-all | bytes 131072 | tf_op jit(solution)/shard_map/all_to_all | solution.py:327
  85.4 0.0 copy-start
  85.4 8.0 %all_to_all.44 = bf16[4,16,16,128]{3,2,1,0:T(8,128)(2,1)S(1)} all-to-all(bf16[4,16,16,128]{3,2,1,0:T(8,128)(2,1)S(1)} %broadcast_in_dim.4), channel_id=1, replica_groups=mesh['dp'=4,'kv_0'=16,'kv_1'=4,'tp'=2] {'kv_1'}, dimensions={0} | all-to-all | bytes 524288 | tf_op jit(solution)/shard_map/all_to_all | solution.py:329
  93.5 5.2 %all-gather.1 = bf16[8,16,16,128]{3,2,1,0:T(8,128)(2,1)S(1)} all-gather(bf16[4,16,16,128]{3,2,1,0:T(8,128)(2,1)S(1)} %all_to_all.44), channel_id=3, replica_groups=mesh['dp'=4,'kv_0'=16,'kv_1'=4,'tp'=2] {'tp'}, dimensions={0}, use_global_device_ids=true | all-gather | bytes 786432 | tf_op jit(solution)/shard_map/all_gather | solution.py:330
  98.6 0.0 copy-done.2
  98.7 0.0 copy-done.1
  98.7 0.0 copy-done
  98.7 0.0 copy-done.6
  98.7 1.7 %feed.1 = (bf16[64,2048]{1,0:T(8,128)(2,1)S(1)}, bf16[64,2048]{1,0:T(8,128)(2,1)S(1)}, f32[1,4096]{1,0:T(1,128)S(1)}, f32[1,8,128,128]{3,2,1,0:T(8,128)}) custom-call(bf16[2,4,16,16,128]{4,3,2,1,0:T(8,128)(2,1)S(1)} %bitcast.15, f32[1,4096]{1,0:T(1,128)S(1)} %bitcast.24, bf16[86,4096]{1,0:T(8,128)(2,1)S(1)} %bitcast.19, bf16[86,4096]{1,0:T(8,128)(2,1)S(1)} %bitcast.20, ...), custom_call_target="tpu_custom_call" | custom-call | tf_op jit(solution)/shard_map/feed/pallas_call | solution.py:332
  100.4 2.2 %all-gather.2 = bf16[128,2048]{1,0:T(8,128)(2,1)S(1)} all-gather(bf16[64,2048]{1,0:T(8,128)(2,1)S(1)} %get-tuple-element.15), channel_id=4, replica_groups=mesh['dp'=4,'kv_0'=16,'kv_1'=4,'tp'=2] {'tp'}, dimensions={0}, use_global_device_ids=true | all-gather | bytes 786432 | tf_op jit(solution)/shard_map/all_gather | solution.py:352
  102.6 0.1 pair_sum.1
  102.6 8.8 %all_to_all.45.x = bf16[4,16,2048]{2,1,0:T(8,128)(2,1)S(1)} all-to-all(bf16[4,16,2048]{2,1,0:T(8,128)(2,1)S(1)} %bitcast.18), channel_id=1, replica_groups=mesh['dp'=4,'kv_0'=16,'kv_1'=4,'tp'=2] {'kv_1'}, dimensions={0} | all-to-all | bytes 524288 | tf_op jit(solution)/shard_map/all_to_all | solution.py:354
  111.4 0.1 half_sum.1
  111.5 14.3 %all_to_all.46.x = bf16[16,16,128]{2,1,0:T(8,128)(2,1)S(1)} all-to-all(bf16[16,16,128]{2,1,0:T(8,128)(2,1)S(1)} %half_sum.1), channel_id=1, replica_groups=mesh['dp'=4,'kv_0'=16,'kv_1'=4,'tp'=2] {'kv_0'}, dimensions={0} | all-to-all | bytes 131072 | tf_op jit(solution)/shard_map/all_to_all | solution.py:362
  125.8 4.2 %all_gather.27.x = f32[32,128]{1,0:T(8,128)S(1)} all-gather(f32[16,128]{1,0:T(8,128)S(1)} %ffn_sum.1), channel_id=1, replica_groups=mesh['dp'=4,'kv_0'=16,'kv_1'=4,'tp'=2] {'tp'}, dimensions={0}, use_global_device_ids=true | all-gather | bytes 24576 | tf_op jit(solution)/shard_map/all_gather | solution.py:366
  130.0 0.0 copy-done.7
  130.0 0.2 final_norm.1
  130.2 18.2 %all_to_all.47 = f32[64,1,128]{2,1,0:T(1,128)S(1)} all-to-all(f32[64,1,128]{2,1,0:T(1,128)S(1)} %bitcast.22), channel_id=1, replica_groups={{0,2,4,6,8,10,12,14,16,18,20,22,24,26,28,30,32,34,36,38,40,42,44,46,48,..., dimensions={0} | all-to-all | bytes 65536 | tf_op jit(solution)/shard_map/all_to_all | solution.py:370
  148.4 0.7 place.1
  (7 shorter events, 0.1 us)
Async XLA Ops:
  14.7 28.7 %copy-start.3 = (f32[1,8,128,128]{3,2,1,0:T(8,128)S(1)}, f32[1,8,128,128]{3,2,1,0:T(8,128)}, u32[]{:S(2)}) copy-start(f32[1,8,128,128]{3,2,1,0:T(8,128)} %state.1) | copy-start | bytes 1572868
  64.5 5.4 %copy-start.4 = (bf16[2048,32]{0,1:T(8,128)(2,1)S(1)}, bf16[2048,32]{0,1:T(8,128)(2,1)}, u32[]{:S(2)}) copy-start(bf16[2048,32]{0,1:T(8,128)(2,1)} %param.20) | copy-start | bytes 393220
  64.5 5.4 %copy-start.5 = (bf16[64,64]{1,0:T(8,128)(2,1)S(1)}, bf16[64,64]{1,0:T(8,128)(2,1)}, u32[]{:S(2)}) copy-start(bf16[64,64]{1,0:T(8,128)(2,1)} %tok.1) | copy-start | bytes 24580
  69.9 28.7 %copy-start.2 = (bf16[86,4096]{1,0:T(8,128)(2,1)S(1)}, bf16[86,4096]{1,0:T(8,128)(2,1)}, u32[]{:S(2)}) copy-start(bf16[86,4096]{1,0:T(8,128)(2,1)} %wd.1) | copy-start | bytes 2113540
  85.4 13.3 %copy-start.1 = (bf16[4096,86]{0,1:T(8,128)(2,1)S(1)}, bf16[4096,86]{0,1:T(8,128)(2,1)}, u32[]{:S(2)}) copy-start(bf16[4096,86]{0,1:T(8,128)(2,1)} %param.23) | copy-start | bytes 2113540
  85.4 13.2 %copy-start = (bf16[4096,86]{0,1:T(8,128)(2,1)S(1)}, bf16[4096,86]{0,1:T(8,128)(2,1)}, u32[]{:S(2)}) copy-start(bf16[4096,86]{0,1:T(8,128)(2,1)} %param.22) | copy-start | bytes 2113540
  93.5 5.2 %copy-start.6 = (f32[4096]{0:T(1024)S(1)}, f32[4096]{0:T(1024)}, u32[]{:S(2)}) copy-start(f32[4096]{0:T(1024)} %param.21) | copy-start | bytes 49156
  125.8 4.2 %copy-start.7 = (f32[4096]{0:T(1024)S(1)}, f32[4096]{0:T(1024)}, u32[]{:S(2)}) copy-start(f32[4096]{0:T(1024)} %param.25) | copy-start | bytes 49156

commit v10 on v9

--- a/solution.py
+++ b/solution.py
@@ -9,7 +9,7 @@
 from jax.sharding import PartitionSpec as P
 
 KV = ("kv_0", "kv_1")
-YZ = ("kv_1", "kv_0")
+Z_TP = ("kv_0", "tp")
 KV_TP = ("kv_0", "kv_1", "tp")
 DP_KV = ("dp", "kv_0", "kv_1")
 F32 = jnp.float32
@@ -55,8 +55,20 @@
 ]
 
 
+def spot(z):
+    return (7 * z) % NZ
+
+
+Z_GROUPS = [[spot(i) * 2 + t for i in range(NZ)] for t in range(2)]
+YZ_GROUPS = [[(spot(i) * NY + y) * 2 + t for y in range(NY) for i in range(NZ)] for t in range(2)]
+
+
+def along_z(x):
+    return lax.all_to_all(x, Z_TP, 0, 0, tiled=True, axis_index_groups=Z_GROUPS)
+
+
 def rows_of(s):
-    return (s % NY) * NZ + s // NY
+    return (s % NY) * NZ + spot(s // NY)
 
 
 def perm_matrix(dtype):
@@ -69,19 +81,26 @@
     return lax.dot_general(a, b, (((ca,), (cb,)), ((), ())), preferred_element_type=F32)
 
 
-def project_kernel(position, tok_hbm, wq, wk, wv, wg, out, tok, weights, sems):
+def project_kernel(position, tok_hbm, wq, wk, wv, wg, out, tok, weights, tok_sem, sems):
     sources = (wq, wk, wv, wg)
     count = len(sources)
     width = weights.shape[2]
-    copies = [pltpu.make_async_copy(tok_hbm, tok, sems.at[count])]
+    load = pltpu.make_async_copy(tok_hbm, tok, tok_sem)
+    load.start()
+    parts = 4
+    depth = weights.shape[1] // parts
+    copies = []
     for i, w in enumerate(sources):
-        copies.append(pltpu.make_async_copy(w, weights.at[i], sems.at[i]))
-    for copy in copies:
-        copy.start()
-    copies[0].wait()
+        for j in range(parts):
+            some = pl.ds(j * depth, depth)
+            copy = pltpu.make_async_copy(w.at[some], weights.at[i, some], sems.at[i, j])
+            copy.start()
+            copies.append(copy)
+    load.wait()
     rows = mm(perm_matrix(BF16), tok[...], 1, 0).astype(BF16)
     for i in range(count):
-        copies[1 + i].wait()
+        for j in range(parts):
+            copies[i * parts + j].wait()
         part = mm(rows, weights[i], 1, 0).astype(BF16)
         out[:, :, i * width : (i + 1) * width] = part.reshape(NY, NZ, width)
 
@@ -165,14 +184,16 @@
 
 
 def feed_kernel(
-    x, gain, wg_t, wu_t, wd, state, own, other, row, state_out, wide, narrow, stats, sem
+    x, gain, wg_t, wu_t, wd, state, own, other, row, state_out, wide, narrow, stats, sems
 ):
-    keep = pltpu.make_async_copy(state, state_out, sem)
-    keep.start()
+    keeps = []
+    for h in range(state.shape[1]):
+        keeps.append(pltpu.make_async_copy(state.at[0, h], state_out.at[0, h], sems.at[h]))
+        keeps[h].start()
     tps = x.shape[0]
     per = x.shape[3]
     tp = lax.axis_index("tp")
-    place = lax.axis_index("kv_1") * NZ + lax.axis_index("kv_0")
+    place = lax.axis_index("kv_1") * NZ + spot(lax.axis_index("kv_0"))
     groups = SEQS // per
     cols = LANES // groups
     chips = groups // tps
@@ -184,7 +205,7 @@
         sources = []
         for q in range(groups):
             kv = a * chips + q // tps
-            sources.append(x[q % tps, kv % NY, kv // NY].astype(F32))
+            sources.append(x[q % tps, kv % NY, spot(kv // NY)].astype(F32))
         for g in range(groups):
             tile = sources[(groups - g) % groups]
             for j in range(1, groups):
@@ -216,7 +237,8 @@
         theirs = pl.multiple_of((1 - tp) * half + c, step)
         own[:, c : c + step] = mm(inner, wd[:, pl.ds(mine, step)], 1, 0).astype(BF16)
         other[:, c : c + step] = mm(inner, wd[:, pl.ds(theirs, step)], 1, 0).astype(BF16)
-    keep.wait()
+    for keep in keeps:
+        keep.wait()
 
 
 def pair_sum_kernel(own, both, out):
@@ -290,7 +312,8 @@
         scratch_shapes=[
             pltpu.VMEM(tokens.shape, BF16),
             pltpu.VMEM((4, *w_query.shape), BF16),
-            pltpu.SemaphoreType.DMA((5,)),
+            pltpu.SemaphoreType.DMA,
+            pltpu.SemaphoreType.DMA((4, 4)),
         ],
         compiler_params=PARAMS,
         interpret=INTERPRET,
@@ -307,14 +330,16 @@
         interpret=INTERPRET,
         name="near_sum",
     )(positions, near)
-    far = lax.all_to_all(near, "kv_0", 0, 0, tiled=True)
+    far = along_z(near)
     updated, attended = kernel_call(
         retention_kernel,
         [sds(state.shape, F32), sds((SEQS, heads, dim), BF16)],
         3,
         name="retention",
     )(far, turns, state)
-    gathered = lax.all_to_all(attended, YZ, 0, 0, tiled=True)
+    gathered = lax.all_to_all(
+        attended, KV_TP, 0, 0, tiled=True, axis_index_groups=YZ_GROUPS
+    )
     gathered = lax.all_gather(gathered, "tp", axis=0)
     per = SEQS * cols // LANES
     mixed = kernel_call(
@@ -324,7 +349,7 @@
         scratch=[pltpu.VMEM((2, SEQS, heads, dim), F32)],
         name="mix",
     )(gathered.reshape(2, SEQS, heads, dim), w_out.T, tokens)
-    rows = lax.all_to_all(mixed, "kv_0", 0, 0, tiled=True)
+    rows = along_z(mixed)
     rows = jnp.broadcast_to(rows[None], (NY, *rows.shape))
     rows = lax.all_to_all(rows, "kv_1", 0, 0, tiled=True)
     rows = lax.all_gather(rows, "tp", axis=0)
@@ -343,7 +368,7 @@
             pltpu.VMEM((SEQS, width), F32),
             pltpu.VMEM((SEQS, width), BF16),
             pltpu.VMEM((2, SEQS, LANES), F32),
-            pltpu.SemaphoreType.DMA,
+            pltpu.SemaphoreType.DMA((heads,)),
         ],
         compiler_params=PARAMS,
         interpret=INTERPRET,
@@ -359,7 +384,7 @@
         scratch=[pltpu.VMEM((NZ, lines, LANES), F32)],
         name="half_sum",
     )(part)
-    part = lax.all_to_all(part, "kv_0", 0, 0, tiled=True)
+    part = along_z(part)
     summed = kernel_call(ffn_sum_kernel, sds((lines, LANES), F32), 2, name="ffn_sum")(
         part, hidden_row.reshape(2 * lines, LANES)
     )

time: 150 us -> 150 us (level)
  no operation moved by 1% of the time
where the time goes in v10:
time: 150 us
  blocking collectives  142 us (95%)
  Pallas kernels  6.79 us (5%)
    all_to_all x3, blocking collectives, along_z(): return lax.all_to_all(x, Z_TP, 0, 0, tiled=True, axis_index_groups=Z_GROUPS)  57.3 us
    all_to_all x1, blocking collectives, on_device(): lax.all_to_all(attended, KV_TP, 0, 0, tiled=True, axis_index_groups=YZ_GR...  20.5 us
    all_to_all x1, blocking collectives, on_device(): lax.all_to_all(spread.reshape(SEQS, 1, LANES), KV_TP, 0, 0, tiled=True, a...  18.5 us
    all_to_all x1, blocking collectives, on_device(): near = lax.all_to_all(parts, 'kv_1', 0, 0, tiled=True)  11.7 us
    all_to_all x1, blocking collectives, on_device(): part = lax.all_to_all(part.reshape(NY, NZ, half), 'kv_1', 0, 0, tiled=True)  8.78 us
    all_to_all x1, blocking collectives, on_device(): rows = lax.all_to_all(rows, 'kv_1', 0, 0, tiled=True)  8.05 us
    all_gather x1, blocking collectives, on_device(): gathered = lax.all_gather(gathered, 'tp', axis=0)  5.84 us
    all_gather x1, blocking collectives, on_device(): rows = lax.all_gather(rows, 'tp', axis=0)  4.8 us

profile of v10, /device:TPU:1, one launch (start us, length us, event | category | flops | bytes accessed | tf_op | source)
XLA Modules:
  0.0 149.8 jit_solution(16776269293578386548)
XLA Ops:
  1.3 1.9 %project.1 = bf16[4,16,4096]{2,1,0:T(8,128)(2,1)S(1)} custom-call(s32[1]{0:T(128)S(6)} %copy.16.position, bf16[64,64]{1,0:T(8,128)(2,1)} %tok.1, bf16[64,1024]{1,0:T(8,128)(2,1)} %wq.1, bf16[64,1024]{1,0:T(8,128)(2,1)} %wk.1, bf16[64,1024]{1,0:T(8,128)(2,1)} %wv.1, bf16[64,1024]{1,0:T(8,128)(2,1)} %wg.1), custom_call_target="tpu_custom_call" | custom-call | tf_op jit(solution)/shard_map/project/pallas_call | solution.py:307
  3.2 11.7 %all_to_all.40.x = bf16[4,16,4096]{2,1,0:T(8,128)(2,1)S(1)} all-to-all(bf16[4,16,4096]{2,1,0:T(8,128)(2,1)S(1)} %project.1), channel_id=1, replica_groups=mesh['dp'=4,'kv_0'=16,'kv_1'=4,'tp'=2] {'kv_1'}, dimensions={0} | all-to-all | bytes 1048576 | tf_op jit(solution)/shard_map/all_to_all | solution.py:322
  14.9 0.0 copy-start.3
  14.9 0.3 near_sum.1
  15.2 28.2 %all_to_all.41.x = bf16[16,32,128]{2,1,0:T(8,128)(2,1)S(1)} all-to-all(bf16[16,32,128]{2,1,0:T(8,128)(2,1)S(1)} %get-tuple-element.10), channel_id=1, replica_groups={{0,56,112,40,96,24,80,8,64,120,48,104,32,88,16,72},{1,57,113,41,97,25,8..., dimensions={0} | all-to-all | bytes 262144 | tf_op jit(solution)/shard_map/all_to_all | solution.py:67
  43.5 0.0 copy-done.3
  43.5 0.8 retention.1
  44.2 20.5 %all_to_all.42 = bf16[64,8,128]{2,1,0:T(8,128)(2,1)S(1)} all-to-all(bf16[64,8,128]{2,1,0:T(8,128)(2,1)S(1)} %get-tuple-element.12), channel_id=1, replica_groups={{0,56,112,40,96,24,80,8,64,120,48,104,32,88,16,72,2,58,114,42,98,26,82,..., dimensions={0} | all-to-all | bytes 262144 | tf_op jit(solution)/shard_map/all_to_all | solution.py:340
  64.7 0.0 copy-start.4
  64.7 5.8 %all-gather = bf16[128,8,128]{2,1,0:T(8,128)(2,1)S(1)} all-gather(bf16[64,8,128]{2,1,0:T(8,128)(2,1)S(1)} %all_to_all.42), channel_id=2, replica_groups=mesh['dp'=4,'kv_0'=16,'kv_1'=4,'tp'=2] {'tp'}, dimensions={0}, use_global_device_ids=true | all-gather | bytes 393216 | tf_op jit(solution)/shard_map/all_gather | solution.py:343
  70.6 0.0 copy-done.4
  70.6 0.0 copy-done.5
  70.6 0.7 mix.1
  71.3 14.5 %all_to_all.43 = bf16[16,16,128]{2,1,0:T(8,128)(2,1)S(1)} all-to-all(bf16[16,16,128]{2,1,0:T(8,128)(2,1)S(1)} %mix.1), channel_id=1, replica_groups={{0,56,112,40,96,24,80,8,64,120,48,104,32,88,16,72},{1,57,113,41,97,25,8..., dimensions={0} | all-to-all | bytes 131072 | tf_op jit(solution)/shard_map/all_to_all | solution.py:67
  85.8 0.0 copy-start
  85.8 8.0 %all_to_all.44 = bf16[4,16,16,128]{3,2,1,0:T(8,128)(2,1)S(1)} all-to-all(bf16[4,16,16,128]{3,2,1,0:T(8,128)(2,1)S(1)} %broadcast_in_dim.4), channel_id=1, replica_groups=mesh['dp'=4,'kv_0'=16,'kv_1'=4,'tp'=2] {'kv_1'}, dimensions={0} | all-to-all | bytes 524288 | tf_op jit(solution)/shard_map/all_to_all | solution.py:354
  93.9 4.8 %all-gather.1 = bf16[8,16,16,128]{3,2,1,0:T(8,128)(2,1)S(1)} all-gather(bf16[4,16,16,128]{3,2,1,0:T(8,128)(2,1)S(1)} %all_to_all.44), channel_id=3, replica_groups=mesh['dp'=4,'kv_0'=16,'kv_1'=4,'tp'=2] {'tp'}, dimensions={0}, use_global_device_ids=true | all-gather | bytes 786432 | tf_op jit(solution)/shard_map/all_gather | solution.py:355
  98.7 0.0 copy-done.2
  98.7 0.0 copy-done.1
  98.7 0.0 copy-done
  98.7 0.0 copy-done.6
  98.7 2.0 %feed.1 = (bf16[64,2048]{1,0:T(8,128)(2,1)S(1)}, bf16[64,2048]{1,0:T(8,128)(2,1)S(1)}, f32[1,4096]{1,0:T(1,128)S(1)}, f32[1,8,128,128]{3,2,1,0:T(8,128)}) custom-call(bf16[2,4,16,16,128]{4,3,2,1,0:T(8,128)(2,1)S(1)} %bitcast.15, f32[1,4096]{1,0:T(1,128)S(1)} %bitcast.24, bf16[86,4096]{1,0:T(8,128)(2,1)S(1)} %bitcast.19, bf16[86,4096]{1,0:T(8,128)(2,1)S(1)} %bitcast.20, ...), custom_call_target="tpu_custom_call" | custom-call | tf_op jit(solution)/shard_map/feed/pallas_call | solution.py:357
  100.7 2.2 %all-gather.2 = bf16[128,2048]{1,0:T(8,128)(2,1)S(1)} all-gather(bf16[64,2048]{1,0:T(8,128)(2,1)S(1)} %get-tuple-element.15), channel_id=4, replica_groups=mesh['dp'=4,'kv_0'=16,'kv_1'=4,'tp'=2] {'tp'}, dimensions={0}, use_global_device_ids=true | all-gather | bytes 786432 | tf_op jit(solution)/shard_map/all_gather | solution.py:377
  102.9 0.1 pair_sum.1
  102.9 8.8 %all_to_all.45.x = bf16[4,16,2048]{2,1,0:T(8,128)(2,1)S(1)} all-to-all(bf16[4,16,2048]{2,1,0:T(8,128)(2,1)S(1)} %bitcast.18), channel_id=1, replica_groups=mesh['dp'=4,'kv_0'=16,'kv_1'=4,'tp'=2] {'kv_1'}, dimensions={0} | all-to-all | bytes 524288 | tf_op jit(solution)/shard_map/all_to_all | solution.py:379
  111.7 0.1 half_sum.1
  111.8 14.6 %all_to_all.46.x = bf16[16,16,128]{2,1,0:T(8,128)(2,1)S(1)} all-to-all(bf16[16,16,128]{2,1,0:T(8,128)(2,1)S(1)} %half_sum.1), channel_id=1, replica_groups={{0,56,112,40,96,24,80,8,64,120,48,104,32,88,16,72},{1,57,113,41,97,25,8..., dimensions={0} | all-to-all | bytes 131072 | tf_op jit(solution)/shard_map/all_to_all | solution.py:67
  126.5 4.0 %all_gather.27.x = f32[32,128]{1,0:T(8,128)S(1)} all-gather(f32[16,128]{1,0:T(8,128)S(1)} %ffn_sum.1), channel_id=1, replica_groups=mesh['dp'=4,'kv_0'=16,'kv_1'=4,'tp'=2] {'tp'}, dimensions={0}, use_global_device_ids=true | all-gather | bytes 24576 | tf_op jit(solution)/shard_map/all_gather | solution.py:391
  130.4 0.0 copy-done.7
  130.4 0.2 final_norm.1
  130.6 18.5 %all_to_all.47 = f32[64,1,128]{2,1,0:T(1,128)S(1)} all-to-all(f32[64,1,128]{2,1,0:T(1,128)S(1)} %bitcast.22), channel_id=1, replica_groups={{0,2,4,6,8,10,12,14,16,18,20,22,24,26,28,30,32,34,36,38,40,42,44,46,48,..., dimensions={0} | all-to-all | bytes 65536 | tf_op jit(solution)/shard_map/all_to_all | solution.py:395
  149.1 0.7 place.1
  (7 shorter events, 0.1 us)
Async XLA Ops:
  14.9 28.5 %copy-start.3 = (f32[1,8,128,128]{3,2,1,0:T(8,128)S(1)}, f32[1,8,128,128]{3,2,1,0:T(8,128)}, u32[]{:S(2)}) copy-start(f32[1,8,128,128]{3,2,1,0:T(8,128)} %state.1) | copy-start | bytes 1572868
  64.7 5.8 %copy-start.4 = (bf16[2048,32]{0,1:T(8,128)(2,1)S(1)}, bf16[2048,32]{0,1:T(8,128)(2,1)}, u32[]{:S(2)}) copy-start(bf16[2048,32]{0,1:T(8,128)(2,1)} %param.20) | copy-start | bytes 393220
  64.7 5.8 %copy-start.5 = (bf16[64,64]{1,0:T(8,128)(2,1)S(1)}, bf16[64,64]{1,0:T(8,128)(2,1)}, u32[]{:S(2)}) copy-start(bf16[64,64]{1,0:T(8,128)(2,1)} %tok.1) | copy-start | bytes 24580
  70.6 28.1 %copy-start.2 = (bf16[86,4096]{1,0:T(8,128)(2,1)S(1)}, bf16[86,4096]{1,0:T(8,128)(2,1)}, u32[]{:S(2)}) copy-start(bf16[86,4096]{1,0:T(8,128)(2,1)} %wd.1) | copy-start | bytes 2113540
  85.8 12.9 %copy-start.1 = (bf16[4096,86]{0,1:T(8,128)(2,1)S(1)}, bf16[4096,86]{0,1:T(8,128)(2,1)}, u32[]{:S(2)}) copy-start(bf16[4096,86]{0,1:T(8,128)(2,1)} %param.23) | copy-start | bytes 2113540
  85.8 12.9 %copy-start = (bf16[4096,86]{0,1:T(8,128)(2,1)S(1)}, bf16[4096,86]{0,1:T(8,128)(2,1)}, u32[]{:S(2)}) copy-start(bf16[4096,86]{0,1:T(8,128)(2,1)} %param.22) | copy-start | bytes 2113540
  93.9 4.8 %copy-start.6 = (f32[4096]{0:T(1024)S(1)}, f32[4096]{0:T(1024)}, u32[]{:S(2)}) copy-start(f32[4096]{0:T(1024)} %param.21) | copy-start | bytes 49156
  126.4 4.0 %copy-start.7 = (f32[4096]{0:T(1024)S(1)}, f32[4096]{0:T(1024)}, u32[]{:S(2)}) copy-start(f32[4096]{0:T(1024)} %param.25) | copy-start | bytes 49156

commit v11 on v9

--- a/solution.py
+++ b/solution.py
@@ -9,7 +9,7 @@
 from jax.sharding import PartitionSpec as P
 
 KV = ("kv_0", "kv_1")
-YZ = ("kv_1", "kv_0")
+Z_TP = ("kv_0", "tp")
 KV_TP = ("kv_0", "kv_1", "tp")
 DP_KV = ("dp", "kv_0", "kv_1")
 F32 = jnp.float32
@@ -55,8 +55,19 @@
 ]
 
 
+def spot(z):
+    return (7 * z) % NZ
+
+
+Z_GROUPS = [[spot(i) * 2 + t for i in range(NZ)] for t in range(2)]
+
+
+def along_z(x):
+    return lax.all_to_all(x, Z_TP, 0, 0, tiled=True, axis_index_groups=Z_GROUPS)
+
+
 def rows_of(s):
-    return (s % NY) * NZ + s // NY
+    return (s % NY) * NZ + spot(s // NY)
 
 
 def perm_matrix(dtype):
@@ -143,7 +154,10 @@
     tps, seqs, heads, dim = x.shape
     cols = w_t.shape[0]
     groups = LANES // cols
-    wide[...] = x[...].astype(F32)
+    for t in range(tps):
+        for y in range(NY):
+            for z in range(NZ):
+                wide[t, y * NZ + spot(z)] = x[t, y * NZ + z].astype(F32)
     own = lax.broadcasted_iota(jnp.int32, (tok.shape[1], LANES), 0)
     lane = lax.broadcasted_iota(jnp.int32, (tok.shape[1], LANES), 1)
     pick = (own == tp * cols + lane % cols).astype(F32).astype(BF16)
@@ -168,11 +182,10 @@
     x, gain, wg_t, wu_t, wd, state, own, other, row, state_out, wide, narrow, stats, sem
 ):
     keep = pltpu.make_async_copy(state, state_out, sem)
-    keep.start()
     tps = x.shape[0]
     per = x.shape[3]
     tp = lax.axis_index("tp")
-    place = lax.axis_index("kv_1") * NZ + lax.axis_index("kv_0")
+    place = lax.axis_index("kv_1") * NZ + spot(lax.axis_index("kv_0"))
     groups = SEQS // per
     cols = LANES // groups
     chips = groups // tps
@@ -184,7 +197,7 @@
         sources = []
         for q in range(groups):
             kv = a * chips + q // tps
-            sources.append(x[q % tps, kv % NY, kv // NY].astype(F32))
+            sources.append(x[q % tps, kv % NY, spot(kv // NY)].astype(F32))
         for g in range(groups):
             tile = sources[(groups - g) % groups]
             for j in range(1, groups):
@@ -194,6 +207,7 @@
             wide[g * per : (g + 1) * per, a * LANES : (a + 1) * LANES] = tile
             sums[g] += tile
             squares[g] += tile * tile
+    keep.start()
     mean = jnp.sum(jnp.concatenate(sums, 0), -1, keepdims=True) / width
     var = jnp.sum(jnp.concatenate(squares, 0), -1, keepdims=True) / width - mean * mean
     scale = lax.rsqrt(var + 1e-05)
@@ -307,14 +321,14 @@
         interpret=INTERPRET,
         name="near_sum",
     )(positions, near)
-    far = lax.all_to_all(near, "kv_0", 0, 0, tiled=True)
+    far = along_z(near)
     updated, attended = kernel_call(
         retention_kernel,
         [sds(state.shape, F32), sds((SEQS, heads, dim), BF16)],
         3,
         name="retention",
     )(far, turns, state)
-    gathered = lax.all_to_all(attended, YZ, 0, 0, tiled=True)
+    gathered = lax.all_to_all(attended, ("kv_1", "kv_0"), 0, 0, tiled=True)
     gathered = lax.all_gather(gathered, "tp", axis=0)
     per = SEQS * cols // LANES
     mixed = kernel_call(
@@ -324,7 +338,7 @@
         scratch=[pltpu.VMEM((2, SEQS, heads, dim), F32)],
         name="mix",
     )(gathered.reshape(2, SEQS, heads, dim), w_out.T, tokens)
-    rows = lax.all_to_all(mixed, "kv_0", 0, 0, tiled=True)
+    rows = along_z(mixed)
     rows = jnp.broadcast_to(rows[None], (NY, *rows.shape))
     rows = lax.all_to_all(rows, "kv_1", 0, 0, tiled=True)
     rows = lax.all_gather(rows, "tp", axis=0)
@@ -359,7 +373,7 @@
         scratch=[pltpu.VMEM((NZ, lines, LANES), F32)],
         name="half_sum",
     )(part)
-    part = lax.all_to_all(part, "kv_0", 0, 0, tiled=True)
+    part = along_z(part)
     summed = kernel_call(ffn_sum_kernel, sds((lines, LANES), F32), 2, name="ffn_sum")(
         part, hidden_row.reshape(2 * lines, LANES)
     )

time: 150 us -> 150 us (level)
  no operation moved by 1% of the time
where the time goes in v11:
time: 150 us; the launch traced here: 149 us
  blocking collectives  141 us (94%)
  Pallas kernels  6.2 us (4%)
    all_to_all x3, blocking collectives, along_z(): return lax.all_to_all(x, Z_TP, 0, 0, tiled=True, axis_index_groups=Z_GROUPS)  57.3 us
    all_to_all x1, blocking collectives, on_device(): gathered = lax.all_to_all(attended, ('kv_1', 'kv_0'), 0, 0, tiled=True)  20.6 us
    all_to_all x1, blocking collectives, on_device(): lax.all_to_all(spread.reshape(SEQS, 1, LANES), KV_TP, 0, 0, tiled=True, a...  18.5 us
    all_to_all x1, blocking collectives, on_device(): near = lax.all_to_all(parts, 'kv_1', 0, 0, tiled=True)  11.7 us
    all_to_all x1, blocking collectives, on_device(): part = lax.all_to_all(part.reshape(NY, NZ, half), 'kv_1', 0, 0, tiled=True)  8.78 us
    all_to_all x1, blocking collectives, on_device(): rows = lax.all_to_all(rows, 'kv_1', 0, 0, tiled=True)  8.05 us
    all_gather x1, blocking collectives, on_device(): gathered = lax.all_gather(gathered, 'tp', axis=0)  5.38 us
    all_gather x1, blocking collectives, on_device(): rows = lax.all_gather(rows, 'tp', axis=0)  5.04 us

profile of v11, /device:TPU:1, one launch (start us, length us, event | category | flops | bytes accessed | tf_op | source)
XLA Modules:
  0.0 149.1 jit_solution(345613558176400677)
XLA Ops:
  1.3 1.6 %project.1 = bf16[4,16,4096]{2,1,0:T(8,128)(2,1)S(1)} custom-call(s32[1]{0:T(128)S(6)} %copy.16.position, bf16[64,64]{1,0:T(8,128)(2,1)} %tok.1, bf16[64,1024]{1,0:T(8,128)(2,1)} %wq.1, bf16[64,1024]{1,0:T(8,128)(2,1)} %wk.1, bf16[64,1024]{1,0:T(8,128)(2,1)} %wv.1, bf16[64,1024]{1,0:T(8,128)(2,1)} %wg.1), custom_call_target="tpu_custom_call" | custom-call | tf_op jit(solution)/shard_map/project/pallas_call | solution.py:299
  2.9 11.7 %all_to_all.40.x = bf16[4,16,4096]{2,1,0:T(8,128)(2,1)S(1)} all-to-all(bf16[4,16,4096]{2,1,0:T(8,128)(2,1)S(1)} %project.1), channel_id=1, replica_groups=mesh['dp'=4,'kv_0'=16,'kv_1'=4,'tp'=2] {'kv_1'}, dimensions={0} | all-to-all | bytes 1048576 | tf_op jit(solution)/shard_map/all_to_all | solution.py:313
  14.7 0.0 copy-start.3
  14.7 0.3 near_sum.1
  14.9 28.2 %all_to_all.41.x = bf16[16,32,128]{2,1,0:T(8,128)(2,1)S(1)} all-to-all(bf16[16,32,128]{2,1,0:T(8,128)(2,1)S(1)} %get-tuple-element.10), channel_id=1, replica_groups={{0,56,112,40,96,24,80,8,64,120,48,104,32,88,16,72},{1,57,113,41,97,25,8..., dimensions={0} | all-to-all | bytes 262144 | tf_op jit(solution)/shard_map/all_to_all | solution.py:66
  43.2 0.0 copy-done.3
  43.2 0.8 retention.1
  43.9 20.6 %all_to_all.42 = bf16[64,8,128]{2,1,0:T(8,128)(2,1)S(1)} all-to-all(bf16[64,8,128]{2,1,0:T(8,128)(2,1)S(1)} %get-tuple-element.12), channel_id=1, replica_groups=mesh['dp'=4,'kv_0'=16,'kv_1'=4,'tp'=2] {'kv_1','kv_0'}, dimensions={0} | all-to-all | bytes 262144 | tf_op jit(solution)/shard_map/all_to_all | solution.py:331
  64.5 0.0 copy-start.4
  64.5 5.4 %all-gather = bf16[128,8,128]{2,1,0:T(8,128)(2,1)S(1)} all-gather(bf16[64,8,128]{2,1,0:T(8,128)(2,1)S(1)} %all_to_all.42), channel_id=2, replica_groups=mesh['dp'=4,'kv_0'=16,'kv_1'=4,'tp'=2] {'tp'}, dimensions={0}, use_global_device_ids=true | all-gather | bytes 393216 | tf_op jit(solution)/shard_map/all_gather | solution.py:332
  69.9 0.0 copy-done.4
  69.9 0.0 copy-done.5
  69.9 0.7 mix.1
  70.6 14.7 %all_to_all.43 = bf16[16,16,128]{2,1,0:T(8,128)(2,1)S(1)} all-to-all(bf16[16,16,128]{2,1,0:T(8,128)(2,1)S(1)} %mix.1), channel_id=1, replica_groups={{0,56,112,40,96,24,80,8,64,120,48,104,32,88,16,72},{1,57,113,41,97,25,8..., dimensions={0} | all-to-all | bytes 131072 | tf_op jit(solution)/shard_map/all_to_all | solution.py:66
  85.4 0.0 copy-start
  85.4 8.0 %all_to_all.44 = bf16[4,16,16,128]{3,2,1,0:T(8,128)(2,1)S(1)} all-to-all(bf16[4,16,16,128]{3,2,1,0:T(8,128)(2,1)S(1)} %broadcast_in_dim.4), channel_id=1, replica_groups=mesh['dp'=4,'kv_0'=16,'kv_1'=4,'tp'=2] {'kv_1'}, dimensions={0} | all-to-all | bytes 524288 | tf_op jit(solution)/shard_map/all_to_all | solution.py:343
  93.4 5.0 %all-gather.1 = bf16[8,16,16,128]{3,2,1,0:T(8,128)(2,1)S(1)} all-gather(bf16[4,16,16,128]{3,2,1,0:T(8,128)(2,1)S(1)} %all_to_all.44), channel_id=3, replica_groups=mesh['dp'=4,'kv_0'=16,'kv_1'=4,'tp'=2] {'tp'}, dimensions={0}, use_global_device_ids=true | all-gather | bytes 786432 | tf_op jit(solution)/shard_map/all_gather | solution.py:344
  98.5 0.0 copy-done.2
  98.5 0.0 copy-done.1
  98.5 0.0 copy-done
  98.5 0.0 copy-done.6
  98.5 1.7 %feed.1 = (bf16[64,2048]{1,0:T(8,128)(2,1)S(1)}, bf16[64,2048]{1,0:T(8,128)(2,1)S(1)}, f32[1,4096]{1,0:T(1,128)S(1)}, f32[1,8,128,128]{3,2,1,0:T(8,128)}) custom-call(bf16[2,4,16,16,128]{4,3,2,1,0:T(8,128)(2,1)S(1)} %bitcast.15, f32[1,4096]{1,0:T(1,128)S(1)} %bitcast.24, bf16[86,4096]{1,0:T(8,128)(2,1)S(1)} %bitcast.19, bf16[86,4096]{1,0:T(8,128)(2,1)S(1)} %bitcast.20, ...), custom_call_target="tpu_custom_call" | custom-call | tf_op jit(solution)/shard_map/feed/pallas_call | solution.py:346
  100.2 2.2 %all-gather.2 = bf16[128,2048]{1,0:T(8,128)(2,1)S(1)} all-gather(bf16[64,2048]{1,0:T(8,128)(2,1)S(1)} %get-tuple-element.15), channel_id=4, replica_groups=mesh['dp'=4,'kv_0'=16,'kv_1'=4,'tp'=2] {'tp'}, dimensions={0}, use_global_device_ids=true | all-gather | bytes 786432 | tf_op jit(solution)/shard_map/all_gather | solution.py:366
  102.4 0.1 pair_sum.1
  102.4 8.8 %all_to_all.45.x = bf16[4,16,2048]{2,1,0:T(8,128)(2,1)S(1)} all-to-all(bf16[4,16,2048]{2,1,0:T(8,128)(2,1)S(1)} %bitcast.18), channel_id=1, replica_groups=mesh['dp'=4,'kv_0'=16,'kv_1'=4,'tp'=2] {'kv_1'}, dimensions={0} | all-to-all | bytes 524288 | tf_op jit(solution)/shard_map/all_to_all | solution.py:368
  111.2 0.1 half_sum.1
  111.3 14.4 %all_to_all.46.x = bf16[16,16,128]{2,1,0:T(8,128)(2,1)S(1)} all-to-all(bf16[16,16,128]{2,1,0:T(8,128)(2,1)S(1)} %half_sum.1), channel_id=1, replica_groups={{0,56,112,40,96,24,80,8,64,120,48,104,32,88,16,72},{1,57,113,41,97,25,8..., dimensions={0} | all-to-all | bytes 131072 | tf_op jit(solution)/shard_map/all_to_all | solution.py:66
  125.7 4.0 %all_gather.27.x = f32[32,128]{1,0:T(8,128)S(1)} all-gather(f32[16,128]{1,0:T(8,128)S(1)} %ffn_sum.1), channel_id=1, replica_groups=mesh['dp'=4,'kv_0'=16,'kv_1'=4,'tp'=2] {'tp'}, dimensions={0}, use_global_device_ids=true | all-gather | bytes 24576 | tf_op jit(solution)/shard_map/all_gather | solution.py:380
  129.7 0.0 copy-done.7
  129.7 0.2 final_norm.1
  129.9 18.5 %all_to_all.47 = f32[64,1,128]{2,1,0:T(1,128)S(1)} all-to-all(f32[64,1,128]{2,1,0:T(1,128)S(1)} %bitcast.22), channel_id=1, replica_groups={{0,2,4,6,8,10,12,14,16,18,20,22,24,26,28,30,32,34,36,38,40,42,44,46,48,..., dimensions={0} | all-to-all | bytes 65536 | tf_op jit(solution)/shard_map/all_to_all | solution.py:384
  148.4 0.7 place.1
  (7 shorter events, 0.1 us)
Async XLA Ops:
  14.7 28.5 %copy-start.3 = (f32[1,8,128,128]{3,2,1,0:T(8,128)S(1)}, f32[1,8,128,128]{3,2,1,0:T(8,128)}, u32[]{:S(2)}) copy-start(f32[1,8,128,128]{3,2,1,0:T(8,128)} %state.1) | copy-start | bytes 1572868
  64.5 5.4 %copy-start.4 = (bf16[2048,32]{0,1:T(8,128)(2,1)S(1)}, bf16[2048,32]{0,1:T(8,128)(2,1)}, u32[]{:S(2)}) copy-start(bf16[2048,32]{0,1:T(8,128)(2,1)} %param.20) | copy-start | bytes 393220
  64.5 5.4 %copy-start.5 = (bf16[64,64]{1,0:T(8,128)(2,1)S(1)}, bf16[64,64]{1,0:T(8,128)(2,1)}, u32[]{:S(2)}) copy-start(bf16[64,64]{1,0:T(8,128)(2,1)} %tok.1) | copy-start | bytes 24580
  69.9 28.6 %copy-start.2 = (bf16[86,4096]{1,0:T(8,128)(2,1)S(1)}, bf16[86,4096]{1,0:T(8,128)(2,1)}, u32[]{:S(2)}) copy-start(bf16[86,4096]{1,0:T(8,128)(2,1)} %wd.1) | copy-start | bytes 2113540
  85.3 13.1 %copy-start.1 = (bf16[4096,86]{0,1:T(8,128)(2,1)S(1)}, bf16[4096,86]{0,1:T(8,128)(2,1)}, u32[]{:S(2)}) copy-start(bf16[4096,86]{0,1:T(8,128)(2,1)} %param.23) | copy-start | bytes 2113540
  85.4 13.1 %copy-start = (bf16[4096,86]{0,1:T(8,128)(2,1)S(1)}, bf16[4096,86]{0,1:T(8,128)(2,1)}, u32[]{:S(2)}) copy-start(bf16[4096,86]{0,1:T(8,128)(2,1)} %param.22) | copy-start | bytes 2113540
  93.4 5.0 %copy-start.6 = (f32[4096]{0:T(1024)S(1)}, f32[4096]{0:T(1024)}, u32[]{:S(2)}) copy-start(f32[4096]{0:T(1024)} %param.21) | copy-start | bytes 49156
  125.7 4.0 %copy-start.7 = (f32[4096]{0:T(1024)S(1)}, f32[4096]{0:T(1024)}, u32[]{:S(2)}) copy-start(f32[4096]{0:T(1024)} %param.25) | copy-start | bytes 49156
